TPU v7x, 256 devices: a whole 4x4x8 slice. The times are simulated.
256 devices in a mesh: sp: 64 (over z, x, core), tp: 4 (over y).
Axes of the slice: x: 4, y: 4, z: 8, core: 2. Of those that a mesh axis runs over, the one named last changes fastest.
Arguments:
- stream: bfloat16 [24576, 2048], P(('sp', 'tp')), may hold values from -6 to 6
- query_narrow: bfloat16 [24576, 512], P('sp', 'tp'), may hold values from -6 to 6
- key_narrow: bfloat16 [24576, 512], P('sp', 'tp'), may hold values from -6.5 to 6.5
- query_wide: bfloat16 [24576, 1024], P('sp', 'tp'), may hold values from -6 to 6
- key_wide: bfloat16 [24576, 1024], P('sp', 'tp'), may hold values from -6.5 to 6.5
- values: bfloat16 [24576, 2, 1024], P('sp', None, 'tp'), may hold values from -6 to 6
- out_gate: bfloat16 [24576, 2, 1024], P('sp', None, 'tp'), may hold values from -6 to 6
- out_weight: bfloat16 [2, 1024, 2048], P(None, 'tp'), may hold values from -0.125 to 0.125
- norm_gain: float32 [2048], replicated, may hold values from 0.1 to 1.9
- mlp_gate: bfloat16 [2048, 5632], P('sp', 'tp'), may hold values from -0.125 to 0.125
- mlp_up: bfloat16 [2048, 5632], P('sp', 'tp'), may hold values from -0.125 to 0.125
- mlp_down: bfloat16 [5632, 2048], P('tp', 'sp'), may hold values from -0.15625 to 0.15625
- log_decay: float32 [2, 2, 8], P(None, None, 'tp'), as said below
Outputs:
- layer_out: bfloat16 [24576, 2048], P(('sp', 'tp'))
Inputs may be any that keep to these rules, and one draw needn't show every extreme that they name: `log_decay`: every entry is negative, with magnitude at least 0.5 / 24576.
All inputs are finite; a program needn't handle non-finite values.
Results may differ from a plain program's by a relative error of at most 0.013.
Values may be sent and summed in bfloat16 or wider, within the bound.
No kernel may reach another device: no remote copies, remote signals or barrier semaphores. Data moves between devices by JAX's collectives and lax.ppermute only.
A program may use at most 128 MiB of HBM per device.

v0:
```python
import jax
import jax.numpy as jnp
from jax import lax
from jax.sharding import Mesh
from jax.sharding import PartitionSpec as P

BLOCK = 128
SP = ("sp_0", "sp_1", "sp_2")
SP_TP = ("sp_0", "sp_1", "sp_2", "tp")


NORM_EPSILON = 1e-06
ROPE_BASE = 10000.0


def gather_turned(arrays, axis, dims):
    turned = [jnp.moveaxis(a, dim, 0) for a, dim in zip(arrays, dims)]
    both = jnp.concatenate([t.reshape(len(t), -1) for t in turned], axis=1)
    whole, at, finished = (lax.all_gather(both, axis, axis=0, tiled=True), 0, [])
    for t, dim in zip(turned, dims):
        piece = whole[:, at : at + t[0].size].reshape(-1, *t.shape[1:])
        finished.append(jnp.moveaxis(piece, 0, dim))
        at += t[0].size
    return tuple(finished)


def filled_with(x, identity):
    return jax.tree.map(
        lambda part, zero: jnp.zeros_like(part) + jnp.asarray(zero, part.dtype), x, identity
    )


def all_in_one(x, axis):
    leaves = jax.tree.leaves(x)
    turns = sorted(range(len(leaves)), key=lambda k: -leaves[k].size)
    width = (1, *leaves[turns[0]].shape)[-1]
    lines = [
        jnp.pad(leaves[k].reshape(-1), (0, -leaves[k].size % width)).reshape(-1, width)
        for k in turns
    ]
    both, at, found = (lax.all_gather(jnp.concatenate(lines), axis), 0, {})
    for k, line in zip(turns, lines):
        piece = both[:, at : at + len(line)].reshape(len(both), -1)
        found[k] = piece[:, : leaves[k].size].reshape(-1, *leaves[k].shape)
        at += len(line)
    numbers = iter(range(len(leaves)))
    return jax.tree.map(lambda _: found[next(numbers)], x)


def carried_in(x, axes, combine, identity, reverse):
    before = start = filled_with(x, identity)
    subtotal = x
    for axis in reversed(axes):
        size, here = (lax.axis_size(axis), lax.axis_index(axis))
        pieces = all_in_one(subtotal, axis)
        inside, subtotal = (start, start)
        for k in reversed(range(size)) if reverse else range(size):
            passed = k > here if reverse else k < here
            subtotal = combine(subtotal, jax.tree.map(lambda part: part[k], pieces))
            inside = jax.tree.map(lambda new, old: jnp.where(passed, new, old), subtotal, inside)
        before = combine(inside, before)
    return before


def in_blocks(x, dim, size):
    lengths = x.shape
    tiles = x.reshape(*lengths[:dim], size, lengths[dim] // size, *lengths[dim + 1 :])
    return jnp.moveaxis(tiles, dim, 0)


def sum_at_owner(x, axis, dim):
    tiles = in_blocks(x, dim, lax.axis_size(axis))
    arrived = lax.all_to_all(tiles, axis, split_axis=0, concat_axis=0, tiled=True)
    return arrived.sum(axis=0)


def laid_out(tiles, dim):
    tiles = jnp.moveaxis(tiles, 0, dim)
    lengths = tiles.shape
    return tiles.reshape(*lengths[:dim], lengths[dim] * lengths[dim + 1], *lengths[dim + 2 :])


def sent_to_all(x, axis):
    size = lax.axis_size(axis)
    return lax.all_to_all(jnp.broadcast_to(x[None], (size, *x.shape)), axis, 0, 0, tiled=True)


def gathered_copies(x, axis, dim):
    return laid_out(sent_to_all(x, axis), dim)


def summed_on_arrival(x, axis, dim):
    size = lax.axis_size(axis)
    tiles = lax.all_to_all(in_blocks(x, dim, size), axis, 0, 0, tiled=True)
    return jnp.sum(tiles.astype(jnp.float32), axis=0)


def rotate(block_in, positions):
    half_size = block_in.shape[-1] // 2
    frequencies = jnp.power(ROPE_BASE, -(jnp.arange(half_size, dtype=jnp.float32) / half_size))
    angles = positions[:, None] * frequencies[None, :]
    cosine = jnp.cos(angles)[:, None, :]
    sine_table = jnp.sin(angles)[:, None, :]
    first_half = block_in[..., :half_size]
    second_half = block_in[..., half_size:]
    return jnp.concatenate(
        [
            first_half * cosine - second_half * sine_table,
            first_half * sine_table + second_half * cosine,
        ],
        -1,
    )


def decay_tables(rate_fwd, rate_bwd, block_len):
    position = jnp.arange(block_len, dtype=jnp.float32)
    offset = position[:, None] - position[None, :]
    forward_part = jnp.exp(rate_fwd[:, None, None] * jnp.maximum(offset, 0.0)[None])
    backward_part = jnp.exp(rate_bwd[:, None, None] * jnp.maximum(-offset, 0.0)[None])
    inner = jnp.where(
        offset[None] > 0, forward_part, jnp.where(offset[None] < 0, backward_part, 2.0)
    )
    keep_fwd = jnp.exp(rate_fwd[:, None] * (block_len - 1.0 - position)[None, :])
    keep_bwd = jnp.exp(rate_bwd[:, None] * position[None, :])
    reach_fwd = jnp.exp(rate_fwd[:, None] * (position + 1.0)[None, :])
    reach_bwd = jnp.exp(rate_bwd[:, None] * (block_len - position)[None, :])
    return (inner, keep_fwd, keep_bwd, reach_fwd, reach_bwd)


def local_part(query_rows, key_rows, value_rows, rate_fwd, rate_bwd, positions):
    length = query_rows.shape[0]
    head_count = rate_fwd.shape[0]
    key_size = query_rows.shape[1] // head_count
    value_size = value_rows.shape[1] // head_count
    block_count = length // BLOCK
    highest_precision = lax.Precision.HIGHEST
    query_rot = rotate(
        query_rows.astype(jnp.float32).reshape(length, head_count, key_size), positions
    ).astype(jnp.bfloat16)
    key_rot = (
        rotate(key_rows.astype(jnp.float32).reshape(length, head_count, key_size), positions)
        * key_size ** (-0.5)
    ).astype(jnp.bfloat16)
    query_blk = query_rot.reshape(block_count, BLOCK, head_count, key_size)
    key_blk = key_rot.reshape(block_count, BLOCK, head_count, key_size)
    value_blk = value_rows.reshape(block_count, BLOCK, head_count, value_size)
    inner, keep_fwd, keep_bwd, reach_fwd, reach_bwd = decay_tables(rate_fwd, rate_bwd, BLOCK)
    scores = jnp.einsum("cthk,cshk->chts", query_blk, key_blk, preferred_element_type=jnp.float32)
    weights = (scores * inner[None]).astype(jnp.bfloat16)
    inside = jnp.einsum("chts,cshv->cthv", weights, value_blk, preferred_element_type=jnp.float32)
    key_wide32 = key_blk.astype(jnp.float32)
    value_wide32 = value_blk.astype(jnp.float32)
    update_fwd = jnp.einsum(
        "cshk,cshv->chkv",
        key_wide32 * keep_fwd.T[None, :, :, None],
        value_wide32,
        precision=highest_precision,
    )
    update_bwd = jnp.einsum(
        "cshk,cshv->chkv",
        key_wide32 * keep_bwd.T[None, :, :, None],
        value_wide32,
        precision=highest_precision,
    )
    block_index = jnp.arange(block_count, dtype=jnp.float32)
    device_fwd = jnp.einsum(
        "qp,pqjl->qjl",
        jnp.exp(rate_fwd[:, None] * (BLOCK * (block_count - 1.0 - block_index))[None, :]),
        update_fwd,
        precision=highest_precision,
    )
    device_bwd = jnp.einsum(
        "qp,pqjl->qjl",
        jnp.exp(rate_bwd[:, None] * (BLOCK * block_index)[None, :]),
        update_bwd,
        precision=highest_precision,
    )
    span_fwd = jnp.exp(rate_fwd * length)
    span_bwd = jnp.exp(rate_bwd * length)
    pieces = (query_blk, inside, update_fwd, update_bwd, reach_fwd, reach_bwd)
    return (pieces, device_fwd, device_bwd, span_fwd, span_bwd)


def finish(pieces, enter_fwd, enter_bwd, rate_fwd, rate_bwd, gate_rows):
    query_blk, inside, update_fwd, update_bwd, reach_fwd, reach_bwd = pieces
    block_count = inside.shape[0]
    highest_precision = lax.Precision.HIGHEST
    block_index = jnp.arange(block_count, dtype=jnp.float32)
    block_lag = block_index[:, None] - block_index[None, :] - 1.0
    earlier_weights = jnp.where(
        block_lag[None] >= 0,
        jnp.exp(rate_fwd[:, None, None] * BLOCK * jnp.maximum(block_lag, 0.0)[None]),
        0.0,
    )
    later_weights = jnp.where(
        block_lag.T[None] >= 0,
        jnp.exp(rate_bwd[:, None, None] * BLOCK * jnp.maximum(block_lag.T, 0.0)[None]),
        0.0,
    )
    start_fwd = (
        jnp.einsum("hcd,dhkv->chkv", earlier_weights, update_fwd, precision=highest_precision)
        + jnp.exp(rate_fwd[None, :] * BLOCK * block_index[:, None])[:, :, None, None]
        * enter_fwd[None]
    )
    start_bwd = (
        jnp.einsum("hcd,dhkv->chkv", later_weights, update_bwd, precision=highest_precision)
        + jnp.exp(rate_bwd[None, :] * BLOCK * (block_count - 1.0 - block_index)[:, None])[
            :, :, None, None
        ]
        * enter_bwd[None]
    )
    query_wide32 = query_blk.astype(jnp.float32)
    carried_state = jnp.einsum(
        "cthk,chkv->cthv",
        query_wide32 * reach_fwd.T[None, :, :, None],
        start_fwd,
        precision=highest_precision,
    ) + jnp.einsum(
        "cthk,chkv->cthv",
        query_wide32 * reach_bwd.T[None, :, :, None],
        start_bwd,
        precision=highest_precision,
    )
    combined = inside + carried_state
    length = block_count * BLOCK
    combined = combined.reshape(length, combined.shape[2], combined.shape[3])
    mean_value = jnp.mean(combined, -1, keepdims=True)
    centred = combined - mean_value
    variance = jnp.mean(centred * centred, -1, keepdims=True)
    scaled = centred * lax.rsqrt(variance + NORM_EPSILON)
    gated = jax.nn.silu(gate_rows.astype(jnp.float32)).reshape(combined.shape) * scaled
    return gated.reshape(length, -1).astype(jnp.bfloat16)


def rms_scale(rows_in, gain):
    widened = rows_in.astype(jnp.float32)
    return (
        widened * lax.rsqrt(jnp.mean(widened * widened, -1, keepdims=True) + NORM_EPSILON) * gain
    ).astype(jnp.bfloat16)


def chain_step(earlier, later_part):
    return (
        earlier[0] * later_part[2][:, None, None] + later_part[0],
        earlier[1] * later_part[3][:, None, None] + later_part[1],
        earlier[2] * later_part[2],
        earlier[3] * later_part[3],
    )


def body(
    stream,
    query_narrow,
    key_narrow,
    query_wide,
    key_wide,
    values,
    out_gate,
    out_weight,
    norm_gain,
    mlp_gate,
    mlp_up,
    mlp_down,
    log_decay,
):
    full_gate, full_up, full_down = gather_turned((mlp_gate, mlp_up, mlp_down), SP, (0, 0, 1))
    length = query_narrow.shape[0]
    positions = (lax.axis_index(SP) * length + jnp.arange(length, dtype=jnp.int32)).astype(
        jnp.float32
    )
    narrow_pieces, narrow_fwd, narrow_bwd, narrow_span_fwd, narrow_span_bwd = local_part(
        query_narrow, key_narrow, values[:, 0], log_decay[0, 0], log_decay[1, 0], positions
    )
    wide_pieces, wide_fwd, wide_bwd, wide_span_fwd, wide_span_bwd = local_part(
        query_wide, key_wide, values[:, 1], log_decay[0, 1], log_decay[1, 1], positions
    )
    identity = (
        jnp.zeros_like(narrow_fwd),
        jnp.zeros_like(wide_fwd),
        jnp.ones_like(narrow_span_fwd),
        jnp.ones_like(wide_span_fwd),
    )
    enter_fwd = carried_in(
        (narrow_fwd, wide_fwd, narrow_span_fwd, wide_span_fwd), SP, chain_step, identity, False
    )
    enter_bwd = carried_in(
        (narrow_bwd, wide_bwd, narrow_span_bwd, wide_span_bwd), SP, chain_step, identity, True
    )
    narrow_out = finish(
        narrow_pieces, enter_fwd[0], enter_bwd[0], log_decay[0, 0], log_decay[1, 0], out_gate[:, 0]
    )
    wide_out = finish(
        wide_pieces, enter_fwd[1], enter_bwd[1], log_decay[0, 1], log_decay[1, 1], out_gate[:, 1]
    )
    proj_rows = sum_at_owner(
        jnp.dot(narrow_out, out_weight[0], preferred_element_type=jnp.float32)
        + jnp.dot(wide_out, out_weight[1], preferred_element_type=jnp.float32),
        "tp",
        0,
    )
    middle = (stream.astype(jnp.float32) + proj_rows).astype(jnp.bfloat16)
    normed = gathered_copies(rms_scale(middle, norm_gain), "tp", 0)
    gate_act = jnp.dot(normed, full_gate, preferred_element_type=jnp.float32)
    up_act = jnp.dot(normed, full_up, preferred_element_type=jnp.float32)
    hidden = (jax.nn.silu(gate_act) * up_act).astype(jnp.bfloat16)
    down_rows = summed_on_arrival(
        jnp.dot(hidden, full_down, preferred_element_type=jnp.float32).astype(jnp.bfloat16), "tp", 0
    )
    return (middle.astype(jnp.float32) + 0.5 * down_rows).astype(jnp.bfloat16)


def solution(mesh):
    finer = Mesh(mesh.devices.reshape(8, 4, 2, mesh.shape["tp"]), ("sp_0", "sp_1", "sp_2", "tp"))
    return jax.shard_map(
        body,
        mesh=finer,
        in_specs=(
            P(SP_TP, None),
            P(SP, "tp"),
            P(SP, "tp"),
            P(SP, "tp"),
            P(SP, "tp"),
            P(SP, None, "tp"),
            P(SP, None, "tp"),
            P(None, "tp", None),
            P(),
            P(SP, "tp"),
            P(SP, "tp"),
            P("tp", SP),
            P(None, None, "tp"),
        ),
        out_specs=P(SP_TP, None),
        check_vma=False,
    )
```

profile of v0, /device:TPU:1, one launch (start us, length us, event | category | flops | bytes accessed | tf_op | source)
XLA Modules:
  0.0 276.4 jit_solution(12559548771833271554)
XLA Ops:
  7.5 1.3 broadcast_multiply_fusion.3
  10.9 2.9 %slice_reduce_fusion = (bf16[384,256]{1,0:T(8,128)(2,1)S(1)}, bf16[384,256]{1,0:T(8,128)(2,1)S(1)}) fusion(bf16[384,2,256]{2,1,0:T(2,128)(2,1)} %param.18), kind=kLoop, calls=%fused_computation.76 | loop fusion | bytes 786432 | tf_op jit(solution)/shard_map/slice | solution.py:275
  20.3 1.1 fusion.37
  21.5 4.9 %all-gather.9 = f32[2,386,128]{2,1,0:T(8,128)S(1)} all-gather(f32[1,386,128]{2,1,0:T(8,128)S(1)} %maximum_bitcast_fusion.3), channel_id=5, replica_groups=mesh['sp_0'=8,'sp_1'=4,'sp_2'=2,'tp'=4] {'sp_2'}, dimensions={0}, use_global_device_ids=true | all-gather | bytes 592896 | tf_op jit(solution)/shard_map/all_gather | solution.py:41
  27.7 11.0 %all-gather.10 = f32[4,386,128]{2,1,0:T(8,128)S(1)} all-gather(f32[1,386,128]{2,1,0:T(8,128)S(1)} %maximum_bitcast_fusion.4), channel_id=6, replica_groups=mesh['sp_0'=8,'sp_1'=4,'sp_2'=2,'tp'=4] {'sp_1'}, dimensions={0}, use_global_device_ids=true | all-gather | bytes 988160 | tf_op jit(solution)/shard_map/all_gather | solution.py:41
  43.5 1.1 fusion.40
  44.7 5.4 %all-gather.6 = f32[2,386,128]{2,1,0:T(8,128)S(1)} all-gather(f32[1,386,128]{2,1,0:T(8,128)S(1)} %maximum_bitcast_fusion), channel_id=2, replica_groups=mesh['sp_0'=8,'sp_1'=4,'sp_2'=2,'tp'=4] {'sp_2'}, dimensions={0}, use_global_device_ids=true | all-gather | bytes 592896 | tf_op jit(solution)/shard_map/all_gather | solution.py:41
  51.1 11.4 %all-gather.7 = f32[4,386,128]{2,1,0:T(8,128)S(1)} all-gather(f32[1,386,128]{2,1,0:T(8,128)S(1)} %maximum_bitcast_fusion.1), channel_id=3, replica_groups=mesh['sp_0'=8,'sp_1'=4,'sp_2'=2,'tp'=4] {'sp_1'}, dimensions={0}, use_global_device_ids=true | all-gather | bytes 988160 | tf_op jit(solution)/shard_map/all_gather | solution.py:41
  72.0 1.7 pad_maximum_fusion
  73.8 1.6 concatenate.70
  75.4 1.7 copy.81
  77.1 1.6 concatenate.71
  78.7 1.7 copy.82
  82.8 1.3 multiply_exponential_fusion.14
  84.1 1.3 multiply_exponential_fusion.1
  90.5 1.6 select_select_fusion
  93.0 1.4 fusion.192
  96.0 26.0 %all-gather.18.cloned.1.call-done = f32[8,386,128]{2,1,0:T(8,128)} async-done(((f32[1,386,128]{2,1,0:T(8,128)}), f32[8,386,128]{2,1,0:T(8,128)}) %all-gather.18.cloned.1.call-update) | async-done | bytes 1581072 | tf_op jit(solution)/shard_map/all_gather | solution.py:41
  122.8 1.4 fusion.177
  124.9 1.2 fusion.17
  127.8 1.2 fusion.18
  134.8 1.2 fusion.178
  136.0 1.1 fusion.179
  145.7 2.0 fusion.29
  148.4 36.4 %all_to_all.15 = f32[4,96,2048]{2,1,0:T(8,128)S(1)} all-to-all(f32[4,96,2048]{2,1,0:T(8,128)S(1)} %bitcast.639), channel_id=1, replica_groups=mesh['sp_0'=8,'sp_1'=4,'sp_2'=2,'tp'=4] {'tp'}, dimensions={0} | all-to-all | bytes 6291456 | tf_op jit(solution)/shard_map/all_to_all | solution.py:73
  184.7 1.2 reduce_sum.67
  185.9 1.3 fusion.33
  187.6 17.3 %all_to_all.16 = bf16[4,96,2048]{2,1,0:T(8,128)(2,1)S(1)} all-to-all(bf16[4,96,2048]{2,1,0:T(8,128)(2,1)S(1)} %broadcast_in_dim.77), channel_id=1, replica_groups=mesh['sp_0'=8,'sp_1'=4,'sp_2'=2,'tp'=4] {'tp'}, dimensions={0} | all-to-all | bytes 3145728 | tf_op jit(solution)/shard_map/all_to_all | solution.py:85
  204.9 23.1 %all-gather.16.cloned.1.call-done = bf16[2048,4224]{1,0:T(8,128)(2,1)} async-done(((bf16[32,4224]{1,0:T(8,128)(2,1)}), bf16[2048,4224]{1,0:T(8,128)(2,1)}) %all-gather.16.cloned.1.call-update) | async-done | bytes 17301520 | tf_op jit(solution)/shard_map/all_gather | solution.py:19
  228.0 6.6 %fusion.4 = f32[384,1408]{1,0:T(8,128)} fusion(bf16[384,2048]{1,0:T(8,128)(2,1)S(1)} %bitcast.640, bf16[2048,4224]{1,0:T(8,128)(2,1)} %all-gather.16.cloned.1.call-done), kind=kOutput, calls=%fused_computation.4 | convolution fusion | flops 2214592512 | bytes 9502720 | tf_op jit(solution)/shard_map/dot_general | solution.py:303
  234.6 10.0 %fusion.12 = bf16[384,2048]{1,0:T(8,128)(2,1)S(1)} fusion(bf16[2048,4224]{1,0:T(8,128)(2,1)} %all-gather.16.cloned.1.call-done, bf16[384,2048]{1,0:T(8,128)(2,1)S(1)} %bitcast.641, f32[384,1408]{1,0:T(8,128)} %fusion.4), kind=kOutput, calls=%fused_computation.10 | convolution fusion | flops 4433215488 | bytes 16842752 | tf_op jit(solution)/shard_map/dot_general | solution.py:307
  244.6 24.1 %all_to_all.17 = bf16[4,96,2048]{2,1,0:T(8,128)(2,1)S(1)} all-to-all(bf16[4,96,2048]{2,1,0:T(8,128)(2,1)S(1)} %bitcast.642), channel_id=1, replica_groups=mesh['sp_0'=8,'sp_1'=4,'sp_2'=2,'tp'=4] {'tp'}, dimensions={0} | all-to-all | bytes 3145728 | tf_op jit(solution)/shard_map/all_to_all | solution.py:94
  (449 shorter events, 53.5 us)
Async XLA Ops:
  6.5 8.0 %copy-start.42 = (bf16[384,256]{1,0:T(8,128)(2,1)S(1)}, bf16[384,256]{1,0:T(8,128)(2,1)}, u32[]{:S(2)}) copy-start(bf16[384,256]{1,0:T(8,128)(2,1)} %param.17) | copy-start | bytes 589828
  6.5 8.2 %copy-start.43 = (bf16[384,256]{1,0:T(8,128)(2,1)S(1)}, bf16[384,256]{1,0:T(8,128)(2,1)}, u32[]{:S(2)}) copy-start(bf16[384,256]{1,0:T(8,128)(2,1)} %param.16) | copy-start | bytes 589828
  6.5 88.0 %all-gather.20.cloned.1.call-start = ((), (), s32[]{:S(2)}) async-start(), calls=%async_computation.5 | async-start | bytes 1806336 | tf_op jit(solution)/shard_map/all_gather | solution.py:41
  7.5 9.8 %copy-start.47 = (f32[2]{0:T(128)}, f32[2]{0:T(128)S(1)}, u32[]{:S(2)}) copy-start(f32[2]{0:T(128)S(1)} %get-tuple-element.161) | copy-start | bytes 28
  7.5 9.8 %copy-start.48 = (f32[2]{0:T(128)}, f32[2]{0:T(128)S(1)}, u32[]{:S(2)}) copy-start(f32[2]{0:T(128)S(1)} %get-tuple-element.162) | copy-start | bytes 28
  7.5 9.8 %copy-start.49 = (f32[2]{0:T(128)}, f32[2]{0:T(128)S(1)}, u32[]{:S(2)}) copy-start(f32[2]{0:T(128)S(1)} %get-tuple-element.163) | copy-start | bytes 28
  7.5 9.8 %copy-start.50 = (f32[2]{0:T(128)}, f32[2]{0:T(128)S(1)}, u32[]{:S(2)}) copy-start(f32[2]{0:T(128)S(1)} %get-tuple-element.164) | copy-start | bytes 28
  16.4 25.8 %copy-start = (bf16[3,128,2,128]{1,3,2,0:T(8,128)(2,1)}, bf16[3,128,2,128]{1,3,2,0:T(8,128)(2,1)S(1)}, u32[]{:S(2)}) copy-start(bf16[3,128,2,128]{1,3,2,0:T(8,128)(2,1)S(1)} %copy.83) | copy-start | bytes 589828
  17.1 24.8 %copy-start.14 = (f32[3,128,2,32]{1,3,2,0:T(8,128)}, f32[3,128,2,32]{1,3,2,0:T(8,128)S(1)}, u32[]{:S(2)}) copy-start(f32[3,128,2,32]{1,3,2,0:T(8,128)S(1)} %get-tuple-element.211) | copy-start | bytes 294916
  19.8 22.5 %copy-start.2 = (bf16[3,128,2,128]{3,1,2,0:T(8,128)(2,1)}, bf16[3,128,2,128]{3,1,2,0:T(8,128)(2,1)S(1)}, u32[]{:S(2)}) copy-start(bf16[3,128,2,128]{3,1,2,0:T(8,128)(2,1)S(1)} %fusion.54) | copy-start | bytes 589828
  26.5 12.1 %copy-start.123 = (f32[2]{0:T(128)}, f32[2]{0:T(128)S(1)}, u32[]{:S(2)}) copy-start(f32[2]{0:T(128)S(1)} %slice_bitcast_fusion.27) | copy-start | bytes 28
  41.8 80.1 %all-gather.18.cloned.1.call-start = ((), (), s32[]{:S(2)}) async-start(), calls=%async_computation.4 | async-start | bytes 1806336 | tf_op jit(solution)/shard_map/all_gather | solution.py:41
  42.3 8.7 %copy-start.8 = (f32[3,2,64,128]{3,2,1,0:T(8,128)}, f32[3,2,64,128]{3,2,1,0:T(8,128)S(1)}, u32[]{:S(2)}) copy-start(f32[3,2,64,128]{3,2,1,0:T(8,128)S(1)} %fusion.65) | copy-start | bytes 589828
  64.8 21.4 %copy-start.86 = (f32[2]{0:T(128)}, f32[2]{0:T(128)S(1)}, u32[]{:S(2)}) copy-start(f32[2]{0:T(128)S(1)} %get-tuple-element.171) | copy-start | bytes 28
  69.4 16.9 %copy-start.97 = (f32[2]{0:T(128)}, f32[2]{0:T(128)S(1)}, u32[]{:S(2)}) copy-start(f32[2]{0:T(128)S(1)} %get-tuple-element.165) | copy-start | bytes 28
  69.5 16.8 %copy-start.116 = (f32[2]{0:T(128)}, f32[2]{0:T(128)S(1)}, u32[]{:S(2)}) copy-start(f32[2]{0:T(128)S(1)} %get-tuple-element.166) | copy-start | bytes 28
  71.8 156.3 %all-gather.16.cloned.1.call-start = ((), (), s32[]{:S(2)}) async-start(), calls=%async_computation.3 | async-start | bytes 17571840 | tf_op jit(solution)/shard_map/all_gather | solution.py:19
  92.9 31.3 %copy-start.24 = (f32[1,256,128]{2,1,0:T(8,128)S(1)}, f32[1,256,128]{2,1,0:T(8,128)}, u32[]{:S(2)}) copy-start(f32[1,256,128]{2,1,0:T(8,128)} %get-tuple-element.83) | copy-start | bytes 393220
  92.9 31.3 %copy-start.25 = (f32[1,256,128]{2,1,0:T(8,128)S(1)}, f32[1,256,128]{2,1,0:T(8,128)}, u32[]{:S(2)}) copy-start(f32[1,256,128]{2,1,0:T(8,128)} %get-tuple-element.84) | copy-start | bytes 393220
  92.9 31.3 %copy-start.95 = (f32[2]{0:T(128)S(1)}, f32[2]{0:T(128)}, u32[]{:S(2)}) copy-start(f32[2]{0:T(128)} %get-tuple-element.12) | copy-start | bytes 28
  92.9 31.3 %copy-start.96 = (f32[2]{0:T(128)S(1)}, f32[2]{0:T(128)}, u32[]{:S(2)}) copy-start(f32[2]{0:T(128)} %get-tuple-element.13) | copy-start | bytes 28
  92.9 31.3 %copy-start.98 = (f32[2]{0:T(128)S(1)}, f32[2]{0:T(128)}, u32[]{:S(2)}) copy-start(f32[2]{0:T(128)} %copy-done.97) | copy-start | bytes 28
  93.0 31.3 %copy-start.115 = (f32[2]{0:T(128)S(1)}, f32[2]{0:T(128)}, u32[]{:S(2)}) copy-start(f32[2]{0:T(128)} %copy-done.114) | copy-start | bytes 28
  93.0 31.3 %copy-start.117 = (f32[2]{0:T(128)S(1)}, f32[2]{0:T(128)}, u32[]{:S(2)}) copy-start(f32[2]{0:T(128)} %copy-done.116) | copy-start | bytes 28
  93.0 31.3 %copy-start.119 = (f32[2]{0:T(128)S(1)}, f32[2]{0:T(128)}, u32[]{:S(2)}) copy-start(f32[2]{0:T(128)} %copy-done.118) | copy-start | bytes 28
  93.0 31.3 %copy-start.121 = (f32[2]{0:T(128)S(1)}, f32[2]{0:T(128)}, u32[]{:S(2)}) copy-start(f32[2]{0:T(128)} %copy-done.120) | copy-start | bytes 28
  93.0 31.3 %copy-start.130 = (f32[2]{0:T(128)S(1)}, f32[2]{0:T(128)}, u32[]{:S(2)}) copy-start(f32[2]{0:T(128)} %copy-done.129) | copy-start | bytes 28
  94.5 30.2 %copy-start.44 = (f32[3,3]{1,0:T(4,128)S(1)}, f32[3,3]{1,0:T(4,128)}, u32[]{:S(2)}) copy-start(f32[3,3]{1,0:T(4,128)} %fusion.139) | copy-start | bytes 112
  94.5 30.2 %copy-start.53 = (f32[2]{0:T(128)S(1)}, f32[2]{0:T(128)}, u32[]{:S(2)}) copy-start(f32[2]{0:T(128)} %get-tuple-element.148) | copy-start | bytes 28
  94.5 30.2 %copy-start.58 = (f32[3,2]{0,1:T(2,128)S(1)}, f32[3,2]{0,1:T(2,128)}, u32[]{:S(2)}) copy-start(f32[3,2]{0,1:T(2,128)} %get-tuple-element.199) | copy-start | bytes 76
  94.5 30.2 %copy-start.61 = (pred[3,3]{1,0:T(4,128)(4,1)S(1)}, pred[3,3]{1,0:T(4,128)(4,1)}, u32[]{:S(2)}) copy-start(pred[3,3]{1,0:T(4,128)(4,1)} %fusion.140) | copy-start | bytes 31
  131.9 5.3 %copy-start.32 = (f32[1,128,128]{2,1,0:T(8,128)S(1)}, f32[1,128,128]{2,1,0:T(8,128)}, u32[]{:S(2)}) copy-start(f32[1,128,128]{2,1,0:T(8,128)} %get-tuple-element.87) | copy-start | bytes 196612
  (102 other events, 313.5 us)
Sparse Core Ops, SparseCore 0:
  42.0 39.4 all-gather.19
  83.3 38.6 all-gather.17
  124.7 103.3 all-gather.15
where the time goes:
time: 277 us; the launch traced here: 276 us
  blocking collectives  110 us (40%)
  waiting for transfers between devices  49.1 us (18%)
  local copies, waits for them, and re-layouts  44.2 us (16%)
  matrix products  32.9 us (12%)
  other arithmetic  24 us (9%)
  between operations  15.6 us (6%)
    all_to_all x1, blocking collectives, sum_at_owner(): lax.all_to_all(tiles, axis, split_axis=0, concat_axis=0, tiled=True)  36.4 us
    all_gather x4, blocking collectives, all_in_one(): both, at, found = (lax.all_gather(jnp.concatenate(lines), axis), 0, {})  32.7 us
    all_gather x2, waiting for transfers between devices, all_in_one(): both, at, found = (lax.all_gather(jnp.concatenate(lines), axis), 0, {})  26 us
    all_to_all x1, blocking collectives, summed_on_arrival(): tiles = lax.all_to_all(in_blocks(x, dim, size), axis, 0, 0, tiled=True)  24.1 us
    all_gather x1, waiting for transfers between devices, gather_turned(): lax.all_gather(both, axis, axis=0, tiled=True)  23.1 us
    all_to_all x1, blocking collectives, sent_to_all(): lax.all_to_all(jnp.broadcast_to(x[None], (size, *x.shape)), axis, 0, 0, t...  17.3 us
    dot_general x1, matrix products, body(): jnp.dot(hidden, full_down, preferred_element_type=jnp.float32)  10 us
    slice x12, local copies, waits for them, and re-layouts, carried_in(): subtotal = combine(subtotal, jax.tree.map(lambda part: part[k], pieces))  8.83 us
  transfers between devices with their start and end apart: 3, of which 2 were waited for; matrix products, arithmetic and copies ran while one was open for 23% of the time, Pallas kernels for 0%

commit v1 on v0

v1 whole, which is shorter than its diff:
```python
import jax
import jax.numpy as jnp
from jax import lax
from jax.experimental import pallas as pl
from jax.experimental.pallas import tpu as pltpu
from jax.sharding import Mesh
from jax.sharding import PartitionSpec as P

SP = ("sp_0", "sp_1", "sp_2")
SP_TP = ("sp_0", "sp_1", "sp_2", "tp")

BLOCK = 128
NORM_EPSILON = 1e-06
ROPE_BASE = 10000.0
f32, bf16 = jnp.float32, jnp.bfloat16


def angle_tables(length, first):
    positions = (first + jnp.arange(length, dtype=jnp.int32)).astype(f32)
    wide = jnp.power(ROPE_BASE, -(jnp.arange(64, dtype=f32) / 64))
    narrow = jnp.power(ROPE_BASE, -(jnp.arange(32, dtype=f32) / 32))
    angles = positions[:, None] * jnp.concatenate([wide, narrow, narrow])[None]
    return jnp.cos(angles), jnp.sin(angles)


def lanes(shape):
    return lax.broadcasted_iota(jnp.int32, shape, len(shape) - 1)


def rows(shape):
    return lax.broadcasted_iota(jnp.int32, shape, 0)


def turned_wide(u, cosine, sine):
    lane = lanes(u.shape)
    c = jnp.where(lane < 64, cosine, pltpu.roll(cosine, 64, 1))
    s = jnp.where(lane < 64, -sine, pltpu.roll(sine, 64, 1))
    return u * c + pltpu.roll(u, 64, 1) * s


def turned_narrow(u, cosine, sine):
    lane = lanes(u.shape)
    c = jnp.where(lane < 64, pltpu.roll(cosine, 64, 1), cosine)
    s = jnp.where(lane < 64, pltpu.roll(sine, 64, 1), sine)
    low = (lane & 32) == 0
    other = jnp.where(low, pltpu.roll(u, 96, 1), pltpu.roll(u, 32, 1))
    return u * c + other * jnp.where(low, -s, s)


def split(x):
    high = x.astype(bf16)
    return high, (x - high.astype(f32)).astype(bf16)


def nt(a, b):
    return lax.dot_general(a, b, (((1,), (1,)), ((), ())), preferred_element_type=f32)


def tn(a, b):
    return lax.dot_general(a, b, (((0,), (0,)), ((), ())), preferred_element_type=f32)


def nn(a, b):
    return jnp.dot(a, b, preferred_element_type=f32)


def state_kernel(ld, kn, kw, v0, v1, cosine, sine, state, krn, krw):
    length = kn.shape[0]
    c, s = cosine[...], sine[...]
    kr_n = (turned_narrow(kn[...].astype(f32), c, s) * 64**-0.5).astype(bf16)
    krn[...] = kr_n
    t = rows((length, 128)).astype(f32)
    for h in range(4):
        g, i = h // 2, h % 2
        f, b = ld[g * 2 + i], ld[4 + g * 2 + i]
        if g == 0:
            kr = kr_n
        else:
            kr = (turned_wide(kw[:, i * 128 : (i + 1) * 128].astype(f32), c, s) * 128**-0.5).astype(bf16)
            krw[:, i * 128 : (i + 1) * 128] = kr
        v = (v0 if g == 0 else v1)[:, i * 128 : (i + 1) * 128].astype(f32)
        scaled = jnp.concatenate([v * jnp.exp(f * (length - 1.0 - t)), v * jnp.exp(b * t)], 1)
        high, low = split(scaled)
        total = tn(kr, high) + tn(kr, low)
        for d in range(2):
            part = total[:, d * 128 : (d + 1) * 128]
            if g == 0:
                state[:, d, i, :] = part[i * 64 : (i + 1) * 64]
            else:
                state[:, d, 2 + 2 * i, :] = part[:64]
                state[:, d, 3 + 2 * i, :] = part[64:]
    for d in range(2):
        for r in (6, 7):
            state[:, d, r, :] = jnp.zeros((64, 128), f32)


def inside_kernel(ld, qn, qw, krn, krw, v0, v1, cosine, sine, qrn, qrw, inside):
    length = qn.shape[0]
    c, s = cosine[...], sine[...]
    qr_n = turned_narrow(qn[...].astype(f32), c, s).astype(bf16)
    qrn[...] = qr_n
    lag = (rows((length, length)) - lanes((length, length))).astype(f32)
    away = jnp.abs(lag)
    for h in range(4):
        g, i = h // 2, h % 2
        f, b = ld[g * 2 + i], ld[4 + g * 2 + i]
        if g == 0:
            qr = jnp.where((lanes(qr_n.shape) // 64) == i, qr_n, jnp.zeros_like(qr_n))
            kr = krn[...]
        else:
            qr = turned_wide(qw[:, i * 128 : (i + 1) * 128].astype(f32), c, s).astype(bf16)
            qrw[:, i * 128 : (i + 1) * 128] = qr
            kr = krw[:, i * 128 : (i + 1) * 128]
        weight = jnp.where(lag == 0, 2.0, jnp.exp(jnp.where(lag > 0, f, b) * away))
        a = (nt(qr, kr) * weight).astype(bf16)
        v = (v0 if g == 0 else v1)[:, i * 128 : (i + 1) * 128]
        inside[:, h * 128 : (h + 1) * 128] = nn(a, v)


def finish_kernel(ld, qrn, qrw, inside, enter, g0, g1, weight, out):
    length = qrn.shape[0]
    t = rows((length, 128)).astype(f32)
    total = None
    for h in range(4):
        g, i = h // 2, h % 2
        f, b = ld[g * 2 + i], ld[4 + g * 2 + i]
        if g == 0:
            q = qrn[...]
            q = jnp.where((lanes(q.shape) // 64) == i, q, jnp.zeros_like(q))
            e = [jnp.concatenate([enter[:, d, i, :]] * 2, 0) for d in range(2)]
        else:
            q = qrw[:, i * 128 : (i + 1) * 128]
            e = [jnp.concatenate([enter[:, d, 2 + 2 * i, :], enter[:, d, 3 + 2 * i, :]], 0) for d in range(2)]
        high, low = split(jnp.concatenate(e, 1))
        carried = nn(q, high) + nn(q, low)
        ret = (
            inside[:, h * 128 : (h + 1) * 128]
            + carried[:, :128] * jnp.exp(f * (t + 1.0))
            + carried[:, 128:] * jnp.exp(b * (length - t))
        )
        mean = jnp.mean(ret, -1, keepdims=True)
        centred = ret - mean
        variance = jnp.mean(centred * centred, -1, keepdims=True)
        gate = (g0 if g == 0 else g1)[:, i * 128 : (i + 1) * 128].astype(f32)
        y = (gate * jax.nn.sigmoid(gate) * (centred * lax.rsqrt(variance + NORM_EPSILON))).astype(bf16)
        part = nn(y, weight[g, i * 128 : (i + 1) * 128, :])
        total = part if total is None else total + part
    out[...] = total.astype(bf16)


def scan_kernel(ld, x, out):
    r = rows((8, 128))

    def factor(base):
        rate = jnp.full((8, 128), ld[base + 3], f32)
        rate = jnp.where(r < 4, ld[base + 2], rate)
        rate = jnp.where(r == 1, ld[base + 1], rate)
        rate = jnp.where(r == 0, ld[base], rate)
        return jnp.exp(rate * 384.0)

    n = x.shape[0]
    forward, backward = factor(0), factor(4)
    acc = jnp.zeros((8, 128), f32)
    for k in range(n):
        out[k, 0] = acc
        acc = acc * forward + x[k, 0]
    acc = jnp.zeros((8, 128), f32)
    for k in reversed(range(n)):
        out[k, 1] = acc
        acc = acc * backward + x[k, 1]


SM = pl.BlockSpec(memory_space=pltpu.SMEM)
VM = pl.BlockSpec(memory_space=pltpu.VMEM)


def call(kernel, n_in, outs, name):
    return pl.pallas_call(
        kernel,
        in_specs=[SM] + [VM] * n_in,
        out_specs=jax.tree.map(lambda _: VM, outs),
        out_shape=outs,
        name=name,
        compiler_params=pltpu.CompilerParams(vmem_limit_bytes=40 * 2**20),
    )


def shape(*s, dtype=f32):
    return jax.ShapeDtypeStruct(s, dtype)


def rms_scale(rows_in, gain):
    widened = rows_in.astype(f32)
    return (
        widened * lax.rsqrt(jnp.mean(widened * widened, -1, keepdims=True) + NORM_EPSILON) * gain
    ).astype(bf16)


def exchanged(x, axis):
    return lax.all_to_all(x, axis, 0, 0, tiled=True)


def body(
    stream,
    query_narrow,
    key_narrow,
    query_wide,
    key_wide,
    values,
    out_gate,
    out_weight,
    norm_gain,
    mlp_gate,
    mlp_up,
    mlp_down,
    log_decay,
):
    length = query_narrow.shape[0]
    hidden_units = mlp_gate.shape[1]
    shards = lax.all_gather(jnp.concatenate([mlp_gate, mlp_up, mlp_down.T], 1), SP, axis=0, tiled=True)
    full_gate = shards[:, :hidden_units]
    full_up = shards[:, hidden_units : 2 * hidden_units]
    full_down = shards[:, 2 * hidden_units :]
    rates = log_decay.reshape(8)
    cosine, sine = angle_tables(length, lax.axis_index(SP) * length)
    v0, v1 = values[:, 0], values[:, 1]
    g0, g1 = out_gate[:, 0], out_gate[:, 1]
    n_rows, w_rows = shape(length, 128, dtype=bf16), shape(length, 256, dtype=bf16)
    states = shape(64, 2, 8, 128)
    state, krn, krw = call(state_kernel, 6, (states, n_rows, w_rows), "state")(
        rates, key_narrow, key_wide, v0, v1, cosine, sine
    )
    qrn, qrw, inside = call(inside_kernel, 8, (n_rows, w_rows, shape(length, 512)), "inside")(
        rates, query_narrow, query_wide, krn, krw, v0, v1, cosine, sine
    )
    enter = exchanged(call(scan_kernel, 1, states, "scan")(rates, exchanged(state, SP)), SP)
    proj = call(finish_kernel, 7, shape(length, 2048, dtype=bf16), "finish")(
        rates, qrn, qrw, inside, enter, g0, g1, out_weight
    )
    n_tp = lax.axis_size("tp")
    tiles = (n_tp, length // n_tp, proj.shape[1])
    proj_rows = jnp.sum(exchanged(proj.reshape(tiles), "tp").astype(f32), axis=0)
    middle = (stream.astype(f32) + proj_rows).astype(bf16)
    normed = exchanged(jnp.broadcast_to(rms_scale(middle, norm_gain)[None], tiles), "tp").reshape(length, -1)
    gate_act = jnp.dot(normed, full_gate, preferred_element_type=f32)
    up_act = jnp.dot(normed, full_up, preferred_element_type=f32)
    hidden = (jax.nn.silu(gate_act) * up_act).astype(bf16)
    down = nt(hidden, full_down).astype(bf16)
    down_rows = jnp.sum(exchanged(down.reshape(tiles), "tp").astype(f32), axis=0)
    return (middle.astype(f32) + 0.5 * down_rows).astype(bf16)


def solution(mesh):
    finer = Mesh(mesh.devices.reshape(8, 4, 2, mesh.shape["tp"]), ("sp_0", "sp_1", "sp_2", "tp"))
    return jax.shard_map(
        body,
        mesh=finer,
        in_specs=(
            P(SP_TP, None),
            P(SP, "tp"),
            P(SP, "tp"),
            P(SP, "tp"),
            P(SP, "tp"),
            P(SP, None, "tp"),
            P(SP, None, "tp"),
            P(None, "tp", None),
            P(),
            P(SP, "tp"),
            P(SP, "tp"),
            P("tp", SP),
            P(None, None, "tp"),
        ),
        out_specs=P(SP_TP, None),
        check_vma=False,
    )
```

time: 277 us -> 177 us (0.64)
  waiting for transfers between devices: 49.1 us -> 10.6 us
  local copies, waits for them, and re-layouts: 44.2 us -> 12.5 us
  other arithmetic: 24 us -> 4.4 us
  matrix products: 32.9 us -> 16.6 us
  Pallas kernels: 0 us -> 9 us
  blocking collectives: 110 us -> 102 us
  starting transfers between devices: 0.27 us -> 5.85 us
    all_gather x3 -> x1, waiting for transfers between devices: 49.1 us -> 0.01 us  [body(): lax.all_gather(jnp.concatenate([mlp_gate, mlp_up, mlp_down.T], 1), SP, ax...]
    all_gather x4 -> x0, blocking collectives: 32.7 us -> none  [all_in_one(): both, at, found = (lax.all_gather(jnp.concatenate(lines), axis), 0, {})]
    all_to_all x3 -> x4, blocking collectives: 77.7 us -> 102 us  [exchanged(): return lax.all_to_all(x, axis, 0, 0, tiled=True)]
    dot_general x22 -> x2, matrix products: 32.9 us -> 16.6 us  [the longest x1 10 us: nt(): lax.dot_general(a, b, (((1,), (1,)), ((), ())), preferred_element_type=f32)]
    slice x20 -> x2, local copies, waits for them, and re-layouts: 14.9 us -> 4.02 us  [the longest x1 2.17 us: body(): g0, g1 = (out_gate[:, 0], out_gate[:, 1])]
    all_to_all x0 -> x1, waiting for transfers between devices: none -> 10.6 us  [exchanged(): return lax.all_to_all(x, axis, 0, 0, tiled=True)]
    mul x49 -> x0, local copies, waits for them, and re-layouts: 9.28 us -> none  [the longest x28 5.28 us: chain_step(): earlier[0] * later_part[2][:, None, None] + later_part[0]]
    pallas_call x0 -> x4, Pallas kernels: none -> 9 us  [the longest x1 3.86 us: body(): call(finish_kernel, 7, shape(length, 2048, dtype=bf16), 'finish')]
  transfers between devices with their start and end apart: 3 -> 2, of which waited for: 2 -> 1; matrix products, arithmetic and copies ran while one was open for 23% -> 4% of each run, Pallas kernels for 0% -> 5%
where the time goes in v1:
time: 177 us; the launch traced here: 174 us
  blocking collectives  102 us (58%)
  matrix products  16.6 us (9%)
  between operations  13.6 us (8%)
  local copies, waits for them, and re-layouts  12.5 us (7%)
  waiting for transfers between devices  10.6 us (6%)
  Pallas kernels  9 us (5%)
  starting transfers between devices  5.85 us (3%)
  other arithmetic  4.4 us (2%)
    all_to_all x4, blocking collectives, exchanged(): return lax.all_to_all(x, axis, 0, 0, tiled=True)  102 us
    all_to_all x1, waiting for transfers between devices, exchanged(): return lax.all_to_all(x, axis, 0, 0, tiled=True)  10.6 us
    dot_general x1, matrix products, nt(): lax.dot_general(a, b, (((1,), (1,)), ((), ())), preferred_element_type=f32)  10 us
    unnamed x34, local copies, waits for them, and re-layouts  7.38 us
    dot_general x1, matrix products, body(): gate_act = jnp.dot(normed, full_gate, preferred_element_type=f32)  6.6 us
    all_to_all x1, starting transfers between devices, exchanged(): return lax.all_to_all(x, axis, 0, 0, tiled=True)  5.85 us
    pallas_call x1, Pallas kernels, body(): call(finish_kernel, 7, shape(length, 2048, dtype=bf16), 'finish')  3.86 us
  transfers between devices with their start and end apart: 2, of which 1 were waited for; matrix products, arithmetic and copies ran while one was open for 4% of the time, Pallas kernels for 5%

profile of v1, /device:TPU:1, one launch (start us, length us, event | category | flops | bytes accessed | tf_op | source)
XLA Modules:
  0.0 174.3 jit_solution(12518785717174018036)
XLA Ops:
  6.5 1.7 %pad_maximum_fusion = bf16[32,4224]{1,0:T(8,128)(2,1)} fusion(bf16[32,1408]{1,0:T(8,128)(2,1)} %bitcast.18, bf16[32,1408]{1,0:T(8,128)(2,1)} %param.23, bf16[32,1408]{1,0:T(8,128)(2,1)} %param.22), kind=kLoop, calls=%fused_computation.22 | loop fusion | flops 811008 | bytes 540672 | tf_op jit(solution)/shard_map/concatenate | solution.py:220
  8.3 0.8 reshape.28.ld
  9.2 0.8 multiply_sine_fusion
  10.0 1.8 %fusion.24 = (bf16[384,1,256]{2,1,0:T(2,128)(2,1)S(1)}, bf16[384,1,256]{2,1,0:T(2,128)(2,1)S(1)}) fusion(bf16[384,2,256]{2,1,0:T(2,128)(2,1)} %param.18), kind=kLoop, calls=%fused_computation.34 | loop fusion | bytes 786432 | tf_op jit(solution)/shard_map/slice | solution.py:226
  11.9 1.7 state.1
  13.7 0.7 copy-done.6
  14.3 0.6 copy-done.10
  15.0 35.4 %all_to_all.25.x = f32[64,2,8,128]{3,2,1,0:T(8,128)S(1)} all-to-all(f32[64,2,8,128]{3,2,1,0:T(8,128)S(1)} %get-tuple-element.16), channel_id=1, replica_groups=mesh['sp_0'=8,'sp_1'=4,'sp_2'=2,'tp'=4] {'sp_0','sp_1','sp_2'}, dimensions={0} | all-to-all | bytes 1048576 | tf_op jit(solution)/shard_map/all_to_all | solution.py:200
  50.4 1.5 scan.1
  51.8 5.8 %all-to-all-start.1 = ((f32[64,2,8,128]{3,2,1,0:T(8,128)}), f32[64,2,8,128]{3,2,1,0:T(8,128)S(1)}, u32[]{:S(2)}, u32[]{:S(2)}) async-start(f32[64,2,8,128]{3,2,1,0:T(8,128)} %scan.1), calls=%async_computation.1 | async-start | bytes 1048576 | tf_op jit(solution)/shard_map/all_to_all | solution.py:200
  57.7 1.1 copy-done.5
  58.8 0.9 copy-done.7
  59.7 0.9 copy-done.11
  60.6 1.9 %inside.1 = (bf16[384,128]{1,0:T(8,128)(2,1)S(1)}, bf16[384,256]{1,0:T(8,128)(2,1)S(1)}, f32[384,512]{1,0:T(8,128)S(1)}) custom-call(f32[8]{0:T(128)S(1)} %reshape.28.ld, bf16[384,128]{1,0:T(8,128)(2,1)S(1)} %copy-done.9, bf16[384,256]{1,0:T(8,128)(2,1)S(1)} %copy-done.5, bf16[384,128]{1,0:T(8,128)(2,1)S(1)} %copy-done.11, bf16[384,256]{1,0:T(8,128)(2,1)S(1)} %copy-done.7, ...), custom_call_target="tpu_custom_call" | custom-call | tf_op jit(solution)/shard_map/inside/pallas_call | solution.py:233
  62.6 2.2 %fusion.23 = (bf16[384,1,256]{2,1,0:T(2,128)(2,1)S(1)}, bf16[384,1,256]{2,1,0:T(2,128)(2,1)S(1)}) fusion(bf16[384,2,256]{2,1,0:T(2,128)(2,1)} %param.19), kind=kLoop, calls=%fused_computation.33 | loop fusion | bytes 786432 | tf_op jit(solution)/shard_map/slice | solution.py:227
  64.9 10.6 %all-to-all-done.1.enter = f32[64,2,8,128]{3,2,1,0:T(8,128)S(1)} async-done(((f32[64,2,8,128]{3,2,1,0:T(8,128)}), f32[64,2,8,128]{3,2,1,0:T(8,128)S(1)}, u32[]{:S(2)}, u32[]{:S(2)}) %all-to-all-start.1) | async-done | bytes 524320 | tf_op jit(solution)/shard_map/all_to_all | solution.py:200
  75.5 1.1 copy-done.2
  76.6 0.9 copy-done.4
  77.6 0.9 copy-done.14
  78.5 3.9 %finish.1 = bf16[384,2048]{1,0:T(8,128)(2,1)S(1)} custom-call(f32[8]{0:T(128)S(1)} %reshape.28.ld, bf16[384,128]{1,0:T(8,128)(2,1)S(1)} %copy-done.14, bf16[384,256]{1,0:T(8,128)(2,1)S(1)} %copy-done.4, f32[384,512]{1,0:T(8,128)S(1)} %copy-done.2, f32[64,2,8,128]{3,2,1,0:T(8,128)S(1)} %all-to-all-done.1.enter, bf16[384,256]{1,0:T(8,128)(2,1)S(1)} %get-tuple-element.28.g0, ...), custom_call_target="tpu_custom_call" | custom-call | tf_op jit(solution)/shard_map/finish/pallas_call | solution.py:237
  82.4 24.1 %all_to_all.26 = bf16[4,96,2048]{2,1,0:T(8,128)(2,1)S(1)} all-to-all(bf16[4,96,2048]{2,1,0:T(8,128)(2,1)S(1)} %bitcast.14), channel_id=1, replica_groups=mesh['sp_0'=8,'sp_1'=4,'sp_2'=2,'tp'=4] {'tp'}, dimensions={0} | all-to-all | bytes 3145728 | tf_op jit(solution)/shard_map/all_to_all | solution.py:200
  106.5 0.3 convert_reduce_fusion.1
  106.8 0.2 fusion.18
  107.0 0.2 copy-done.16
  107.2 0.2 fusion.20
  107.3 0.2 broadcast_in_dim.2
  107.5 21.5 %all_to_all.27 = bf16[4,96,2048]{2,1,0:T(8,128)(2,1)S(1)} all-to-all(bf16[4,96,2048]{2,1,0:T(8,128)(2,1)S(1)} %broadcast_in_dim.2), channel_id=1, replica_groups=mesh['sp_0'=8,'sp_1'=4,'sp_2'=2,'tp'=4] {'tp'}, dimensions={0} | all-to-all | bytes 3145728 | tf_op jit(solution)/shard_map/all_to_all | solution.py:200
  129.0 6.6 %fusion.4 = f32[384,1408]{1,0:T(8,128)} fusion(bf16[384,2048]{1,0:T(8,128)(2,1)S(1)} %bitcast.15, bf16[2048,4224]{1,0:T(8,128)(2,1)} %all-gather.2.cloned.1.call-done), kind=kOutput, calls=%fused_computation.4 | convolution fusion | flops 2214592512 | bytes 9502720 | tf_op jit(solution)/shard_map/dot_general | solution.py:245
  135.6 10.0 %fusion.12 = bf16[384,2048]{1,0:T(8,128)(2,1)S(1)} fusion(bf16[2048,4224]{1,0:T(8,128)(2,1)} %all-gather.2.cloned.1.call-done, bf16[384,2048]{1,0:T(8,128)(2,1)S(1)} %bitcast.16, f32[384,1408]{1,0:T(8,128)} %fusion.4), kind=kOutput, calls=%fused_computation.10 | convolution fusion | flops 4433215488 | bytes 16842752 | tf_op jit(solution)/shard_map/dot_general | solution.py:56
  145.7 20.6 %all_to_all.28 = bf16[4,96,2048]{2,1,0:T(8,128)(2,1)S(1)} all-to-all(bf16[4,96,2048]{2,1,0:T(8,128)(2,1)S(1)} %bitcast.17), channel_id=1, replica_groups=mesh['sp_0'=8,'sp_1'=4,'sp_2'=2,'tp'=4] {'tp'}, dimensions={0} | all-to-all | bytes 3145728 | tf_op jit(solution)/shard_map/all_to_all | solution.py:200
  166.3 0.3 convert_reduce_fusion
  166.6 0.9 fusion.21
  (35 shorter events, 0.3 us)
Async XLA Ops:
  6.5 5.4 %copy-start.8 = (bf16[384,256]{1,0:T(8,128)(2,1)S(1)}, bf16[384,256]{1,0:T(8,128)(2,1)}, u32[]{:S(2)}) copy-start(bf16[384,256]{1,0:T(8,128)(2,1)} %kw.1) | copy-start | bytes 589828
  6.5 5.4 %copy-start.12 = (bf16[384,128]{1,0:T(8,128)(2,1)S(1)}, bf16[384,128]{1,0:T(8,128)(2,1)}, u32[]{:S(2)}) copy-start(bf16[384,128]{1,0:T(8,128)(2,1)} %kn.1) | copy-start | bytes 294916
  6.5 122.5 %all-gather.2.cloned.1.call-start = ((), (), s32[]{:S(2)}) async-start(), calls=%async_computation.5 | async-start | bytes 17571840 | tf_op jit(solution)/shard_map/all_gather | solution.py:220
  11.9 45.8 %copy-start.9 = (bf16[384,128]{1,0:T(8,128)(2,1)S(1)}, bf16[384,128]{1,0:T(8,128)(2,1)}, u32[]{:S(2)}) copy-start(bf16[384,128]{1,0:T(8,128)(2,1)} %qn.1) | copy-start | bytes 294916
  13.7 0.7 copy-start.6
  14.3 0.6 copy-start.10
  51.8 23.7 %all-to-all-start.1 = ((f32[64,2,8,128]{3,2,1,0:T(8,128)}), f32[64,2,8,128]{3,2,1,0:T(8,128)S(1)}, u32[]{:S(2)}, u32[]{:S(2)}) async-start(f32[64,2,8,128]{3,2,1,0:T(8,128)} %scan.1), calls=%async_computation.1 | async-start | bytes 1048576 | tf_op jit(solution)/shard_map/all_to_all | solution.py:200
  57.7 17.8 %copy-start = (bf16[2,256,2048]{2,1,0:T(8,128)(2,1)S(1)}, bf16[2,256,2048]{2,1,0:T(8,128)(2,1)}, u32[]{:S(2)}) copy-start(bf16[2,256,2048]{2,1,0:T(8,128)(2,1)} %weight.1) | copy-start | bytes 6291460
  57.7 1.1 copy-start.5
  58.8 0.9 copy-start.7
  59.7 0.9 copy-start.11
  62.6 2.2 %copy-start.1 = (f32[384,512]{1,0:T(8,128)}, f32[384,512]{1,0:T(8,128)S(1)}, u32[]{:S(2)}) copy-start(f32[384,512]{1,0:T(8,128)S(1)} %get-tuple-element.15.inside) | copy-start | bytes 2359300
  62.6 2.2 %copy-start.3 = (bf16[384,256]{1,0:T(8,128)(2,1)}, bf16[384,256]{1,0:T(8,128)(2,1)S(1)}, u32[]{:S(2)}) copy-start(bf16[384,256]{1,0:T(8,128)(2,1)S(1)} %get-tuple-element.14.qrw) | copy-start | bytes 589828
  62.6 2.2 %copy-start.13 = (bf16[384,128]{1,0:T(8,128)(2,1)}, bf16[384,128]{1,0:T(8,128)(2,1)S(1)}, u32[]{:S(2)}) copy-start(bf16[384,128]{1,0:T(8,128)(2,1)S(1)} %get-tuple-element.13.qrn) | copy-start | bytes 294916
  75.5 1.1 copy-start.2
  76.6 0.9 copy-start.4
  77.6 0.9 copy-start.14
  82.3 24.4 %copy-start.15 = (bf16[96,2048]{1,0:T(8,128)(2,1)S(1)}, bf16[96,2048]{1,0:T(8,128)(2,1)}, u32[]{:S(2)}) copy-start(bf16[96,2048]{1,0:T(8,128)(2,1)} %param.13) | copy-start | bytes 1179652
  106.5 0.7 copy-start.16
Sparse Core Ops, SparseCore 0:
  10.1 110.0 all-gather.1

commit v2 on v1

v2 whole, which is shorter than its diff:
```python
import jax
import jax.numpy as jnp
from jax import lax
from jax.experimental import pallas as pl
from jax.experimental.pallas import tpu as pltpu
from jax.sharding import Mesh
from jax.sharding import PartitionSpec as P

SP = ("sp_0", "sp_1", "sp_2")
SP_TP = ("sp_0", "sp_1", "sp_2", "tp")

BLOCK = 128
NORM_EPSILON = 1e-06
ROPE_BASE = 10000.0
f32, bf16 = jnp.float32, jnp.bfloat16


def angle_tables(length, first):
    positions = (first + jnp.arange(length, dtype=jnp.int32)).astype(f32)
    wide = jnp.power(ROPE_BASE, -(jnp.arange(64, dtype=f32) / 64))
    narrow = jnp.power(ROPE_BASE, -(jnp.arange(32, dtype=f32) / 32))
    angles = positions[:, None] * jnp.concatenate([wide, narrow, narrow])[None]
    return jnp.cos(angles), jnp.sin(angles)


def lanes(shape):
    return lax.broadcasted_iota(jnp.int32, shape, len(shape) - 1)


def rows(shape):
    return lax.broadcasted_iota(jnp.int32, shape, 0)


def turned_wide(u, cosine, sine):
    lane = lanes(u.shape)
    c = jnp.where(lane < 64, cosine, pltpu.roll(cosine, 64, 1))
    s = jnp.where(lane < 64, -sine, pltpu.roll(sine, 64, 1))
    return u * c + pltpu.roll(u, 64, 1) * s


def turned_narrow(u, cosine, sine):
    lane = lanes(u.shape)
    c = jnp.where(lane < 64, pltpu.roll(cosine, 64, 1), cosine)
    s = jnp.where(lane < 64, pltpu.roll(sine, 64, 1), sine)
    low = (lane & 32) == 0
    other = jnp.where(low, pltpu.roll(u, 96, 1), pltpu.roll(u, 32, 1))
    return u * c + other * jnp.where(low, -s, s)


def split(x):
    high = x.astype(bf16)
    return high, (x - high.astype(f32)).astype(bf16)


def nt(a, b):
    return lax.dot_general(a, b, (((1,), (1,)), ((), ())), preferred_element_type=f32)


def tn(a, b):
    return lax.dot_general(a, b, (((0,), (0,)), ((), ())), preferred_element_type=f32)


def nn(a, b):
    return jnp.dot(a, b, preferred_element_type=f32)


STATE = bf16


def turned_all(narrow, wide, cosine, sine, scales):
    c, s = cosine[...], sine[...]
    parts = [turned_narrow(narrow[...].astype(f32), c, s) * scales[0]]
    for i in range(2):
        parts.append(turned_wide(wide[:, i * 128 : (i + 1) * 128].astype(f32), c, s) * scales[1])
    return [p.astype(bf16) for p in parts]


def of_head(parts, h):
    if h >= 2:
        return parts[h - 1]
    return jnp.where((lanes(parts[0].shape) // 64) == h, parts[0], jnp.zeros_like(parts[0]))


KEY_SCALES = (64**-0.5, 128**-0.5)


def state_kernel(ld, kn, kw, v0, v1, cosine, sine, out, state):
    length = kn.shape[0]
    keys = turned_all(kn, kw, cosine, sine, KEY_SCALES)
    t = rows((length, 128)).astype(f32)
    for h in range(4):
        g, i = h // 2, h % 2
        f, b = ld[g * 2 + i], ld[4 + g * 2 + i]
        v = (v0 if g == 0 else v1)[:, i * 128 : (i + 1) * 128].astype(f32)
        scaled = jnp.concatenate([v * jnp.exp(f * (length - 1.0 - t)), v * jnp.exp(b * t)], 1)
        high, low = split(scaled)
        kr = keys[0] if g == 0 else keys[1 + i]
        total = tn(kr, high) + tn(kr, low)
        for d in range(2):
            part = total[:, d * 128 : (d + 1) * 128]
            if g == 0:
                state[:, d, i, :] = part[i * 64 : (i + 1) * 64]
            else:
                state[:, d, 2 + 2 * i, :] = part[:64]
                state[:, d, 3 + 2 * i, :] = part[64:]
    for d in range(2):
        for r in (6, 7):
            state[:, d, r, :] = jnp.zeros((64, 128), f32)
    out[...] = state[...].astype(STATE)


def inside_kernel(ld, qn, qw, kn, kw, v0, v1, cosine, sine, turned, inside):
    length = qn.shape[0]
    queries = turned_all(qn, qw, cosine, sine, (1.0, 1.0))
    keys = turned_all(kn, kw, cosine, sine, KEY_SCALES)
    for k in range(3):
        turned[:, k * 128 : (k + 1) * 128] = queries[k]
    lag = (rows((length, length)) - lanes((length, length))).astype(f32)
    away = jnp.abs(lag)
    for h in range(4):
        g, i = h // 2, h % 2
        f, b = ld[g * 2 + i], ld[4 + g * 2 + i]
        kr = keys[0] if g == 0 else keys[1 + i]
        weight = jnp.where(lag == 0, 2.0, jnp.exp(jnp.where(lag > 0, f, b) * away))
        a = (nt(of_head(queries, h), kr) * weight).astype(bf16)
        v = (v0 if g == 0 else v1)[:, i * 128 : (i + 1) * 128]
        inside[:, h * 128 : (h + 1) * 128] = nn(a, v)


def finish_kernel(ld, turned_in, inside_in, enter_in, g0, g1, out, turned, inside, enter, sems):
    copies = [
        pltpu.make_async_copy(turned_in, turned, sems.at[0]),
        pltpu.make_async_copy(inside_in, inside, sems.at[1]),
    ]
    for copy in copies:
        copy.start()
    enter[...] = enter_in[...].astype(f32)
    length = turned.shape[0]
    t = rows((length, 128)).astype(f32)
    states = []
    for h in range(4):
        g, i = h // 2, h % 2
        if g == 0:
            e = [jnp.concatenate([enter[:, d, i, :]] * 2, 0) for d in range(2)]
        else:
            e = [jnp.concatenate([enter[:, d, 2 + 2 * i, :], enter[:, d, 3 + 2 * i, :]], 0) for d in range(2)]
        states.append(split(jnp.concatenate(e, 1)))
    for copy in copies:
        copy.wait()
    queries = [turned[:, k * 128 : (k + 1) * 128] for k in range(3)]
    for h in range(4):
        g, i = h // 2, h % 2
        f, b = ld[g * 2 + i], ld[4 + g * 2 + i]
        q = of_head(queries, h)
        high, low = states[h]
        carried = nn(q, high) + nn(q, low)
        ret = (
            inside[:, h * 128 : (h + 1) * 128]
            + carried[:, :128] * jnp.exp(f * (t + 1.0))
            + carried[:, 128:] * jnp.exp(b * (length - t))
        )
        mean = jnp.mean(ret, -1, keepdims=True)
        centred = ret - mean
        variance = jnp.mean(centred * centred, -1, keepdims=True)
        gate = (g0 if g == 0 else g1)[:, i * 128 : (i + 1) * 128].astype(f32)
        y = gate * jax.nn.sigmoid(gate) * (centred * lax.rsqrt(variance + NORM_EPSILON))
        out[:, h * 128 : (h + 1) * 128] = y.astype(bf16)


def scan_kernel(ld, x, out):
    r = rows((8, 128))

    def factor(base):
        rate = jnp.full((8, 128), ld[base + 3], f32)
        rate = jnp.where(r < 4, ld[base + 2], rate)
        rate = jnp.where(r == 1, ld[base + 1], rate)
        rate = jnp.where(r == 0, ld[base], rate)
        return jnp.exp(rate * 384.0)

    n = x.shape[0]
    forward, backward = factor(0), factor(4)
    acc = jnp.zeros((8, 128), f32)
    for k in range(n):
        out[k, 0] = acc.astype(STATE)
        acc = acc * forward + x[k, 0].astype(f32)
    acc = jnp.zeros((8, 128), f32)
    for k in reversed(range(n)):
        out[k, 1] = acc.astype(STATE)
        acc = acc * backward + x[k, 1].astype(f32)


def proj_kernel(place, y, stream, gain, own, *refs):
    others, (middle, normed, blocks, sems) = refs[:6], refs[6:]
    sources = [own.at[0], own.at[1], *others]
    copies = [pltpu.make_async_copy(s, blocks.at[k], sems.at[k]) for k, s in enumerate(sources)]
    for copy in copies:
        copy.start()
    tp, core = place[0], place[1]
    total = stream[...].astype(f32)
    for k, copy in enumerate(copies):
        if k < 2:
            rows_in = y[tp, :, k * 256 : (k + 1) * 256]
        else:
            piece = y[(tp + 4 - (k // 2)) % 4]
            first, second = (core, 1 - core) if k % 2 == 0 else (1 - core, core)
            rows_in = jnp.where(first == 0, piece[:, :256], piece[:, 256:])
        copy.wait()
        part = nn(rows_in, blocks[k])
        proj = part if k == 0 else proj + part
    mid = (total + proj).astype(bf16)
    middle[...] = mid
    wide = mid.astype(f32)
    scale = lax.rsqrt(jnp.mean(wide * wide, -1, keepdims=True) + NORM_EPSILON)
    normed[...] = (wide * scale * gain[...]).astype(bf16)


SM = pl.BlockSpec(memory_space=pltpu.SMEM)
VM = pl.BlockSpec(memory_space=pltpu.VMEM)
HB = pl.BlockSpec(memory_space=pltpu.HBM)


def call(kernel, in_specs, outs, name, scratch=()):
    return pl.pallas_call(
        kernel,
        in_specs=in_specs,
        out_specs=jax.tree.map(lambda _: VM, outs),
        out_shape=outs,
        scratch_shapes=scratch,
        name=name,
        compiler_params=pltpu.CompilerParams(vmem_limit_bytes=40 * 2**20),
    )


def shape(*s, dtype=f32):
    return jax.ShapeDtypeStruct(s, dtype)


def exchanged(x, axis):
    return lax.all_to_all(x, axis, 0, 0, tiled=True)


def after(x, token):
    return lax.optimization_barrier((x, token))[0]


def shifted(x, by):
    n = lax.axis_size("tp")
    return lax.ppermute(x, "tp", [(k, (k + by) % n) for k in range(n)])


def body(
    stream,
    query_narrow,
    key_narrow,
    query_wide,
    key_wide,
    values,
    out_gate,
    out_weight,
    norm_gain,
    mlp_gate,
    mlp_up,
    mlp_down,
    log_decay,
):
    length, width = query_narrow.shape[0], stream.shape[1]
    hidden_units = mlp_gate.shape[1]
    shards = lax.all_gather(jnp.concatenate([mlp_gate, mlp_up], 1), SP, axis=0, tiled=True)
    full_gate, full_up = shards[:, :hidden_units], shards[:, hidden_units:]
    full_down = lax.all_gather(mlp_down.T, SP, axis=0, tiled=True)

    rates = log_decay.reshape(8)
    cosine, sine = angle_tables(length, lax.axis_index(SP) * length)
    v0, v1 = values[:, 0], values[:, 1]
    g0, g1 = out_gate[:, 0], out_gate[:, 1]
    states = shape(64, 2, 8, 128, dtype=STATE)
    state = call(state_kernel, [SM] + [VM] * 6, states, "state", (pltpu.VMEM((64, 2, 8, 128), f32),))(
        rates, key_narrow, key_wide, v0, v1, cosine, sine
    )
    core = lax.axis_index("sp_2")
    half = lax.dynamic_index_in_dim(after(out_weight, state), core, 0, keepdims=False)
    same = [shifted(half, s) for s in (1, 2, 3)]
    turned, inside = call(
        inside_kernel, [SM] + [VM] * 8, (shape(length, 384, dtype=bf16), shape(length, 512)), "inside"
    )(rates, query_narrow, query_wide, key_narrow, key_wide, v0, v1, cosine, sine)
    arrived = exchanged(state, SP)
    enter = call(scan_kernel, [SM, VM], states, "scan")(rates, arrived)
    enter = exchanged(enter, SP)
    y = call(
        finish_kernel,
        [SM, HB, HB, VM, VM, VM],
        shape(length, 512, dtype=bf16),
        "finish",
        (pltpu.VMEM((length, 384), bf16), pltpu.VMEM((length, 512), f32), pltpu.VMEM((64, 2, 8, 128), f32), pltpu.SemaphoreType.DMA((2,))),
    )(rates, turned, inside, enter, g0, g1)
    other = [lax.ppermute(after(w, y), "sp_2", [(0, 1), (1, 0)]) for w in same]
    n_tp = lax.axis_size("tp")
    y = exchanged(y.reshape(n_tp, length // n_tp, 512), "tp")
    own = shape(length // n_tp, width, dtype=bf16)
    place = jnp.stack([lax.axis_index("tp"), core]).astype(jnp.int32)
    pieces = [w for pair in zip(same, other) for w in pair]
    middle, normed = call(
        proj_kernel,
        [SM, VM, VM, VM] + [HB] * 7,
        (own, own),
        "proj",
        (pltpu.VMEM((8, 256, width), bf16), pltpu.SemaphoreType.DMA((8,))),
    )(place, y, stream, norm_gain[None], out_weight, *pieces)

    def mixed(x):
        gate_act = jnp.dot(x, full_gate, preferred_element_type=f32)
        up_act = jnp.dot(x, full_up, preferred_element_type=f32)
        return (jax.nn.silu(gate_act) * up_act).astype(bf16)

    near = mixed(jnp.concatenate([shifted(normed, 1), shifted(normed, 3)], 0))
    far = mixed(jnp.concatenate([normed, shifted(normed, 2)], 0))
    near, far, full_down = lax.optimization_barrier((near, far, full_down))
    near = nt(near, full_down).astype(bf16)
    far = nt(far, full_down).astype(bf16)
    n = length // n_tp
    total = far[:n].astype(f32) + shifted(far[n:], 2).astype(f32)
    total = total + shifted(near[:n], 3).astype(f32) + shifted(near[n:], 1).astype(f32)
    return (middle.astype(f32) + 0.5 * total).astype(bf16)


def solution(mesh):
    finer = Mesh(mesh.devices.reshape(8, 4, 2, mesh.shape["tp"]), ("sp_0", "sp_1", "sp_2", "tp"))
    return jax.shard_map(
        body,
        mesh=finer,
        in_specs=(
            P(SP_TP, None),
            P(SP, "tp"),
            P(SP, "tp"),
            P(SP, "tp"),
            P(SP, "tp"),
            P(SP, None, "tp"),
            P(SP, None, "tp"),
            P(None, "tp", None),
            P(),
            P(SP, "tp"),
            P(SP, "tp"),
            P("tp", SP),
            P(None, None, "tp"),
        ),
        out_specs=P(SP_TP, None),
        check_vma=False,
    )
```

time: 177 us -> 217 us (1.23); the launches traced: 174 us -> 217 us
  waiting for transfers between devices: 10.6 us -> 109 us
  blocking collectives: 102 us -> 27.4 us
  starting transfers between devices: 5.85 us -> 21.3 us
  Pallas kernels: 9 us -> 11.8 us
  matrix products: 16.6 us -> 18.9 us
    all_to_all x4 -> x1, blocking collectives: 102 us -> 27.4 us  [exchanged(): return lax.all_to_all(x, axis, 0, 0, tiled=True)]
    all_gather x1 -> x2, waiting for transfers between devices: 0.01 us -> 60.9 us  [the longest x1 60.9 us: body(): full_down = lax.all_gather(mlp_down.T, SP, axis=0, tiled=True)]
    ppermute x0 -> x12, waiting for transfers between devices: none -> 31.6 us  [the longest x9 31.6 us: shifted(): return lax.ppermute(x, 'tp', [(k, (k + by) % n) for k in range(n)])]
    ppermute x0 -> x12, starting transfers between devices: none -> 12.7 us  [the longest x9 11.8 us: shifted(): return lax.ppermute(x, 'tp', [(k, (k + by) % n) for k in range(n)])]
    dot_general x1 -> x4, matrix products: 6.6 us -> 12 us  [the longest x2 9.05 us: mixed(): gate_act = jnp.dot(x, full_gate, preferred_element_type=f32)]
    all_to_all x1 -> x2, waiting for transfers between devices: 10.6 us -> 15.5 us  [exchanged(): return lax.all_to_all(x, axis, 0, 0, tiled=True)]
    dot_general x1 -> x2, matrix products: 10 us -> 6.89 us  [nt(): lax.dot_general(a, b, (((1,), (1,)), ((), ())), preferred_element_type=f32)]
    pallas_call x4 -> x5, Pallas kernels: 9 us -> 11.8 us  [the longest x1 4.03 us: body(): call(proj_kernel, [SM, VM, VM, VM] + [HB] * 7, (own, own), 'proj', (pltpu...]
  transfers between devices with their start and end apart: 2 -> 16, of which waited for: 1 -> 9; matrix products, arithmetic and copies ran while one was open for 4% -> 10% of each run, Pallas kernels for 5% -> 5%
where the time goes in v2:
time: 217 us
  waiting for transfers between devices  109 us (50%)
  blocking collectives  27.4 us (13%)
  starting transfers between devices  21.3 us (10%)
  matrix products  18.9 us (9%)
  between operations  13.7 us (6%)
  Pallas kernels  11.8 us (5%)
  local copies, waits for them, and re-layouts  11 us (5%)
  other arithmetic  3.68 us (2%)
    all_gather x1, waiting for transfers between devices, body(): full_down = lax.all_gather(mlp_down.T, SP, axis=0, tiled=True)  60.9 us
    ppermute x9, waiting for transfers between devices, shifted(): return lax.ppermute(x, 'tp', [(k, (k + by) % n) for k in range(n)])  31.6 us
    all_to_all x1, blocking collectives, exchanged(): return lax.all_to_all(x, axis, 0, 0, tiled=True)  27.4 us
    all_to_all x2, waiting for transfers between devices, exchanged(): return lax.all_to_all(x, axis, 0, 0, tiled=True)  15.5 us
    ppermute x9, starting transfers between devices, shifted(): return lax.ppermute(x, 'tp', [(k, (k + by) % n) for k in range(n)])  11.8 us
    dot_general x2, matrix products, mixed(): gate_act = jnp.dot(x, full_gate, preferred_element_type=f32)  9.05 us
    all_to_all x2, starting transfers between devices, exchanged(): return lax.all_to_all(x, axis, 0, 0, tiled=True)  8.6 us
    dot_general x2, matrix products, nt(): lax.dot_general(a, b, (((1,), (1,)), ((), ())), preferred_element_type=f32)  6.89 us
  transfers between devices with their start and end apart: 16, of which 9 were waited for; matrix products, arithmetic and copies ran while one was open for 10% of the time, Pallas kernels for 5%

profile of v2, /device:TPU:1, one launch (start us, length us, event | category | flops | bytes accessed | tf_op | source)
XLA Modules:
  0.0 216.6 jit_solution(10286175963459234845)
XLA Ops:
  6.5 1.7 pad_maximum_fusion
  10.6 1.9 fusion.10
  12.7 1.8 state.1
  14.5 1.0 dynamic-slice_bitcast_fusion
  15.5 3.6 %collective-permute-start.4 = (bf16[256,2048]{1,0:T(8,128)(2,1)}, bf16[256,2048]{1,0:T(8,128)(2,1)}, u32[]{:S(2)}, u32[]{:S(2)}) collective-permute-start(bf16[256,2048]{1,0:T(8,128)(2,1)} %dynamic-slice_bitcast_fusion), channel_id=1, source_target_pairs={{0,3},{1,0},{2,1},{3,2},{4,7},{5,4},{6,5},{7,6},{8,11},{9,8},{10,9... | collective-permute-start | bytes 3145736 | tf_op jit(solution)/shard_map/ppermute | solution.py:248
  20.1 27.4 %all_to_all.15.x = bf16[64,2,8,128]{3,2,1,0:T(8,128)(2,1)S(1)} all-to-all(bf16[64,2,8,128]{3,2,1,0:T(8,128)(2,1)S(1)} %state.1), channel_id=1, replica_groups=mesh['sp_0'=8,'sp_1'=4,'sp_2'=2,'tp'=4] {'sp_0','sp_1','sp_2'}, dimensions={0} | all-to-all | bytes 524288 | tf_op jit(solution)/shard_map/all_to_all | solution.py:239
  47.5 1.4 scan.1
  48.9 5.1 %all-to-all-start.1 = ((bf16[64,2,8,128]{3,2,1,0:T(8,128)(2,1)}), bf16[64,2,8,128]{3,2,1,0:T(8,128)(2,1)S(1)}, u32[]{:S(2)}, u32[]{:S(2)}) async-start(bf16[64,2,8,128]{3,2,1,0:T(8,128)(2,1)} %scan.1), calls=%async_computation.1 | async-start | bytes 524288 | tf_op jit(solution)/shard_map/all_to_all | solution.py:239
  55.0 2.1 inside.1
  57.1 2.2 %fusion.9 = (bf16[384,1,256]{2,1,0:T(2,128)(2,1)S(1)}, bf16[384,1,256]{2,1,0:T(2,128)(2,1)S(1)}) fusion(bf16[384,2,256]{2,1,0:T(2,128)(2,1)} %param.19), kind=kLoop, calls=%fused_computation.31 | loop fusion | bytes 786432 | tf_op jit(solution)/shard_map/slice | solution.py:275
  59.4 7.8 %all-to-all-done.1.enter_in = bf16[64,2,8,128]{3,2,1,0:T(8,128)(2,1)S(1)} async-done(((bf16[64,2,8,128]{3,2,1,0:T(8,128)(2,1)}), bf16[64,2,8,128]{3,2,1,0:T(8,128)(2,1)S(1)}, u32[]{:S(2)}, u32[]{:S(2)}) %all-to-all-start.1) | async-done | bytes 262176 | tf_op jit(solution)/shard_map/all_to_all | solution.py:239
  67.2 1.1 copy-done.3
  69.3 2.6 %finish.1 = bf16[384,512]{1,0:T(8,128)(2,1)} custom-call(f32[8]{0:T(128)S(1)} %reshape.12.ld, bf16[384,384]{1,0:T(8,128)(2,1)S(1)} %copy-done.9, f32[384,512]{1,0:T(8,128)S(1)} %copy-done.3, bf16[64,2,8,128]{3,2,1,0:T(8,128)(2,1)S(1)} %all-to-all-done.1.enter_in, bf16[384,256]{1,0:T(8,128)(2,1)S(1)} %get-tuple-element.38.g0, ...), custom_call_target="tpu_custom_call" | custom-call | tf_op jit(solution)/shard_map/finish/pallas_call | solution.py:289
  72.7 3.5 %all-to-all-start.2 = ((bf16[4,96,512]{2,1,0:T(8,128)(2,1)}), bf16[4,96,512]{2,1,0:T(8,128)(2,1)S(1)}, u32[]{:S(2)}, u32[]{:S(2)}) async-start(bf16[4,96,512]{2,1,0:T(8,128)(2,1)} %bitcast.6), calls=%async_computation.2 | async-start | bytes 786432 | tf_op jit(solution)/shard_map/all_to_all | solution.py:239
  76.3 7.7 %all-to-all-done.2.y = bf16[4,96,512]{2,1,0:T(8,128)(2,1)S(1)} async-done(((bf16[4,96,512]{2,1,0:T(8,128)(2,1)}), bf16[4,96,512]{2,1,0:T(8,128)(2,1)S(1)}, u32[]{:S(2)}, u32[]{:S(2)}) %all-to-all-start.2) | async-done | bytes 393248 | tf_op jit(solution)/shard_map/all_to_all | solution.py:239
  84.0 1.0 copy-done.7
  85.0 4.0 %proj.1 = (bf16[96,2048]{1,0:T(8,128)(2,1)S(1)}, bf16[96,2048]{1,0:T(8,128)(2,1)S(1)}) custom-call(s32[2]{0:T(128)S(1)} %pad_add_fusion.place, bf16[4,96,512]{2,1,0:T(8,128)(2,1)S(1)} %all-to-all-done.2.y, bf16[96,2048]{1,0:T(8,128)(2,1)S(1)} %copy-done.7, f32[1,2048]{1,0:T(1,128)S(1)} %bitcast.23, bf16[2,256,2048]{2,1,0:T(8,128)(2,1)S(1)} %copy-done, ...), custom_call_target="tpu_custom_call" | custom-call | tf_op jit(solution)/shard_map/proj/pallas_call | solution.py:302
  90.2 1.7 collective-permute-start.8
  92.7 8.4 %collective-permute-done.6 = bf16[96,2048]{1,0:T(8,128)(2,1)S(1)} collective-permute-done((bf16[96,2048]{1,0:T(8,128)(2,1)S(1)}, bf16[96,2048]{1,0:T(8,128)(2,1)S(1)}, u32[]{:S(2)}, u32[]{:S(2)}) %collective-permute-start.6) | collective-permute-done | bytes 393248 | tf_op jit(solution)/shard_map/ppermute | solution.py:248
  101.1 7.3 %collective-permute-done.8 = bf16[96,2048]{1,0:T(8,128)(2,1)S(1)} collective-permute-done((bf16[96,2048]{1,0:T(8,128)(2,1)S(1)}, bf16[96,2048]{1,0:T(8,128)(2,1)S(1)}, u32[]{:S(2)}, u32[]{:S(2)}) %collective-permute-start.8) | collective-permute-done | bytes 393248 | tf_op jit(solution)/shard_map/ppermute | solution.py:248
  108.4 1.4 collective-permute-done.7
  109.8 4.2 %fusion.4 = f32[192,1408]{1,0:T(8,128)S(1)} fusion(bf16[192,2048]{1,0:T(8,128)(2,1)S(1)} %constant_dynamic-update-slice_fusion.2, bf16[2048,2816]{1,0:T(8,128)(2,1)} %all-gather.3.cloned.1.call-done), kind=kOutput, calls=%fused_computation.4 | convolution fusion | flops 1107296256 | bytes 7634944 | tf_op jit(solution)/shard_map/dot_general | solution.py:311
  114.0 4.9 %fusion.6 = f32[192,1408]{1,0:T(8,128)S(1)} fusion(bf16[192,2048]{1,0:T(8,128)(2,1)S(1)} %constant_dynamic-update-slice_fusion, bf16[2048,2816]{1,0:T(8,128)(2,1)} %all-gather.3.cloned.1.call-done), kind=kOutput, calls=%fused_computation.6 | convolution fusion | flops 1107296256 | bytes 7634944 | tf_op jit(solution)/shard_map/dot_general | solution.py:311
  118.9 1.5 multiply_convert_fusion
  120.4 1.5 multiply_convert_fusion.1
  121.9 60.9 %all-gather.5.cloned.1.call-done = bf16[2048,1408]{1,0:T(8,128)(2,1)} async-done(((bf16[32,1408]{1,0:T(8,128)(2,1)}), bf16[2048,1408]{1,0:T(8,128)(2,1)}) %all-gather.5.cloned.1.call-update) | async-done | bytes 5767184 | tf_op jit(solution)/shard_map/all_gather | solution.py:270
  182.8 4.8 %convolution_convert_fusion.1 = bf16[192,2048]{1,0:T(8,128)(2,1)S(1)} fusion(bf16[192,1408]{1,0:T(8,128)(2,1)S(1)} %multiply_convert_fusion, bf16[2048,1408]{1,0:T(8,128)(2,1)} %all-gather.5.cloned.1.call-done), kind=kOutput, calls=%fused_computation.9 | convolution fusion | flops 1107689472 | bytes 7094272 | tf_op jit(solution)/shard_map/dot_general | solution.py:56
  187.7 2.8 %collective-permute-start.9 = (bf16[96,2048]{1,0:T(8,128)(2,1)S(1)}, bf16[96,2048]{1,0:T(8,128)(2,1)S(1)}, u32[]{:S(2)}, u32[]{:S(2)}) collective-permute-start(bf16[96,2048]{1,0:T(8,128)(2,1)S(1)} %slice.43), channel_id=1, source_target_pairs={{0,2},{1,3},{2,0},{3,1},{4,6},{5,7},{6,4},{7,5},{8,10},{9,11},{10,... | collective-permute-start | bytes 1179656 | tf_op jit(solution)/shard_map/ppermute | solution.py:248
  190.5 2.1 convolution_convert_fusion
  194.2 5.5 %collective-permute-done.9 = bf16[96,2048]{1,0:T(8,128)(2,1)S(1)} collective-permute-done((bf16[96,2048]{1,0:T(8,128)(2,1)S(1)}, bf16[96,2048]{1,0:T(8,128)(2,1)S(1)}, u32[]{:S(2)}, u32[]{:S(2)}) %collective-permute-start.9) | collective-permute-done | bytes 393248 | tf_op jit(solution)/shard_map/ppermute | solution.py:248
  199.7 8.5 %collective-permute-done.10 = bf16[96,2048]{1,0:T(8,128)(2,1)S(1)} collective-permute-done((bf16[96,2048]{1,0:T(8,128)(2,1)S(1)}, bf16[96,2048]{1,0:T(8,128)(2,1)S(1)}, u32[]{:S(2)}, u32[]{:S(2)}) %collective-permute-start.10) | collective-permute-done | bytes 393248 | tf_op jit(solution)/shard_map/ppermute | solution.py:248
  208.7 1.1 add_convert_fusion
  (64 shorter events, 10.6 us)
Async XLA Ops:
  6.5 6.1 %copy-start.6 = (bf16[384,128]{1,0:T(8,128)(2,1)S(1)}, bf16[384,128]{1,0:T(8,128)(2,1)}, u32[]{:S(2)}) copy-start(bf16[384,128]{1,0:T(8,128)(2,1)} %kn.3) | copy-start | bytes 294916
  6.5 6.1 %copy-start.1 = (bf16[384,256]{1,0:T(8,128)(2,1)S(1)}, bf16[384,256]{1,0:T(8,128)(2,1)}, u32[]{:S(2)}) copy-start(bf16[384,256]{1,0:T(8,128)(2,1)} %kw.3) | copy-start | bytes 589828
  6.5 103.3 %all-gather.3.cloned.1.call-start = ((), (), s32[]{:S(2)}) async-start(), calls=%async_computation.3 | async-start | bytes 11714560 | tf_op jit(solution)/shard_map/all_gather | solution.py:268
  8.2 174.6 %all-gather.5.cloned.1.call-start = ((), (), s32[]{:S(2)}) async-start(), calls=%async_computation.4 | async-start | bytes 5857280 | tf_op jit(solution)/shard_map/all_gather | solution.py:270
  10.6 3.8 %copy-start = (bf16[2,256,2048]{2,1,0:T(8,128)(2,1)S(1)}, bf16[2,256,2048]{2,1,0:T(8,128)(2,1)}, u32[]{:S(2)}) copy-start(bf16[2,256,2048]{2,1,0:T(8,128)(2,1)} %own.1) | copy-start | bytes 6291460
  14.4 39.6 %copy-start.11 = (bf16[384,128]{1,0:T(8,128)(2,1)S(1)}, bf16[384,128]{1,0:T(8,128)(2,1)}, u32[]{:S(2)}) copy-start(bf16[384,128]{1,0:T(8,128)(2,1)} %qn.1) | copy-start | bytes 294916
  15.5 56.3 %collective-permute-start.4 = (bf16[256,2048]{1,0:T(8,128)(2,1)}, bf16[256,2048]{1,0:T(8,128)(2,1)}, u32[]{:S(2)}, u32[]{:S(2)}) collective-permute-start(bf16[256,2048]{1,0:T(8,128)(2,1)} %dynamic-slice_bitcast_fusion), channel_id=1, source_target_pairs={{0,3},{1,0},{2,1},{3,2},{4,7},{5,4},{6,5},{7,6},{8,11},{9,8},{10,9... | collective-permute-start | bytes 3145736 | tf_op jit(solution)/shard_map/ppermute | solution.py:248
  19.1 53.1 %collective-permute-start.2 = (bf16[256,2048]{1,0:T(8,128)(2,1)}, bf16[256,2048]{1,0:T(8,128)(2,1)}, u32[]{:S(2)}, u32[]{:S(2)}) collective-permute-start(bf16[256,2048]{1,0:T(8,128)(2,1)} %dynamic-slice_bitcast_fusion), channel_id=1, source_target_pairs={{0,2},{1,3},{2,0},{3,1},{4,6},{5,7},{6,4},{7,5},{8,10},{9,11},{10,... | collective-permute-start | bytes 3145736 | tf_op jit(solution)/shard_map/ppermute | solution.py:248
  19.4 53.0 %collective-permute-start = (bf16[256,2048]{1,0:T(8,128)(2,1)}, bf16[256,2048]{1,0:T(8,128)(2,1)}, u32[]{:S(2)}, u32[]{:S(2)}) collective-permute-start(bf16[256,2048]{1,0:T(8,128)(2,1)} %dynamic-slice_bitcast_fusion), channel_id=1, source_target_pairs={{0,1},{1,2},{2,3},{3,0},{4,5},{5,6},{6,7},{7,4},{8,9},{9,10},{10,1... | collective-permute-start | bytes 3145736 | tf_op jit(solution)/shard_map/ppermute | solution.py:248
  48.9 18.2 %all-to-all-start.1 = ((bf16[64,2,8,128]{3,2,1,0:T(8,128)(2,1)}), bf16[64,2,8,128]{3,2,1,0:T(8,128)(2,1)S(1)}, u32[]{:S(2)}, u32[]{:S(2)}) async-start(bf16[64,2,8,128]{3,2,1,0:T(8,128)(2,1)} %scan.1), calls=%async_computation.1 | async-start | bytes 524288 | tf_op jit(solution)/shard_map/all_to_all | solution.py:239
  54.1 0.9 copy-start.10
  57.1 2.2 %copy-start.2 = (f32[384,512]{1,0:T(8,128)}, f32[384,512]{1,0:T(8,128)S(1)}, u32[]{:S(2)}) copy-start(f32[384,512]{1,0:T(8,128)S(1)} %get-tuple-element.17.inside_in) | copy-start | bytes 2359300
  57.1 2.2 %copy-start.8 = (bf16[384,384]{1,0:T(8,128)(2,1)}, bf16[384,384]{1,0:T(8,128)(2,1)S(1)}, u32[]{:S(2)}) copy-start(bf16[384,384]{1,0:T(8,128)(2,1)S(1)} %get-tuple-element.16.turned_in) | copy-start | bytes 884740
  59.3 24.7 %copy-start.12 = (f32[2048]{0:T(1024)S(1)}, f32[2048]{0:T(1024)}, u32[]{:S(2)}) copy-start(f32[2048]{0:T(1024)} %param.21) | copy-start | bytes 24580
  67.2 1.1 copy-start.3
  68.3 1.0 copy-start.9
  71.8 12.1 %collective-permute-start.5 = (bf16[256,2048]{1,0:T(8,128)(2,1)}, bf16[256,2048]{1,0:T(8,128)(2,1)S(1)}, u32[]{:S(2)}, u32[]{:S(2)}) collective-permute-start(bf16[256,2048]{1,0:T(8,128)(2,1)} %collective-permute-done.4.refs_4_), channel_id=1, source_target_pairs={{0,4},{4,0},{1,5},{5,1},{2,6},{6,2},{3,7},{7,3},{8,12},{12,8},{9,1... | collective-permute-start | bytes 3145736 | tf_op jit(solution)/shard_map/ppermute | solution.py:296
  72.2 11.8 %collective-permute-start.3 = (bf16[256,2048]{1,0:T(8,128)(2,1)}, bf16[256,2048]{1,0:T(8,128)(2,1)}, u32[]{:S(2)}, u32[]{:S(2)}) collective-permute-start(bf16[256,2048]{1,0:T(8,128)(2,1)} %collective-permute-done.2.refs_2_), channel_id=1, source_target_pairs={{0,4},{4,0},{1,5},{5,1},{2,6},{6,2},{3,7},{7,3},{8,12},{12,8},{9,1... | collective-permute-start | bytes 3145736 | tf_op jit(solution)/shard_map/ppermute | solution.py:296
  72.4 11.6 %collective-permute-start.1 = (bf16[256,2048]{1,0:T(8,128)(2,1)}, bf16[256,2048]{1,0:T(8,128)(2,1)}, u32[]{:S(2)}, u32[]{:S(2)}) collective-permute-start(bf16[256,2048]{1,0:T(8,128)(2,1)} %collective-permute-done.refs_0_), channel_id=1, source_target_pairs={{0,4},{4,0},{1,5},{5,1},{2,6},{6,2},{3,7},{7,3},{8,12},{12,8},{9,1... | collective-permute-start | bytes 3145736 | tf_op jit(solution)/shard_map/ppermute | solution.py:296
  72.7 11.3 %all-to-all-start.2 = ((bf16[4,96,512]{2,1,0:T(8,128)(2,1)}), bf16[4,96,512]{2,1,0:T(8,128)(2,1)S(1)}, u32[]{:S(2)}, u32[]{:S(2)}) async-start(bf16[4,96,512]{2,1,0:T(8,128)(2,1)} %bitcast.6), calls=%async_computation.2 | async-start | bytes 786432 | tf_op jit(solution)/shard_map/all_to_all | solution.py:239
  84.0 1.0 copy-start.7
  89.0 0.7 copy-start.4
  89.8 11.2 %collective-permute-start.6 = (bf16[96,2048]{1,0:T(8,128)(2,1)S(1)}, bf16[96,2048]{1,0:T(8,128)(2,1)S(1)}, u32[]{:S(2)}, u32[]{:S(2)}) collective-permute-start(bf16[96,2048]{1,0:T(8,128)(2,1)S(1)} %get-tuple-element.23), channel_id=1, source_target_pairs={{0,1},{1,2},{2,3},{3,0},{4,5},{5,6},{6,7},{7,4},{8,9},{9,10},{10,1... | collective-permute-start | bytes 1179656 | tf_op jit(solution)/shard_map/ppermute | solution.py:248
  90.2 18.1 %collective-permute-start.8 = (bf16[96,2048]{1,0:T(8,128)(2,1)S(1)}, bf16[96,2048]{1,0:T(8,128)(2,1)S(1)}, u32[]{:S(2)}, u32[]{:S(2)}) collective-permute-start(bf16[96,2048]{1,0:T(8,128)(2,1)S(1)} %get-tuple-element.23), channel_id=1, source_target_pairs={{0,2},{1,3},{2,0},{3,1},{4,6},{5,7},{6,4},{7,5},{8,10},{9,11},{10,... | collective-permute-start | bytes 1179656 | tf_op jit(solution)/shard_map/ppermute | solution.py:248
  91.9 17.8 %collective-permute-start.7 = (bf16[96,2048]{1,0:T(8,128)(2,1)S(1)}, bf16[96,2048]{1,0:T(8,128)(2,1)S(1)}, u32[]{:S(2)}, u32[]{:S(2)}) collective-permute-start(bf16[96,2048]{1,0:T(8,128)(2,1)S(1)} %get-tuple-element.23), channel_id=1, source_target_pairs={{0,3},{1,0},{2,1},{3,2},{4,7},{5,4},{6,5},{7,6},{8,11},{9,8},{10,9... | collective-permute-start | bytes 1179656 | tf_op jit(solution)/shard_map/ppermute | solution.py:248
  109.8 9.1 %copy-start.13 = (bf16[2048,2816]{1,0:T(8,128)(2,1)S(1)}, bf16[2048,2816]{1,0:T(8,128)(2,1)}, u32[]{:S(2)}) copy-start(bf16[2048,2816]{1,0:T(8,128)(2,1)} %all-gather.3.cloned.1.call-done) | copy-start | bytes 34603012
  182.8 7.7 %copy-start.14 = (bf16[2048,1408]{1,0:T(8,128)(2,1)S(1)}, bf16[2048,1408]{1,0:T(8,128)(2,1)}, u32[]{:S(2)}) copy-start(bf16[2048,1408]{1,0:T(8,128)(2,1)} %all-gather.5.cloned.1.call-done) | copy-start | bytes 17301508
  187.7 21.1 %copy-start.5 = (bf16[96,2048]{1,0:T(8,128)(2,1)S(1)}, bf16[96,2048]{1,0:T(8,128)(2,1)}, u32[]{:S(2)}) copy-start(bf16[96,2048]{1,0:T(8,128)(2,1)} %copy-done.4) | copy-start | bytes 1179652
  187.7 12.0 %collective-permute-start.9 = (bf16[96,2048]{1,0:T(8,128)(2,1)S(1)}, bf16[96,2048]{1,0:T(8,128)(2,1)S(1)}, u32[]{:S(2)}, u32[]{:S(2)}) collective-permute-start(bf16[96,2048]{1,0:T(8,128)(2,1)S(1)} %slice.43), channel_id=1, source_target_pairs={{0,2},{1,3},{2,0},{3,1},{4,6},{5,7},{6,4},{7,5},{8,10},{9,11},{10,... | collective-permute-start | bytes 1179656 | tf_op jit(solution)/shard_map/ppermute | solution.py:248
  192.6 15.6 %collective-permute-start.10 = (bf16[96,2048]{1,0:T(8,128)(2,1)S(1)}, bf16[96,2048]{1,0:T(8,128)(2,1)S(1)}, u32[]{:S(2)}, u32[]{:S(2)}) collective-permute-start(bf16[96,2048]{1,0:T(8,128)(2,1)S(1)} %get-tuple-element.27), channel_id=1, source_target_pairs={{0,3},{1,0},{2,1},{3,2},{4,7},{5,4},{6,5},{7,6},{8,11},{9,8},{10,9... | collective-permute-start | bytes 1179656 | tf_op jit(solution)/shard_map/ppermute | solution.py:248
  193.6 15.2 %collective-permute-start.11 = (bf16[96,2048]{1,0:T(8,128)(2,1)S(1)}, bf16[96,2048]{1,0:T(8,128)(2,1)S(1)}, u32[]{:S(2)}, u32[]{:S(2)}) collective-permute-start(bf16[96,2048]{1,0:T(8,128)(2,1)S(1)} %get-tuple-element.28), channel_id=1, source_target_pairs={{0,1},{1,2},{2,3},{3,0},{4,5},{5,6},{6,7},{7,4},{8,9},{9,10},{10,1... | collective-permute-start | bytes 1179656 | tf_op jit(solution)/shard_map/ppermute | solution.py:248
Sparse Core Ops, SparseCore 0:
  10.1 93.1 all-gather.2
  106.0 76.7 all-gather.4

commit v3 on v2

--- a/solution.py
+++ b/solution.py
@@ -6,10 +6,10 @@
 from jax.sharding import Mesh
 from jax.sharding import PartitionSpec as P
 
+
 SP = ("sp_0", "sp_1", "sp_2")
 SP_TP = ("sp_0", "sp_1", "sp_2", "tp")
 
-BLOCK = 128
 NORM_EPSILON = 1e-06
 ROPE_BASE = 10000.0
 f32, bf16 = jnp.float32, jnp.bfloat16
@@ -84,14 +84,14 @@
 KEY_SCALES = (64**-0.5, 128**-0.5)
 
 
-def state_kernel(ld, kn, kw, v0, v1, cosine, sine, out, state):
+def state_kernel(ld, kn, kw, values, cosine, sine, out, state):
     length = kn.shape[0]
     keys = turned_all(kn, kw, cosine, sine, KEY_SCALES)
     t = rows((length, 128)).astype(f32)
     for h in range(4):
         g, i = h // 2, h % 2
-        f, b = ld[g * 2 + i], ld[4 + g * 2 + i]
-        v = (v0 if g == 0 else v1)[:, i * 128 : (i + 1) * 128].astype(f32)
+        f, b = ld[0, g, i], ld[1, g, i]
+        v = values[:, g, i * 128 : (i + 1) * 128].astype(f32)
         scaled = jnp.concatenate([v * jnp.exp(f * (length - 1.0 - t)), v * jnp.exp(b * t)], 1)
         high, low = split(scaled)
         kr = keys[0] if g == 0 else keys[1 + i]
@@ -109,25 +109,31 @@
     out[...] = state[...].astype(STATE)
 
 
-def inside_kernel(ld, qn, qw, kn, kw, v0, v1, cosine, sine, turned, inside):
+def inside_kernel(ld, qn, qw, kn, kw, values, cosine, sine, turned_out, inside_out, turned, inside, sems):
     length = qn.shape[0]
     queries = turned_all(qn, qw, cosine, sine, (1.0, 1.0))
     keys = turned_all(kn, kw, cosine, sine, KEY_SCALES)
     for k in range(3):
         turned[:, k * 128 : (k + 1) * 128] = queries[k]
+    turned_copy = pltpu.make_async_copy(turned, turned_out, sems.at[0])
+    turned_copy.start()
     lag = (rows((length, length)) - lanes((length, length))).astype(f32)
     away = jnp.abs(lag)
     for h in range(4):
         g, i = h // 2, h % 2
-        f, b = ld[g * 2 + i], ld[4 + g * 2 + i]
+        f, b = ld[0, g, i], ld[1, g, i]
         kr = keys[0] if g == 0 else keys[1 + i]
         weight = jnp.where(lag == 0, 2.0, jnp.exp(jnp.where(lag > 0, f, b) * away))
         a = (nt(of_head(queries, h), kr) * weight).astype(bf16)
-        v = (v0 if g == 0 else v1)[:, i * 128 : (i + 1) * 128]
+        v = values[:, g, i * 128 : (i + 1) * 128]
         inside[:, h * 128 : (h + 1) * 128] = nn(a, v)
-
-
-def finish_kernel(ld, turned_in, inside_in, enter_in, g0, g1, out, turned, inside, enter, sems):
+    inside_copy = pltpu.make_async_copy(inside, inside_out, sems.at[1])
+    inside_copy.start()
+    turned_copy.wait()
+    inside_copy.wait()
+
+
+def finish_kernel(ld, turned_in, inside_in, enter_in, gates, out, turned, inside, enter, sems):
     copies = [
         pltpu.make_async_copy(turned_in, turned, sems.at[0]),
         pltpu.make_async_copy(inside_in, inside, sems.at[1]),
@@ -150,7 +156,7 @@
     queries = [turned[:, k * 128 : (k + 1) * 128] for k in range(3)]
     for h in range(4):
         g, i = h // 2, h % 2
-        f, b = ld[g * 2 + i], ld[4 + g * 2 + i]
+        f, b = ld[0, g, i], ld[1, g, i]
         q = of_head(queries, h)
         high, low = states[h]
         carried = nn(q, high) + nn(q, low)
@@ -162,7 +168,7 @@
         mean = jnp.mean(ret, -1, keepdims=True)
         centred = ret - mean
         variance = jnp.mean(centred * centred, -1, keepdims=True)
-        gate = (g0 if g == 0 else g1)[:, i * 128 : (i + 1) * 128].astype(f32)
+        gate = gates[:, g, i * 128 : (i + 1) * 128].astype(f32)
         y = gate * jax.nn.sigmoid(gate) * (centred * lax.rsqrt(variance + NORM_EPSILON))
         out[:, h * 128 : (h + 1) * 128] = y.astype(bf16)
 
@@ -170,15 +176,15 @@
 def scan_kernel(ld, x, out):
     r = rows((8, 128))
 
-    def factor(base):
-        rate = jnp.full((8, 128), ld[base + 3], f32)
-        rate = jnp.where(r < 4, ld[base + 2], rate)
-        rate = jnp.where(r == 1, ld[base + 1], rate)
-        rate = jnp.where(r == 0, ld[base], rate)
+    def factor(d):
+        rate = jnp.full((8, 128), ld[d, 1, 1], f32)
+        rate = jnp.where(r < 4, ld[d, 1, 0], rate)
+        rate = jnp.where(r == 1, ld[d, 0, 1], rate)
+        rate = jnp.where(r == 0, ld[d, 0, 0], rate)
         return jnp.exp(rate * 384.0)
 
     n = x.shape[0]
-    forward, backward = factor(0), factor(4)
+    forward, backward = factor(0), factor(1)
     acc = jnp.zeros((8, 128), f32)
     for k in range(n):
         out[k, 0] = acc.astype(STATE)
@@ -202,7 +208,7 @@
             rows_in = y[tp, :, k * 256 : (k + 1) * 256]
         else:
             piece = y[(tp + 4 - (k // 2)) % 4]
-            first, second = (core, 1 - core) if k % 2 == 0 else (1 - core, core)
+            first, _ = (core, 1 - core) if k % 2 == 0 else (1 - core, core)
             rows_in = jnp.where(first == 0, piece[:, :256], piece[:, 256:])
         copy.wait()
         part = nn(rows_in, blocks[k])
@@ -219,14 +225,13 @@
 HB = pl.BlockSpec(memory_space=pltpu.HBM)
 
 
-def call(kernel, in_specs, outs, name, scratch=()):
+def call(kernel, in_specs, outs, scratch=(), out_specs=None):
     return pl.pallas_call(
         kernel,
         in_specs=in_specs,
-        out_specs=jax.tree.map(lambda _: VM, outs),
+        out_specs=out_specs or jax.tree.map(lambda _: VM, outs),
         out_shape=outs,
         scratch_shapes=scratch,
-        name=name,
         compiler_params=pltpu.CompilerParams(vmem_limit_bytes=40 * 2**20),
     )
 
@@ -265,35 +270,40 @@
 ):
     length, width = query_narrow.shape[0], stream.shape[1]
     hidden_units = mlp_gate.shape[1]
-    shards = lax.all_gather(jnp.concatenate([mlp_gate, mlp_up], 1), SP, axis=0, tiled=True)
-    full_gate, full_up = shards[:, :hidden_units], shards[:, hidden_units:]
-    full_down = lax.all_gather(mlp_down.T, SP, axis=0, tiled=True)
-
-    rates = log_decay.reshape(8)
+    shards = lax.all_gather(jnp.concatenate([mlp_gate, mlp_up, mlp_down.T], 1), SP, axis=0, tiled=True)
+    full_gate, full_up, full_down = (shards[:, k * hidden_units : (k + 1) * hidden_units] for k in range(3))
+
+    rates = log_decay
     cosine, sine = angle_tables(length, lax.axis_index(SP) * length)
-    v0, v1 = values[:, 0], values[:, 1]
-    g0, g1 = out_gate[:, 0], out_gate[:, 1]
     states = shape(64, 2, 8, 128, dtype=STATE)
-    state = call(state_kernel, [SM] + [VM] * 6, states, "state", (pltpu.VMEM((64, 2, 8, 128), f32),))(
-        rates, key_narrow, key_wide, v0, v1, cosine, sine
+    state = call(state_kernel, [SM] + [VM] * 5, states, (pltpu.VMEM((64, 2, 8, 128), f32),))(
+        rates, key_narrow, key_wide, values, cosine, sine
     )
     core = lax.axis_index("sp_2")
     half = lax.dynamic_index_in_dim(after(out_weight, state), core, 0, keepdims=False)
-    same = [shifted(half, s) for s in (1, 2, 3)]
+    same = []
+    for s in (1, 2, 3):
+        same.append(shifted(half, s))
+    kept = [((length, 384), bf16), ((length, 512), f32)]
     turned, inside = call(
-        inside_kernel, [SM] + [VM] * 8, (shape(length, 384, dtype=bf16), shape(length, 512)), "inside"
-    )(rates, query_narrow, query_wide, key_narrow, key_wide, v0, v1, cosine, sine)
+        inside_kernel,
+        [SM] + [VM] * 7,
+        tuple(pltpu.HBM(*k) for k in kept),
+        tuple(pltpu.VMEM(*k) for k in kept) + (pltpu.SemaphoreType.DMA((2,)),),
+        (HB, HB),
+    )(rates, query_narrow, query_wide, key_narrow, key_wide, values, cosine, sine)
     arrived = exchanged(state, SP)
-    enter = call(scan_kernel, [SM, VM], states, "scan")(rates, arrived)
+    enter = call(scan_kernel, [SM, VM], states)(rates, arrived)
     enter = exchanged(enter, SP)
     y = call(
         finish_kernel,
-        [SM, HB, HB, VM, VM, VM],
+        [SM, HB, HB, VM, VM],
         shape(length, 512, dtype=bf16),
-        "finish",
         (pltpu.VMEM((length, 384), bf16), pltpu.VMEM((length, 512), f32), pltpu.VMEM((64, 2, 8, 128), f32), pltpu.SemaphoreType.DMA((2,))),
-    )(rates, turned, inside, enter, g0, g1)
-    other = [lax.ppermute(after(w, y), "sp_2", [(0, 1), (1, 0)]) for w in same]
+    )(rates, turned, inside, enter, out_gate)
+    other = []
+    for s in (1, 2, 3):
+        other.append(lax.ppermute(after(same[s - 1], y), "sp_2", [(0, 1), (1, 0)]))
     n_tp = lax.axis_size("tp")
     y = exchanged(y.reshape(n_tp, length // n_tp, 512), "tp")
     own = shape(length // n_tp, width, dtype=bf16)
@@ -303,7 +313,6 @@
         proj_kernel,
         [SM, VM, VM, VM] + [HB] * 7,
         (own, own),
-        "proj",
         (pltpu.VMEM((8, 256, width), bf16), pltpu.SemaphoreType.DMA((8,))),
     )(place, y, stream, norm_gain[None], out_weight, *pieces)
 
@@ -314,7 +323,6 @@
 
     near = mixed(jnp.concatenate([shifted(normed, 1), shifted(normed, 3)], 0))
     far = mixed(jnp.concatenate([normed, shifted(normed, 2)], 0))
-    near, far, full_down = lax.optimization_barrier((near, far, full_down))
     near = nt(near, full_down).astype(bf16)
     far = nt(far, full_down).astype(bf16)
     n = length // n_tp

time: 217 us -> 169 us (0.78)
  waiting for transfers between devices: 109 us -> 47.8 us
  matrix products: 18.9 us -> 26 us
  Pallas kernels: 11.8 us -> 15.9 us
    all_gather x2 -> x1, waiting for transfers between devices: 60.9 us -> 4.45 us  [body(): lax.all_gather(jnp.concatenate([mlp_gate, mlp_up, mlp_down.T], 1), SP, ax...]
    dot_general x2 -> x0, matrix products: 9.05 us -> none  [mixed(): gate_act = jnp.dot(x, full_gate, preferred_element_type=f32)]
    dot_general x2, matrix products: 6.89 us -> 15.9 us  [nt(): lax.dot_general(a, b, (((1,), (1,)), ((), ())), preferred_element_type=f32)]
    dot_general x2, matrix products: 2.96 us -> 10.1 us  [mixed(): up_act = jnp.dot(x, full_up, preferred_element_type=f32)]
    unnamed x32 -> x38, local copies, waits for them, and re-layouts: 4.86 us -> 9.41 us
    pallas_call x5, Pallas kernels: 11.8 us -> 15.9 us  [the longest x1 4.13 us: body(): call(finish_kernel, [SM, HB, HB, VM, VM], shape(length, 512, dtype=bf16),...]
    slice x2 -> x0, local copies, waits for them, and re-layouts: 4.12 us -> none  [the longest x1 2.18 us: body(): g0, g1 = (out_gate[:, 0], out_gate[:, 1])]
    ppermute x9, waiting for transfers between devices: 31.6 us -> 27.6 us  [shifted(): return lax.ppermute(x, 'tp', [(k, (k + by) % n) for k in range(n)])]
  transfers between devices with their start and end apart: 16 -> 15, of which waited for: 9 -> 8; matrix products, arithmetic and copies ran while one was open for 10% -> 9% of each run, Pallas kernels for 5% -> 9%
where the time goes in v3:
time: 169 us; the launch traced here: 168 us
  waiting for transfers between devices  47.8 us (28%)
  blocking collectives  28 us (17%)
  matrix products  26 us (15%)
  starting transfers between devices  22.1 us (13%)
  Pallas kernels  15.9 us (9%)
  between operations  13.7 us (8%)
  local copies, waits for them, and re-layouts  10.6 us (6%)
  other arithmetic  3.85 us (2%)
    all_to_all x1, blocking collectives, exchanged(): return lax.all_to_all(x, axis, 0, 0, tiled=True)  28 us
    ppermute x9, waiting for transfers between devices, shifted(): return lax.ppermute(x, 'tp', [(k, (k + by) % n) for k in range(n)])  27.6 us
    dot_general x2, matrix products, nt(): lax.dot_general(a, b, (((1,), (1,)), ((), ())), preferred_element_type=f32)  15.9 us
    all_to_all x2, waiting for transfers between devices, exchanged(): return lax.all_to_all(x, axis, 0, 0, tiled=True)  15.7 us
    ppermute x9, starting transfers between devices, shifted(): return lax.ppermute(x, 'tp', [(k, (k + by) % n) for k in range(n)])  12.6 us
    dot_general x2, matrix products, mixed(): up_act = jnp.dot(x, full_up, preferred_element_type=f32)  10.1 us
    unnamed x38, local copies, waits for them, and re-layouts  9.41 us
    all_to_all x2, starting transfers between devices, exchanged(): return lax.all_to_all(x, axis, 0, 0, tiled=True)  8.55 us
  transfers between devices with their start and end apart: 15, of which 8 were waited for; matrix products, arithmetic and copies ran while one was open for 9% of the time, Pallas kernels for 9%

profile of v3, /device:TPU:1, one launch (start us, length us, event | category | flops | bytes accessed | tf_op | source)
XLA Modules:
  0.0 168.0 jit_solution(9342451028223208337)
XLA Ops:
  6.5 1.8 %pad_maximum_fusion = bf16[32,4224]{1,0:T(8,128)(2,1)} fusion(bf16[32,1408]{1,0:T(8,128)(2,1)} %bitcast.12, bf16[32,1408]{1,0:T(8,128)(2,1)} %param.23, bf16[32,1408]{1,0:T(8,128)(2,1)} %param.22), kind=kLoop, calls=%fused_computation.22 | loop fusion | flops 811008 | bytes 540672 | tf_op jit(solution)/shard_map/concatenate | solution.py:273
  9.3 1.0 copy-done.1
  12.8 2.5 %shard_map.128 = bf16[64,2,8,128]{3,2,1,0:T(8,128)(2,1)S(1)} custom-call(f32[2,2,2]{2,1,0:T(2,128)S(1)} %copy-done.15, bf16[384,128]{1,0:T(8,128)(2,1)S(1)} %copy-done.10, bf16[384,256]{1,0:T(8,128)(2,1)S(1)} %copy-done.4, bf16[384,2,256]{2,1,0:T(2,128)(2,1)S(1)} %copy-done.1, f32[384,128]{1,0:T(8,128)S(1)} %get-tuple-element.24.cosine, ...), custom_call_target="tpu_custom_call" | custom-call | tf_op jit(solution)/shard_map/pallas_call | solution.py:279
  15.4 1.0 dynamic-slice_bitcast_fusion
  16.5 3.7 %collective-permute-start.2 = (bf16[256,2048]{1,0:T(8,128)(2,1)}, bf16[256,2048]{1,0:T(8,128)(2,1)}, u32[]{:S(2)}, u32[]{:S(2)}) collective-permute-start(bf16[256,2048]{1,0:T(8,128)(2,1)} %dynamic-slice_bitcast_fusion), channel_id=1, source_target_pairs={{0,2},{1,3},{2,0},{3,1},{4,6},{5,7},{6,4},{7,5},{8,10},{9,11},{10,... | collective-permute-start | bytes 3145736 | tf_op jit(solution)/shard_map/ppermute | solution.py:253
  21.7 28.0 %all_to_all.15.x = bf16[64,2,8,128]{3,2,1,0:T(8,128)(2,1)S(1)} all-to-all(bf16[64,2,8,128]{3,2,1,0:T(8,128)(2,1)S(1)} %shard_map.128), channel_id=1, replica_groups=mesh['sp_0'=8,'sp_1'=4,'sp_2'=2,'tp'=4] {'sp_0','sp_1','sp_2'}, dimensions={0} | all-to-all | bytes 524288 | tf_op jit(solution)/shard_map/all_to_all | solution.py:244
  49.6 1.4 shard_map.129
  51.1 5.1 %all-to-all-start.1 = ((bf16[64,2,8,128]{3,2,1,0:T(8,128)(2,1)}), bf16[64,2,8,128]{3,2,1,0:T(8,128)(2,1)S(1)}, u32[]{:S(2)}, u32[]{:S(2)}) async-start(bf16[64,2,8,128]{3,2,1,0:T(8,128)(2,1)} %shard_map.129), calls=%async_computation.1 | async-start | bytes 524288 | tf_op jit(solution)/shard_map/all_to_all | solution.py:244
  57.1 4.0 %shard_map.127 = (bf16[384,384]{1,0:T(8,128)(2,1)}, f32[384,512]{1,0:T(8,128)}) custom-call(f32[2,2,2]{2,1,0:T(2,128)S(1)} %copy-done.16, bf16[384,128]{1,0:T(8,128)(2,1)S(1)} %copy-done.14, bf16[384,256]{1,0:T(8,128)(2,1)S(1)} %copy-done.13, bf16[384,128]{1,0:T(8,128)(2,1)S(1)} %copy-done.11, bf16[384,256]{1,0:T(8,128)(2,1)S(1)} %copy-done.5, ...), custom_call_target="tpu_custom_call" | custom-call | tf_op jit(solution)/shard_map/pallas_call | solution.py:288
  61.1 8.1 %all-to-all-done.1.enter_in = bf16[64,2,8,128]{3,2,1,0:T(8,128)(2,1)S(1)} async-done(((bf16[64,2,8,128]{3,2,1,0:T(8,128)(2,1)}), bf16[64,2,8,128]{3,2,1,0:T(8,128)(2,1)S(1)}, u32[]{:S(2)}, u32[]{:S(2)}) %all-to-all-start.1) | async-done | bytes 262176 | tf_op jit(solution)/shard_map/all_to_all | solution.py:244
  69.2 1.2 copy-done.3
  70.4 1.0 copy-done.6
  71.4 1.0 copy-done.12
  72.4 4.1 %shard_map.130 = bf16[384,512]{1,0:T(8,128)(2,1)} custom-call(f32[2,2,2]{2,1,0:T(2,128)S(1)} %copy-done.16, bf16[384,384]{1,0:T(8,128)(2,1)S(1)} %copy-done.12, f32[384,512]{1,0:T(8,128)S(1)} %copy-done.3, bf16[64,2,8,128]{3,2,1,0:T(8,128)(2,1)S(1)} %all-to-all-done.1.enter_in, bf16[384,2,256]{2,1,0:T(2,128)(2,1)S(1)} %copy-done.6), custom_call_target="tpu_custom_call" | custom-call | tf_op jit(solution)/shard_map/pallas_call | solution.py:298
  77.6 3.5 %all-to-all-start.2 = ((bf16[4,96,512]{2,1,0:T(8,128)(2,1)}), bf16[4,96,512]{2,1,0:T(8,128)(2,1)S(1)}, u32[]{:S(2)}, u32[]{:S(2)}) async-start(bf16[4,96,512]{2,1,0:T(8,128)(2,1)} %bitcast.2), calls=%async_computation.2 | async-start | bytes 786432 | tf_op jit(solution)/shard_map/all_to_all | solution.py:244
  81.1 7.6 %all-to-all-done.2.y = bf16[4,96,512]{2,1,0:T(8,128)(2,1)S(1)} async-done(((bf16[4,96,512]{2,1,0:T(8,128)(2,1)}), bf16[4,96,512]{2,1,0:T(8,128)(2,1)S(1)}, u32[]{:S(2)}, u32[]{:S(2)}) %all-to-all-start.2) | async-done | bytes 393248 | tf_op jit(solution)/shard_map/all_to_all | solution.py:244
  88.8 1.0 copy-done.9
  89.8 3.9 %shard_map.131 = (bf16[96,2048]{1,0:T(8,128)(2,1)S(1)}, bf16[96,2048]{1,0:T(8,128)(2,1)S(1)}) custom-call(s32[2]{0:T(128)S(1)} %pad_add_fusion.place, bf16[4,96,512]{2,1,0:T(8,128)(2,1)S(1)} %all-to-all-done.2.y, bf16[96,2048]{1,0:T(8,128)(2,1)S(1)} %copy-done.9, f32[1,2048]{1,0:T(1,128)S(1)} %bitcast.11, bf16[2,256,2048]{2,1,0:T(8,128)(2,1)S(1)} %copy-done, ...), custom_call_target="tpu_custom_call" | custom-call | tf_op jit(solution)/shard_map/pallas_call | solution.py:312
  95.0 1.8 %collective-permute-start.6 = (bf16[96,2048]{1,0:T(8,128)(2,1)S(1)}, bf16[96,2048]{1,0:T(8,128)(2,1)S(1)}, u32[]{:S(2)}, u32[]{:S(2)}) collective-permute-start(bf16[96,2048]{1,0:T(8,128)(2,1)S(1)} %get-tuple-element.20), channel_id=1, source_target_pairs={{0,2},{1,3},{2,0},{3,1},{4,6},{5,7},{6,4},{7,5},{8,10},{9,11},{10,... | collective-permute-start | bytes 1179656 | tf_op jit(solution)/shard_map/ppermute | solution.py:253
  97.4 7.5 %collective-permute-done.8 = bf16[96,2048]{1,0:T(8,128)(2,1)S(1)} collective-permute-done((bf16[96,2048]{1,0:T(8,128)(2,1)S(1)}, bf16[96,2048]{1,0:T(8,128)(2,1)S(1)}, u32[]{:S(2)}, u32[]{:S(2)}) %collective-permute-start.8) | collective-permute-done | bytes 393248 | tf_op jit(solution)/shard_map/ppermute | solution.py:253
  105.0 8.5 %collective-permute-done.6 = bf16[96,2048]{1,0:T(8,128)(2,1)S(1)} collective-permute-done((bf16[96,2048]{1,0:T(8,128)(2,1)S(1)}, bf16[96,2048]{1,0:T(8,128)(2,1)S(1)}, u32[]{:S(2)}, u32[]{:S(2)}) %collective-permute-start.6) | collective-permute-done | bytes 393248 | tf_op jit(solution)/shard_map/ppermute | solution.py:253
  113.5 1.1 collective-permute-done.9
  114.7 4.5 %all-gather.2.cloned.1.call-done = bf16[2048,4224]{1,0:T(8,128)(2,1)} async-done(((bf16[32,4224]{1,0:T(8,128)(2,1)}), bf16[2048,4224]{1,0:T(8,128)(2,1)}) %all-gather.2.cloned.1.call-update) | async-done | bytes 17301520 | tf_op jit(solution)/shard_map/all_gather | solution.py:273
  119.1 5.1 %fusion.6 = f32[192,1408]{1,0:T(8,128)} fusion(bf16[192,2048]{1,0:T(8,128)(2,1)S(1)} %constant_dynamic-update-slice_fusion, bf16[2048,4224]{1,0:T(8,128)(2,1)} %all-gather.2.cloned.1.call-done), kind=kOutput, calls=%fused_computation.6 | convolution fusion | flops 1107296256 | bytes 7634944 | tf_op jit(solution)/shard_map/dot_general | solution.py:321
  124.2 7.9 %fusion.12 = bf16[192,2048]{1,0:T(8,128)(2,1)S(1)} fusion(bf16[2048,4224]{1,0:T(8,128)(2,1)} %all-gather.2.cloned.1.call-done, f32[192,1408]{1,0:T(8,128)} %fusion.6, bf16[192,2048]{1,0:T(8,128)(2,1)S(1)} %constant_dynamic-update-slice_fusion), kind=kOutput, calls=%fused_computation.12 | convolution fusion | flops 2216607744 | bytes 14188544 | tf_op jit(solution)/shard_map/dot_general | solution.py:56
  132.2 2.8 %collective-permute-start.7 = (bf16[96,2048]{1,0:T(8,128)(2,1)S(1)}, bf16[96,2048]{1,0:T(8,128)(2,1)S(1)}, u32[]{:S(2)}, u32[]{:S(2)}) collective-permute-start(bf16[96,2048]{1,0:T(8,128)(2,1)S(1)} %slice.32), channel_id=1, source_target_pairs={{0,2},{1,3},{2,0},{3,1},{4,6},{5,7},{6,4},{7,5},{8,10},{9,11},{10,... | collective-permute-start | bytes 1179656 | tf_op jit(solution)/shard_map/ppermute | solution.py:253
  135.0 5.1 %fusion.4 = f32[192,1408]{1,0:T(8,128)} fusion(bf16[192,2048]{1,0:T(8,128)(2,1)S(1)} %constant_dynamic-update-slice_fusion.2, bf16[2048,4224]{1,0:T(8,128)(2,1)} %all-gather.2.cloned.1.call-done), kind=kOutput, calls=%fused_computation.4 | convolution fusion | flops 1107296256 | bytes 7634944 | tf_op jit(solution)/shard_map/dot_general | solution.py:321
  140.0 8.0 %fusion.15 = bf16[192,2048]{1,0:T(8,128)(2,1)S(1)} fusion(bf16[2048,4224]{1,0:T(8,128)(2,1)} %all-gather.2.cloned.1.call-done, f32[192,1408]{1,0:T(8,128)} %fusion.4, bf16[192,2048]{1,0:T(8,128)(2,1)S(1)} %constant_dynamic-update-slice_fusion.2), kind=kOutput, calls=%fused_computation.13 | convolution fusion | flops 2216607744 | bytes 14188544 | tf_op jit(solution)/shard_map/dot_general | solution.py:56
  148.1 1.0 collective-permute-start.10
  149.6 8.7 %collective-permute-done.10 = bf16[96,2048]{1,0:T(8,128)(2,1)S(1)} collective-permute-done((bf16[96,2048]{1,0:T(8,128)(2,1)S(1)}, bf16[96,2048]{1,0:T(8,128)(2,1)S(1)}, u32[]{:S(2)}, u32[]{:S(2)}) %collective-permute-start.10) | collective-permute-done | bytes 393248 | tf_op jit(solution)/shard_map/ppermute | solution.py:253
  158.3 1.8 %collective-permute-done.11 = bf16[96,2048]{1,0:T(8,128)(2,1)S(1)} collective-permute-done((bf16[96,2048]{1,0:T(8,128)(2,1)S(1)}, bf16[96,2048]{1,0:T(8,128)(2,1)S(1)}, u32[]{:S(2)}, u32[]{:S(2)}) %collective-permute-start.11) | collective-permute-done | bytes 393248 | tf_op jit(solution)/shard_map/ppermute | solution.py:253
  160.1 1.1 add_convert_fusion
  (60 shorter events, 9.7 us)
Async XLA Ops:
  6.5 8.9 %copy-start = (bf16[2,256,2048]{2,1,0:T(8,128)(2,1)S(1)}, bf16[2,256,2048]{2,1,0:T(8,128)(2,1)}, u32[]{:S(2)}) copy-start(bf16[2,256,2048]{2,1,0:T(8,128)(2,1)} %own.1) | copy-start | bytes 6291460
  6.5 112.6 %all-gather.2.cloned.1.call-start = ((), (), s32[]{:S(2)}) async-start(), calls=%async_computation.3 | async-start | bytes 17571840 | tf_op jit(solution)/shard_map/all_gather | solution.py:273
  9.3 1.0 copy-start.1
  10.3 0.9 copy-start.4
  11.2 0.9 copy-start.10
  12.8 36.8 %copy-start.16 = (f32[2,2,2]{2,1,0:T(2,128)S(1)}, f32[2,2,2]{2,1,0:T(2,128)}, u32[]{:S(2)}) copy-start(f32[2,2,2]{2,1,0:T(2,128)} %ld.7) | copy-start | bytes 100
  15.4 40.8 %copy-start.2 = (bf16[384,2,256]{2,1,0:T(2,128)(2,1)S(1)}, bf16[384,2,256]{2,1,0:T(2,128)(2,1)}, u32[]{:S(2)}) copy-start(bf16[384,2,256]{2,1,0:T(2,128)(2,1)} %values.3) | copy-start | bytes 1179652
  15.4 40.8 %copy-start.5 = (bf16[384,256]{1,0:T(8,128)(2,1)S(1)}, bf16[384,256]{1,0:T(8,128)(2,1)}, u32[]{:S(2)}) copy-start(bf16[384,256]{1,0:T(8,128)(2,1)} %kw.3) | copy-start | bytes 589828
  15.4 40.8 %copy-start.11 = (bf16[384,128]{1,0:T(8,128)(2,1)S(1)}, bf16[384,128]{1,0:T(8,128)(2,1)}, u32[]{:S(2)}) copy-start(bf16[384,128]{1,0:T(8,128)(2,1)} %kn.3) | copy-start | bytes 294916
  15.4 40.8 %copy-start.14 = (bf16[384,128]{1,0:T(8,128)(2,1)S(1)}, bf16[384,128]{1,0:T(8,128)(2,1)}, u32[]{:S(2)}) copy-start(bf16[384,128]{1,0:T(8,128)(2,1)} %qn.1) | copy-start | bytes 294916
  16.5 60.1 %collective-permute-start.2 = (bf16[256,2048]{1,0:T(8,128)(2,1)}, bf16[256,2048]{1,0:T(8,128)(2,1)}, u32[]{:S(2)}, u32[]{:S(2)}) collective-permute-start(bf16[256,2048]{1,0:T(8,128)(2,1)} %dynamic-slice_bitcast_fusion), channel_id=1, source_target_pairs={{0,2},{1,3},{2,0},{3,1},{4,6},{5,7},{6,4},{7,5},{8,10},{9,11},{10,... | collective-permute-start | bytes 3145736 | tf_op jit(solution)/shard_map/ppermute | solution.py:253
  20.2 56.9 %collective-permute-start.4 = (bf16[256,2048]{1,0:T(8,128)(2,1)}, bf16[256,2048]{1,0:T(8,128)(2,1)}, u32[]{:S(2)}, u32[]{:S(2)}) collective-permute-start(bf16[256,2048]{1,0:T(8,128)(2,1)} %dynamic-slice_bitcast_fusion), channel_id=1, source_target_pairs={{0,3},{1,0},{2,1},{3,2},{4,7},{5,4},{6,5},{7,6},{8,11},{9,8},{10,9... | collective-permute-start | bytes 3145736 | tf_op jit(solution)/shard_map/ppermute | solution.py:253
  21.0 56.2 %collective-permute-start = (bf16[256,2048]{1,0:T(8,128)(2,1)}, bf16[256,2048]{1,0:T(8,128)(2,1)}, u32[]{:S(2)}, u32[]{:S(2)}) collective-permute-start(bf16[256,2048]{1,0:T(8,128)(2,1)} %dynamic-slice_bitcast_fusion), channel_id=1, source_target_pairs={{0,1},{1,2},{2,3},{3,0},{4,5},{5,6},{6,7},{7,4},{8,9},{9,10},{10,1... | collective-permute-start | bytes 3145736 | tf_op jit(solution)/shard_map/ppermute | solution.py:253
  51.1 18.2 %all-to-all-start.1 = ((bf16[64,2,8,128]{3,2,1,0:T(8,128)(2,1)}), bf16[64,2,8,128]{3,2,1,0:T(8,128)(2,1)S(1)}, u32[]{:S(2)}, u32[]{:S(2)}) async-start(bf16[64,2,8,128]{3,2,1,0:T(8,128)(2,1)} %shard_map.129), calls=%async_computation.1 | async-start | bytes 524288 | tf_op jit(solution)/shard_map/all_to_all | solution.py:244
  56.2 0.9 copy-start.13
  57.1 31.6 %copy-start.17 = (f32[2048]{0:T(1024)S(1)}, f32[2048]{0:T(1024)}, u32[]{:S(2)}) copy-start(f32[2048]{0:T(1024)} %param.21) | copy-start | bytes 24580
  69.2 1.2 copy-start.3
  70.4 1.0 copy-start.6
  71.4 1.0 copy-start.12
  76.5 12.2 %collective-permute-start.3 = (bf16[256,2048]{1,0:T(8,128)(2,1)}, bf16[256,2048]{1,0:T(8,128)(2,1)S(1)}, u32[]{:S(2)}, u32[]{:S(2)}) collective-permute-start(bf16[256,2048]{1,0:T(8,128)(2,1)} %collective-permute-done.2.refs_2_), channel_id=1, source_target_pairs={{0,4},{4,0},{1,5},{5,1},{2,6},{6,2},{3,7},{7,3},{8,12},{12,8},{9,1... | collective-permute-start | bytes 3145736 | tf_op jit(solution)/shard_map/ppermute | solution.py:306
  77.1 11.7 %collective-permute-start.5 = (bf16[256,2048]{1,0:T(8,128)(2,1)}, bf16[256,2048]{1,0:T(8,128)(2,1)}, u32[]{:S(2)}, u32[]{:S(2)}) collective-permute-start(bf16[256,2048]{1,0:T(8,128)(2,1)} %collective-permute-done.4.refs_4_), channel_id=1, source_target_pairs={{0,4},{4,0},{1,5},{5,1},{2,6},{6,2},{3,7},{7,3},{8,12},{12,8},{9,1... | collective-permute-start | bytes 3145736 | tf_op jit(solution)/shard_map/ppermute | solution.py:306
  77.2 11.6 %collective-permute-start.1 = (bf16[256,2048]{1,0:T(8,128)(2,1)}, bf16[256,2048]{1,0:T(8,128)(2,1)}, u32[]{:S(2)}, u32[]{:S(2)}) collective-permute-start(bf16[256,2048]{1,0:T(8,128)(2,1)} %collective-permute-done.refs_0_), channel_id=1, source_target_pairs={{0,4},{4,0},{1,5},{5,1},{2,6},{6,2},{3,7},{7,3},{8,12},{12,8},{9,1... | collective-permute-start | bytes 3145736 | tf_op jit(solution)/shard_map/ppermute | solution.py:306
  77.6 11.2 %all-to-all-start.2 = ((bf16[4,96,512]{2,1,0:T(8,128)(2,1)}), bf16[4,96,512]{2,1,0:T(8,128)(2,1)S(1)}, u32[]{:S(2)}, u32[]{:S(2)}) async-start(bf16[4,96,512]{2,1,0:T(8,128)(2,1)} %bitcast.2), calls=%async_computation.2 | async-start | bytes 786432 | tf_op jit(solution)/shard_map/all_to_all | solution.py:244
  88.8 1.0 copy-start.9
  93.7 0.7 copy-start.7
  94.4 10.5 %collective-permute-start.8 = (bf16[96,2048]{1,0:T(8,128)(2,1)S(1)}, bf16[96,2048]{1,0:T(8,128)(2,1)S(1)}, u32[]{:S(2)}, u32[]{:S(2)}) collective-permute-start(bf16[96,2048]{1,0:T(8,128)(2,1)S(1)} %get-tuple-element.20), channel_id=1, source_target_pairs={{0,1},{1,2},{2,3},{3,0},{4,5},{5,6},{6,7},{7,4},{8,9},{9,10},{10,1... | collective-permute-start | bytes 1179656 | tf_op jit(solution)/shard_map/ppermute | solution.py:253
  95.0 18.5 %collective-permute-start.6 = (bf16[96,2048]{1,0:T(8,128)(2,1)S(1)}, bf16[96,2048]{1,0:T(8,128)(2,1)S(1)}, u32[]{:S(2)}, u32[]{:S(2)}) collective-permute-start(bf16[96,2048]{1,0:T(8,128)(2,1)S(1)} %get-tuple-element.20), channel_id=1, source_target_pairs={{0,2},{1,3},{2,0},{3,1},{4,6},{5,7},{6,4},{7,5},{8,10},{9,11},{10,... | collective-permute-start | bytes 1179656 | tf_op jit(solution)/shard_map/ppermute | solution.py:253
  96.8 17.8 %collective-permute-start.9 = (bf16[96,2048]{1,0:T(8,128)(2,1)S(1)}, bf16[96,2048]{1,0:T(8,128)(2,1)S(1)}, u32[]{:S(2)}, u32[]{:S(2)}) collective-permute-start(bf16[96,2048]{1,0:T(8,128)(2,1)S(1)} %get-tuple-element.20), channel_id=1, source_target_pairs={{0,3},{1,0},{2,1},{3,2},{4,7},{5,4},{6,5},{7,6},{8,11},{9,8},{10,9... | collective-permute-start | bytes 1179656 | tf_op jit(solution)/shard_map/ppermute | solution.py:253
  132.2 17.5 %collective-permute-start.7 = (bf16[96,2048]{1,0:T(8,128)(2,1)S(1)}, bf16[96,2048]{1,0:T(8,128)(2,1)S(1)}, u32[]{:S(2)}, u32[]{:S(2)}) collective-permute-start(bf16[96,2048]{1,0:T(8,128)(2,1)S(1)} %slice.32), channel_id=1, source_target_pairs={{0,2},{1,3},{2,0},{3,1},{4,6},{5,7},{6,4},{7,5},{8,10},{9,11},{10,... | collective-permute-start | bytes 1179656 | tf_op jit(solution)/shard_map/ppermute | solution.py:253
  140.0 20.1 %copy-start.8 = (bf16[96,2048]{1,0:T(8,128)(2,1)S(1)}, bf16[96,2048]{1,0:T(8,128)(2,1)}, u32[]{:S(2)}) copy-start(bf16[96,2048]{1,0:T(8,128)(2,1)} %copy-done.7) | copy-start | bytes 1179652
  148.1 10.2 %collective-permute-start.10 = (bf16[96,2048]{1,0:T(8,128)(2,1)S(1)}, bf16[96,2048]{1,0:T(8,128)(2,1)S(1)}, u32[]{:S(2)}, u32[]{:S(2)}) collective-permute-start(bf16[96,2048]{1,0:T(8,128)(2,1)S(1)} %get-tuple-element.21), channel_id=1, source_target_pairs={{0,3},{1,0},{2,1},{3,2},{4,7},{5,4},{6,5},{7,6},{8,11},{9,8},{10,9... | collective-permute-start | bytes 1179656 | tf_op jit(solution)/shard_map/ppermute | solution.py:253
  149.0 11.1 %collective-permute-start.11 = (bf16[96,2048]{1,0:T(8,128)(2,1)S(1)}, bf16[96,2048]{1,0:T(8,128)(2,1)S(1)}, u32[]{:S(2)}, u32[]{:S(2)}) collective-permute-start(bf16[96,2048]{1,0:T(8,128)(2,1)S(1)} %get-tuple-element.22), channel_id=1, source_target_pairs={{0,1},{1,2},{2,3},{3,0},{4,5},{5,6},{6,7},{7,4},{8,9},{9,10},{10,1... | collective-permute-start | bytes 1179656 | tf_op jit(solution)/shard_map/ppermute | solution.py:253
  (1 other events, 0.7 us)
Sparse Core Ops, SparseCore 0:
  10.1 109.0 all-gather.1

commit v4 on v3

--- a/solution.py
+++ b/solution.py
@@ -65,6 +65,7 @@
 
 
 STATE = bf16
+STAGES = 4
 
 
 def turned_all(narrow, wide, cosine, sine, scales):
@@ -84,14 +85,14 @@
 KEY_SCALES = (64**-0.5, 128**-0.5)
 
 
-def state_kernel(ld, kn, kw, values, cosine, sine, out, state):
+def state_kernel(ld, kn, kw, v0, v1, cosine, sine, out, state):
     length = kn.shape[0]
     keys = turned_all(kn, kw, cosine, sine, KEY_SCALES)
     t = rows((length, 128)).astype(f32)
     for h in range(4):
         g, i = h // 2, h % 2
         f, b = ld[0, g, i], ld[1, g, i]
-        v = values[:, g, i * 128 : (i + 1) * 128].astype(f32)
+        v = (v0 if g == 0 else v1)[:, i * 128 : (i + 1) * 128].astype(f32)
         scaled = jnp.concatenate([v * jnp.exp(f * (length - 1.0 - t)), v * jnp.exp(b * t)], 1)
         high, low = split(scaled)
         kr = keys[0] if g == 0 else keys[1 + i]
@@ -109,7 +110,7 @@
     out[...] = state[...].astype(STATE)
 
 
-def inside_kernel(ld, qn, qw, kn, kw, values, cosine, sine, turned_out, inside_out, turned, inside, sems):
+def inside_kernel(ld, qn, qw, kn, kw, v0, v1, cosine, sine, turned_out, inside_out, turned, inside, sems):
     length = qn.shape[0]
     queries = turned_all(qn, qw, cosine, sine, (1.0, 1.0))
     keys = turned_all(kn, kw, cosine, sine, KEY_SCALES)
@@ -125,7 +126,7 @@
         kr = keys[0] if g == 0 else keys[1 + i]
         weight = jnp.where(lag == 0, 2.0, jnp.exp(jnp.where(lag > 0, f, b) * away))
         a = (nt(of_head(queries, h), kr) * weight).astype(bf16)
-        v = values[:, g, i * 128 : (i + 1) * 128]
+        v = (v0 if g == 0 else v1)[:, i * 128 : (i + 1) * 128]
         inside[:, h * 128 : (h + 1) * 128] = nn(a, v)
     inside_copy = pltpu.make_async_copy(inside, inside_out, sems.at[1])
     inside_copy.start()
@@ -133,7 +134,7 @@
     inside_copy.wait()
 
 
-def finish_kernel(ld, turned_in, inside_in, enter_in, gates, out, turned, inside, enter, sems):
+def finish_kernel(ld, turned_in, inside_in, enter_in, g0, g1, out, turned, inside, enter, sems):
     copies = [
         pltpu.make_async_copy(turned_in, turned, sems.at[0]),
         pltpu.make_async_copy(inside_in, inside, sems.at[1]),
@@ -168,7 +169,7 @@
         mean = jnp.mean(ret, -1, keepdims=True)
         centred = ret - mean
         variance = jnp.mean(centred * centred, -1, keepdims=True)
-        gate = gates[:, g, i * 128 : (i + 1) * 128].astype(f32)
+        gate = (g0 if g == 0 else g1)[:, i * 128 : (i + 1) * 128].astype(f32)
         y = gate * jax.nn.sigmoid(gate) * (centred * lax.rsqrt(variance + NORM_EPSILON))
         out[:, h * 128 : (h + 1) * 128] = y.astype(bf16)
 
@@ -244,8 +245,36 @@
     return lax.all_to_all(x, axis, 0, 0, tiled=True)
 
 
+def mixer_kernel(first, second, weights, out_a, out_b, held, act, hidden, sems):
+    n, width = first.shape
+    units = hidden.shape[1]
+    step = width // STAGES
+    spans = [pl.ds(k * step, step) for k in range(STAGES)]
+    parts = [(span, pl.ds(at, size)) for at, size in ((0, 2 * units), (2 * units, units)) for span in spans]
+    copies = [pltpu.make_async_copy(weights.at[p], held.at[p], sems.at[k]) for k, p in enumerate(parts)]
+    for copy in copies:
+        copy.start()
+    for k, span in enumerate(spans):
+        x = jnp.concatenate([first[:, span], second[:, span]], 0)
+        copies[k].wait()
+        part = nn(x, held[span, : 2 * units])
+        act[...] = part if k == 0 else act[...] + part
+    gate = act[:, :units]
+    hidden[...] = (gate * jax.nn.sigmoid(gate) * act[:, units:]).astype(bf16)
+    h = hidden[...]
+    for k, span in enumerate(spans):
+        copies[STAGES + k].wait()
+        part = nt(h, held[span, 2 * units :]).astype(bf16)
+        out_a[:, span] = part[:n]
+        out_b[:, span] = part[n:]
+
+
 def after(x, token):
     return lax.optimization_barrier((x, token))[0]
+
+
+def in_hbm(x):
+    return pltpu.with_memory_space_constraint(x, pltpu.HBM)
 
 
 def shifted(x, by):
@@ -271,13 +300,14 @@
     length, width = query_narrow.shape[0], stream.shape[1]
     hidden_units = mlp_gate.shape[1]
     shards = lax.all_gather(jnp.concatenate([mlp_gate, mlp_up, mlp_down.T], 1), SP, axis=0, tiled=True)
-    full_gate, full_up, full_down = (shards[:, k * hidden_units : (k + 1) * hidden_units] for k in range(3))
 
     rates = log_decay
     cosine, sine = angle_tables(length, lax.axis_index(SP) * length)
+    v0, v1 = values[:, 0], values[:, 1]
+    g0, g1 = out_gate[:, 0], out_gate[:, 1]
     states = shape(64, 2, 8, 128, dtype=STATE)
-    state = call(state_kernel, [SM] + [VM] * 5, states, (pltpu.VMEM((64, 2, 8, 128), f32),))(
-        rates, key_narrow, key_wide, values, cosine, sine
+    state = call(state_kernel, [SM] + [VM] * 6, states, (pltpu.VMEM((64, 2, 8, 128), f32),))(
+        rates, key_narrow, key_wide, v0, v1, cosine, sine
     )
     core = lax.axis_index("sp_2")
     half = lax.dynamic_index_in_dim(after(out_weight, state), core, 0, keepdims=False)
@@ -287,20 +317,20 @@
     kept = [((length, 384), bf16), ((length, 512), f32)]
     turned, inside = call(
         inside_kernel,
-        [SM] + [VM] * 7,
+        [SM] + [VM] * 8,
         tuple(pltpu.HBM(*k) for k in kept),
         tuple(pltpu.VMEM(*k) for k in kept) + (pltpu.SemaphoreType.DMA((2,)),),
         (HB, HB),
-    )(rates, query_narrow, query_wide, key_narrow, key_wide, values, cosine, sine)
+    )(rates, query_narrow, query_wide, key_narrow, key_wide, v0, v1, cosine, sine)
     arrived = exchanged(state, SP)
     enter = call(scan_kernel, [SM, VM], states)(rates, arrived)
     enter = exchanged(enter, SP)
     y = call(
         finish_kernel,
-        [SM, HB, HB, VM, VM],
+        [SM, HB, HB, VM, VM, VM],
         shape(length, 512, dtype=bf16),
         (pltpu.VMEM((length, 384), bf16), pltpu.VMEM((length, 512), f32), pltpu.VMEM((64, 2, 8, 128), f32), pltpu.SemaphoreType.DMA((2,))),
-    )(rates, turned, inside, enter, out_gate)
+    )(rates, in_hbm(turned), in_hbm(inside), enter, g0, g1)
     other = []
     for s in (1, 2, 3):
         other.append(lax.ppermute(after(same[s - 1], y), "sp_2", [(0, 1), (1, 0)]))
@@ -314,20 +344,29 @@
         [SM, VM, VM, VM] + [HB] * 7,
         (own, own),
         (pltpu.VMEM((8, 256, width), bf16), pltpu.SemaphoreType.DMA((8,))),
-    )(place, y, stream, norm_gain[None], out_weight, *pieces)
-
-    def mixed(x):
-        gate_act = jnp.dot(x, full_gate, preferred_element_type=f32)
-        up_act = jnp.dot(x, full_up, preferred_element_type=f32)
-        return (jax.nn.silu(gate_act) * up_act).astype(bf16)
-
-    near = mixed(jnp.concatenate([shifted(normed, 1), shifted(normed, 3)], 0))
-    far = mixed(jnp.concatenate([normed, shifted(normed, 2)], 0))
-    near = nt(near, full_down).astype(bf16)
-    far = nt(far, full_down).astype(bf16)
-    n = length // n_tp
-    total = far[:n].astype(f32) + shifted(far[n:], 2).astype(f32)
-    total = total + shifted(near[:n], 3).astype(f32) + shifted(near[n:], 1).astype(f32)
+    )(place, y, stream, norm_gain[None], in_hbm(out_weight), *pieces)
+
+    def mixed(first, second):
+        n, _ = first.shape
+        return call(
+            mixer_kernel,
+            [VM, VM, HB],
+            (own, own),
+            (
+                pltpu.VMEM(shards.shape, bf16),
+                pltpu.VMEM((2 * n, 2 * hidden_units), f32),
+                pltpu.VMEM((2 * n, hidden_units), bf16),
+                pltpu.SemaphoreType.DMA((2 * STAGES,)),
+            ),
+        )(first, second, in_hbm(shards))
+
+    to_third, to_first = mixed(shifted(normed, 1), shifted(normed, 3))
+    arrivals = [shifted(to_third, 3), shifted(to_first, 1)]
+    total, to_second = mixed(after(normed, to_first), shifted(normed, 2))
+    arrivals.append(shifted(to_second, 2))
+    total = total.astype(f32)
+    for arrival in arrivals:
+        total = total + arrival.astype(f32)
     return (middle.astype(f32) + 0.5 * total).astype(bf16)
 
 

time: 169 us -> 164 us (0.970)
  matrix products: 26 us -> 0 us
  Pallas kernels: 15.9 us -> 31.8 us
  waiting for transfers between devices: 47.8 us -> 59 us
  local copies, waits for them, and re-layouts: 10.6 us -> 5.92 us
    dot_general x4 -> x0, matrix products: 26 us -> none  [the longest x2 15.9 us: nt(): lax.dot_general(a, b, (((1,), (1,)), ((), ())), preferred_element_type=f32)]
    all_gather x1, waiting for transfers between devices: 4.45 us -> 19.3 us  [body(): lax.all_gather(jnp.concatenate([mlp_gate, mlp_up, mlp_down.T], 1), SP, ax...]
    pallas_call x3 -> x5, Pallas kernels: 10.6 us -> 25.2 us  [the longest x2 17 us: mixed(): call(mixer_kernel, [VM, VM, HB], (own, own), (pltpu.VMEM(shards.shape, bf...]
    unnamed x38 -> x16, local copies, waits for them, and re-layouts: 9.41 us -> 0.96 us
    slice x2, local copies, waits for them, and re-layouts: 0.08 us -> 3.76 us  [the longest x1 1.94 us: body(): v0, v1 = (values[:, 0], values[:, 1])]
    ppermute x9, waiting for transfers between devices: 27.6 us -> 24.8 us  [shifted(): return lax.ppermute(x, 'tp', [(k, (k + by) % n) for k in range(n)])]
  transfers between devices with their start and end apart: 15 -> 15, of which waited for: 8 -> 6; matrix products, arithmetic and copies ran while one was open for 9% -> 4% of each run, Pallas kernels for 9% -> 19%
where the time goes in v4:
time: 164 us
  waiting for transfers between devices  59 us (36%)
  Pallas kernels  31.8 us (19%)
  blocking collectives  27.9 us (17%)
  starting transfers between devices  21.9 us (13%)
  between operations  13.6 us (8%)
  local copies, waits for them, and re-layouts  5.92 us (4%)
  other arithmetic  3.73 us (2%)
    all_to_all x1, blocking collectives, exchanged(): return lax.all_to_all(x, axis, 0, 0, tiled=True)  27.9 us
    ppermute x9, waiting for transfers between devices, shifted(): return lax.ppermute(x, 'tp', [(k, (k + by) % n) for k in range(n)])  24.8 us
    all_gather x1, waiting for transfers between devices, body(): lax.all_gather(jnp.concatenate([mlp_gate, mlp_up, mlp_down.T], 1), SP, ax...  19.3 us
    pallas_call x2, Pallas kernels, mixed(): call(mixer_kernel, [VM, VM, HB], (own, own), (pltpu.VMEM(shards.shape, bf...  17 us
    all_to_all x2, waiting for transfers between devices, exchanged(): return lax.all_to_all(x, axis, 0, 0, tiled=True)  14.8 us
    ppermute x9, starting transfers between devices, shifted(): return lax.ppermute(x, 'tp', [(k, (k + by) % n) for k in range(n)])  12.3 us
    all_to_all x2, starting transfers between devices, exchanged(): return lax.all_to_all(x, axis, 0, 0, tiled=True)  8.63 us
    pallas_call x1, Pallas kernels, body(): call(proj_kernel, [SM, VM, VM, VM] + [HB] * 7, (own, own), (pltpu.VMEM((8...  5.24 us
  transfers between devices with their start and end apart: 15, of which 6 were waited for; matrix products, arithmetic and copies ran while one was open for 4% of the time, Pallas kernels for 19%

profile of v4, /device:TPU:1, one launch (start us, length us, event | category | flops | bytes accessed | tf_op | source)
XLA Modules:
  0.0 163.8 jit_solution(14835615672129535008)
XLA Ops:
  6.5 1.7 %pad_maximum_fusion = bf16[32,4224]{1,0:T(8,128)(2,1)} fusion(bf16[32,1408]{1,0:T(8,128)(2,1)} %bitcast.16, bf16[32,1408]{1,0:T(8,128)(2,1)} %param.23, bf16[32,1408]{1,0:T(8,128)(2,1)} %param.22), kind=kLoop, calls=%fused_computation.4 | loop fusion | flops 811008 | bytes 540672 | tf_op jit(solution)/shard_map/concatenate | solution.py:302
  8.4 0.8 multiply_sine_fusion
  9.2 1.9 %fusion.1 = (bf16[384,1,256]{2,1,0:T(2,128)(2,1)S(1)}, bf16[384,1,256]{2,1,0:T(2,128)(2,1)S(1)}) fusion(bf16[384,2,256]{2,1,0:T(2,128)(2,1)} %param.18), kind=kLoop, calls=%fused_computation.15 | loop fusion | bytes 786432 | tf_op jit(solution)/shard_map/slice | solution.py:306
  11.2 1.8 %shard_map.128 = bf16[64,2,8,128]{3,2,1,0:T(8,128)(2,1)S(1)} custom-call(f32[2,2,2]{2,1,0:T(2,128)S(1)} %copy-done.5, bf16[384,128]{1,0:T(8,128)(2,1)S(1)} %copy-done.2, bf16[384,256]{1,0:T(8,128)(2,1)S(1)} %copy-done, bf16[384,256]{1,0:T(8,128)(2,1)S(1)} %get-tuple-element.38.v0, bf16[384,256]{1,0:T(8,128)(2,1)S(1)} %get-tuple-element.37.v1, ...), custom_call_target="tpu_custom_call" | custom-call | tf_op jit(solution)/shard_map/pallas_call | solution.py:309
  13.1 1.1 dynamic-slice_bitcast_fusion
  14.1 3.6 %collective-permute-start.4 = (bf16[256,2048]{1,0:T(8,128)(2,1)}, bf16[256,2048]{1,0:T(8,128)(2,1)S(1)}, u32[]{:S(2)}, u32[]{:S(2)}) collective-permute-start(bf16[256,2048]{1,0:T(8,128)(2,1)} %dynamic-slice_bitcast_fusion), channel_id=1, source_target_pairs={{0,3},{1,0},{2,1},{3,2},{4,7},{5,4},{6,5},{7,6},{8,11},{9,8},{10,9... | collective-permute-start | bytes 3145736 | tf_op jit(solution)/shard_map/ppermute | solution.py:282
  17.7 0.4 collective-permute-start.2
  18.0 0.7 collective-permute-start
  18.7 27.9 %all_to_all.15.x = bf16[64,2,8,128]{3,2,1,0:T(8,128)(2,1)S(1)} all-to-all(bf16[64,2,8,128]{3,2,1,0:T(8,128)(2,1)S(1)} %shard_map.128), channel_id=1, replica_groups=mesh['sp_0'=8,'sp_1'=4,'sp_2'=2,'tp'=4] {'sp_0','sp_1','sp_2'}, dimensions={0} | all-to-all | bytes 524288 | tf_op jit(solution)/shard_map/all_to_all | solution.py:245
  46.6 1.4 shard_map.129
  48.0 5.2 %all-to-all-start.1 = ((bf16[64,2,8,128]{3,2,1,0:T(8,128)(2,1)}), bf16[64,2,8,128]{3,2,1,0:T(8,128)(2,1)S(1)}, u32[]{:S(2)}, u32[]{:S(2)}) async-start(bf16[64,2,8,128]{3,2,1,0:T(8,128)(2,1)} %shard_map.129), calls=%async_computation.1 | async-start | bytes 524288 | tf_op jit(solution)/shard_map/all_to_all | solution.py:245
  53.2 0.9 copy-done.3
  54.2 3.0 %shard_map.127 = (bf16[384,384]{1,0:T(8,128)(2,1)}, f32[384,512]{1,0:T(8,128)}) custom-call(f32[2,2,2]{2,1,0:T(2,128)S(1)} %copy-done.5, bf16[384,128]{1,0:T(8,128)(2,1)S(1)} %copy-done.4, bf16[384,256]{1,0:T(8,128)(2,1)S(1)} %copy-done.3, bf16[384,128]{1,0:T(8,128)(2,1)S(1)} %copy-done.2, bf16[384,256]{1,0:T(8,128)(2,1)S(1)} %copy-done, ...), custom_call_target="tpu_custom_call" | custom-call | tf_op jit(solution)/shard_map/pallas_call | solution.py:318
  57.1 1.8 %fusion = (bf16[384,1,256]{2,1,0:T(2,128)(2,1)S(1)}, bf16[384,1,256]{2,1,0:T(2,128)(2,1)S(1)}) fusion(bf16[384,2,256]{2,1,0:T(2,128)(2,1)} %param.19), kind=kLoop, calls=%fused_computation.14 | loop fusion | bytes 786432 | tf_op jit(solution)/shard_map/slice | solution.py:307
  59.1 7.1 %all-to-all-done.1.enter_in = bf16[64,2,8,128]{3,2,1,0:T(8,128)(2,1)S(1)} async-done(((bf16[64,2,8,128]{3,2,1,0:T(8,128)(2,1)}), bf16[64,2,8,128]{3,2,1,0:T(8,128)(2,1)S(1)}, u32[]{:S(2)}, u32[]{:S(2)}) %all-to-all-start.1) | async-done | bytes 262176 | tf_op jit(solution)/shard_map/all_to_all | solution.py:245
  66.2 3.4 %shard_map.130 = bf16[384,512]{1,0:T(8,128)(2,1)} custom-call(f32[2,2,2]{2,1,0:T(2,128)S(1)} %copy-done.5, bf16[384,384]{1,0:T(8,128)(2,1)} %get-tuple-element.18.turned_in, f32[384,512]{1,0:T(8,128)} %get-tuple-element.19.inside_in, bf16[64,2,8,128]{3,2,1,0:T(8,128)(2,1)S(1)} %all-to-all-done.1.enter_in, bf16[384,256]{1,0:T(8,128)(2,1)S(1)} %get-tuple-element.40.g0, ...), custom_call_target="tpu_custom_call" | custom-call | tf_op jit(solution)/shard_map/pallas_call | solution.py:328
  69.7 0.4 collective-permute-start.5
  70.6 3.5 %all-to-all-start.2 = ((bf16[4,96,512]{2,1,0:T(8,128)(2,1)}), bf16[4,96,512]{2,1,0:T(8,128)(2,1)S(1)}, u32[]{:S(2)}, u32[]{:S(2)}) async-start(bf16[4,96,512]{2,1,0:T(8,128)(2,1)} %bitcast.6), calls=%async_computation.2 | async-start | bytes 786432 | tf_op jit(solution)/shard_map/all_to_all | solution.py:245
  74.1 7.7 %all-to-all-done.2.y = bf16[4,96,512]{2,1,0:T(8,128)(2,1)S(1)} async-done(((bf16[4,96,512]{2,1,0:T(8,128)(2,1)}), bf16[4,96,512]{2,1,0:T(8,128)(2,1)S(1)}, u32[]{:S(2)}, u32[]{:S(2)}) %all-to-all-start.2) | async-done | bytes 393248 | tf_op jit(solution)/shard_map/all_to_all | solution.py:245
  81.8 5.2 %shard_map.131 = (bf16[96,2048]{1,0:T(8,128)(2,1)S(1)}, bf16[96,2048]{1,0:T(8,128)(2,1)}) custom-call(s32[2]{0:T(128)S(1)} %pad_add_fusion.place, bf16[4,96,512]{2,1,0:T(8,128)(2,1)S(1)} %all-to-all-done.2.y, bf16[96,2048]{1,0:T(8,128)(2,1)S(1)} %copy-done.1, f32[1,2048]{1,0:T(1,128)S(1)} %bitcast.15, bf16[2,256,2048]{2,1,0:T(8,128)(2,1)} %own.1, ...), custom_call_target="tpu_custom_call" | custom-call | tf_op jit(solution)/shard_map/pallas_call | solution.py:342
  87.1 0.3 collective-permute-start.6
  87.4 2.4 %collective-permute-start.7 = (bf16[96,2048]{1,0:T(8,128)(2,1)}, bf16[96,2048]{1,0:T(8,128)(2,1)S(1)}, u32[]{:S(2)}, u32[]{:S(2)}) collective-permute-start(bf16[96,2048]{1,0:T(8,128)(2,1)} %get-tuple-element.27.first), channel_id=1, source_target_pairs={{0,3},{1,0},{2,1},{3,2},{4,7},{5,4},{6,5},{7,6},{8,11},{9,8},{10,9... | collective-permute-start | bytes 1179656 | tf_op jit(solution)/shard_map/ppermute | solution.py:282
  89.8 9.2 %collective-permute-done.6.first = bf16[96,2048]{1,0:T(8,128)(2,1)S(1)} collective-permute-done((bf16[96,2048]{1,0:T(8,128)(2,1)}, bf16[96,2048]{1,0:T(8,128)(2,1)S(1)}, u32[]{:S(2)}, u32[]{:S(2)}) %collective-permute-start.6) | collective-permute-done | bytes 393248 | tf_op jit(solution)/shard_map/ppermute | solution.py:282
  99.1 19.3 %all-gather.2.cloned.1.call-done.weights = bf16[2048,4224]{1,0:T(8,128)(2,1)} async-done(((bf16[32,4224]{1,0:T(8,128)(2,1)}), bf16[2048,4224]{1,0:T(8,128)(2,1)}) %all-gather.2.cloned.1.call-update) | async-done | bytes 17301520 | tf_op jit(solution)/shard_map/all_gather | solution.py:302
  118.4 8.0 %shard_map.132 = (bf16[96,2048]{1,0:T(8,128)(2,1)S(1)}, bf16[96,2048]{1,0:T(8,128)(2,1)S(1)}) custom-call(bf16[96,2048]{1,0:T(8,128)(2,1)S(1)} %collective-permute-done.6.first, bf16[96,2048]{1,0:T(8,128)(2,1)S(1)} %collective-permute-done.7.second, bf16[2048,4224]{1,0:T(8,128)(2,1)} %all-gather.2.cloned.1.call-done.weights), custom_call_target="tpu_custom_call" | custom-call | tf_op jit(solution)/shard_map/pallas_call | solution.py:351
  126.4 1.3 collective-permute-start.10
  127.7 9.0 %shard_map.133 = (bf16[96,2048]{1,0:T(8,128)(2,1)S(1)}, bf16[96,2048]{1,0:T(8,128)(2,1)S(1)}) custom-call(bf16[96,2048]{1,0:T(8,128)(2,1)} %get-tuple-element.27.first, bf16[96,2048]{1,0:T(8,128)(2,1)S(1)} %collective-permute-done.8.second, bf16[2048,4224]{1,0:T(8,128)(2,1)} %all-gather.2.cloned.1.call-done.weights), custom_call_target="tpu_custom_call" | custom-call | tf_op jit(solution)/shard_map/pallas_call | solution.py:351
  136.7 2.5 %collective-permute-start.11 = (bf16[96,2048]{1,0:T(8,128)(2,1)S(1)}, bf16[96,2048]{1,0:T(8,128)(2,1)S(1)}, u32[]{:S(2)}, u32[]{:S(2)}) collective-permute-start(bf16[96,2048]{1,0:T(8,128)(2,1)S(1)} %get-tuple-element.30), channel_id=1, source_target_pairs={{0,2},{1,3},{2,0},{3,1},{4,6},{5,7},{6,4},{7,5},{8,10},{9,11},{10,... | collective-permute-start | bytes 1179656 | tf_op jit(solution)/shard_map/ppermute | solution.py:282
  139.2 1.1 collective-permute-start.9
  140.3 8.0 %collective-permute-done.11 = bf16[96,2048]{1,0:T(8,128)(2,1)S(1)} collective-permute-done((bf16[96,2048]{1,0:T(8,128)(2,1)S(1)}, bf16[96,2048]{1,0:T(8,128)(2,1)S(1)}, u32[]{:S(2)}, u32[]{:S(2)}) %collective-permute-start.11) | collective-permute-done | bytes 393248 | tf_op jit(solution)/shard_map/ppermute | solution.py:282
  148.4 7.5 %collective-permute-done.9 = bf16[96,2048]{1,0:T(8,128)(2,1)S(1)} collective-permute-done((bf16[96,2048]{1,0:T(8,128)(2,1)S(1)}, bf16[96,2048]{1,0:T(8,128)(2,1)S(1)}, u32[]{:S(2)}, u32[]{:S(2)}) %collective-permute-start.9) | collective-permute-done | bytes 393248 | tf_op jit(solution)/shard_map/ppermute | solution.py:282
  155.9 1.1 add_convert_fusion
  (36 shorter events, 0.9 us)
Async XLA Ops:
  6.5 4.7 %copy-start.2 = (bf16[384,128]{1,0:T(8,128)(2,1)S(1)}, bf16[384,128]{1,0:T(8,128)(2,1)}, u32[]{:S(2)}) copy-start(bf16[384,128]{1,0:T(8,128)(2,1)} %kn.3) | copy-start | bytes 294916
  6.5 4.7 %copy-start = (bf16[384,256]{1,0:T(8,128)(2,1)S(1)}, bf16[384,256]{1,0:T(8,128)(2,1)}, u32[]{:S(2)}) copy-start(bf16[384,256]{1,0:T(8,128)(2,1)} %kw.3) | copy-start | bytes 589828
  6.5 4.7 %copy-start.5 = (f32[2,2,2]{2,1,0:T(2,128)S(1)}, f32[2,2,2]{2,1,0:T(2,128)}, u32[]{:S(2)}) copy-start(f32[2,2,2]{2,1,0:T(2,128)} %ld.7) | copy-start | bytes 100
  6.5 111.9 %all-gather.2.cloned.1.call-start = ((), (), s32[]{:S(2)}) async-start(), calls=%async_computation.3 | async-start | bytes 17571840 | tf_op jit(solution)/shard_map/all_gather | solution.py:302
  9.2 3.9 %copy-start.7 = (bf16[2,256,2048]{2,1,0:T(8,128)(2,1)S(1)}, bf16[2,256,2048]{2,1,0:T(8,128)(2,1)}, u32[]{:S(2)}) copy-start(bf16[2,256,2048]{2,1,0:T(8,128)(2,1)} %own.1) | copy-start | bytes 6291460
  13.0 40.2 %copy-start.4 = (bf16[384,128]{1,0:T(8,128)(2,1)S(1)}, bf16[384,128]{1,0:T(8,128)(2,1)}, u32[]{:S(2)}) copy-start(bf16[384,128]{1,0:T(8,128)(2,1)} %qn.1) | copy-start | bytes 294916
  14.1 55.5 %collective-permute-start.4 = (bf16[256,2048]{1,0:T(8,128)(2,1)}, bf16[256,2048]{1,0:T(8,128)(2,1)S(1)}, u32[]{:S(2)}, u32[]{:S(2)}) collective-permute-start(bf16[256,2048]{1,0:T(8,128)(2,1)} %dynamic-slice_bitcast_fusion), channel_id=1, source_target_pairs={{0,3},{1,0},{2,1},{3,2},{4,7},{5,4},{6,5},{7,6},{8,11},{9,8},{10,9... | collective-permute-start | bytes 3145736 | tf_op jit(solution)/shard_map/ppermute | solution.py:282
  17.7 52.4 %collective-permute-start.2 = (bf16[256,2048]{1,0:T(8,128)(2,1)}, bf16[256,2048]{1,0:T(8,128)(2,1)S(1)}, u32[]{:S(2)}, u32[]{:S(2)}) collective-permute-start(bf16[256,2048]{1,0:T(8,128)(2,1)} %dynamic-slice_bitcast_fusion), channel_id=1, source_target_pairs={{0,2},{1,3},{2,0},{3,1},{4,6},{5,7},{6,4},{7,5},{8,10},{9,11},{10,... | collective-permute-start | bytes 3145736 | tf_op jit(solution)/shard_map/ppermute | solution.py:282
  18.0 52.2 %collective-permute-start = (bf16[256,2048]{1,0:T(8,128)(2,1)}, bf16[256,2048]{1,0:T(8,128)(2,1)}, u32[]{:S(2)}, u32[]{:S(2)}) collective-permute-start(bf16[256,2048]{1,0:T(8,128)(2,1)} %dynamic-slice_bitcast_fusion), channel_id=1, source_target_pairs={{0,1},{1,2},{2,3},{3,0},{4,5},{5,6},{6,7},{7,4},{8,9},{9,10},{10,1... | collective-permute-start | bytes 3145736 | tf_op jit(solution)/shard_map/ppermute | solution.py:282
  48.0 18.2 %all-to-all-start.1 = ((bf16[64,2,8,128]{3,2,1,0:T(8,128)(2,1)}), bf16[64,2,8,128]{3,2,1,0:T(8,128)(2,1)S(1)}, u32[]{:S(2)}, u32[]{:S(2)}) async-start(bf16[64,2,8,128]{3,2,1,0:T(8,128)(2,1)} %shard_map.129), calls=%async_computation.1 | async-start | bytes 524288 | tf_op jit(solution)/shard_map/all_to_all | solution.py:245
  53.2 0.9 copy-start.3
  59.0 22.8 %copy-start.1 = (bf16[96,2048]{1,0:T(8,128)(2,1)S(1)}, bf16[96,2048]{1,0:T(8,128)(2,1)}, u32[]{:S(2)}) copy-start(bf16[96,2048]{1,0:T(8,128)(2,1)} %stream.1) | copy-start | bytes 1179652
  59.0 22.8 %copy-start.6 = (f32[2048]{0:T(1024)S(1)}, f32[2048]{0:T(1024)}, u32[]{:S(2)}) copy-start(f32[2048]{0:T(1024)} %param.21) | copy-start | bytes 24580
  69.7 12.1 %collective-permute-start.5 = (bf16[256,2048]{1,0:T(8,128)(2,1)S(1)}, bf16[256,2048]{1,0:T(8,128)(2,1)}, u32[]{:S(2)}, u32[]{:S(2)}) collective-permute-start(bf16[256,2048]{1,0:T(8,128)(2,1)S(1)} %collective-permute-done.4.refs_4_), channel_id=1, source_target_pairs={{0,4},{4,0},{1,5},{5,1},{2,6},{6,2},{3,7},{7,3},{8,12},{12,8},{9,1... | collective-permute-start | bytes 3145736 | tf_op jit(solution)/shard_map/ppermute | solution.py:336
  70.1 11.7 %collective-permute-start.3 = (bf16[256,2048]{1,0:T(8,128)(2,1)S(1)}, bf16[256,2048]{1,0:T(8,128)(2,1)}, u32[]{:S(2)}, u32[]{:S(2)}) collective-permute-start(bf16[256,2048]{1,0:T(8,128)(2,1)S(1)} %collective-permute-done.2.refs_2_), channel_id=1, source_target_pairs={{0,4},{4,0},{1,5},{5,1},{2,6},{6,2},{3,7},{7,3},{8,12},{12,8},{9,1... | collective-permute-start | bytes 3145736 | tf_op jit(solution)/shard_map/ppermute | solution.py:336
  70.3 11.5 %collective-permute-start.1 = (bf16[256,2048]{1,0:T(8,128)(2,1)}, bf16[256,2048]{1,0:T(8,128)(2,1)}, u32[]{:S(2)}, u32[]{:S(2)}) collective-permute-start(bf16[256,2048]{1,0:T(8,128)(2,1)} %collective-permute-done.refs_0_), channel_id=1, source_target_pairs={{0,4},{4,0},{1,5},{5,1},{2,6},{6,2},{3,7},{7,3},{8,12},{12,8},{9,1... | collective-permute-start | bytes 3145736 | tf_op jit(solution)/shard_map/ppermute | solution.py:336
  70.6 11.2 %all-to-all-start.2 = ((bf16[4,96,512]{2,1,0:T(8,128)(2,1)}), bf16[4,96,512]{2,1,0:T(8,128)(2,1)S(1)}, u32[]{:S(2)}, u32[]{:S(2)}) async-start(bf16[4,96,512]{2,1,0:T(8,128)(2,1)} %bitcast.6), calls=%async_computation.2 | async-start | bytes 786432 | tf_op jit(solution)/shard_map/all_to_all | solution.py:245
  87.1 12.0 %collective-permute-start.6 = (bf16[96,2048]{1,0:T(8,128)(2,1)}, bf16[96,2048]{1,0:T(8,128)(2,1)S(1)}, u32[]{:S(2)}, u32[]{:S(2)}) collective-permute-start(bf16[96,2048]{1,0:T(8,128)(2,1)} %get-tuple-element.27.first), channel_id=1, source_target_pairs={{0,1},{1,2},{2,3},{3,0},{4,5},{5,6},{6,7},{7,4},{8,9},{9,10},{10,1... | collective-permute-start | bytes 1179656 | tf_op jit(solution)/shard_map/ppermute | solution.py:282
  87.4 11.7 %collective-permute-start.7 = (bf16[96,2048]{1,0:T(8,128)(2,1)}, bf16[96,2048]{1,0:T(8,128)(2,1)S(1)}, u32[]{:S(2)}, u32[]{:S(2)}) collective-permute-start(bf16[96,2048]{1,0:T(8,128)(2,1)} %get-tuple-element.27.first), channel_id=1, source_target_pairs={{0,3},{1,0},{2,1},{3,2},{4,7},{5,4},{6,5},{7,6},{8,11},{9,8},{10,9... | collective-permute-start | bytes 1179656 | tf_op jit(solution)/shard_map/ppermute | solution.py:282
  89.8 37.8 %collective-permute-start.8 = (bf16[96,2048]{1,0:T(8,128)(2,1)}, bf16[96,2048]{1,0:T(8,128)(2,1)S(1)}, u32[]{:S(2)}, u32[]{:S(2)}) collective-permute-start(bf16[96,2048]{1,0:T(8,128)(2,1)} %get-tuple-element.27.first), channel_id=1, source_target_pairs={{0,2},{1,3},{2,0},{3,1},{4,6},{5,7},{6,4},{7,5},{8,10},{9,11},{10,... | collective-permute-start | bytes 1179656 | tf_op jit(solution)/shard_map/ppermute | solution.py:282
  126.4 22.0 %collective-permute-start.10 = (bf16[96,2048]{1,0:T(8,128)(2,1)S(1)}, bf16[96,2048]{1,0:T(8,128)(2,1)S(1)}, u32[]{:S(2)}, u32[]{:S(2)}) collective-permute-start(bf16[96,2048]{1,0:T(8,128)(2,1)S(1)} %get-tuple-element.26), channel_id=1, source_target_pairs={{0,1},{1,2},{2,3},{3,0},{4,5},{5,6},{6,7},{7,4},{8,9},{9,10},{10,1... | collective-permute-start | bytes 1179656 | tf_op jit(solution)/shard_map/ppermute | solution.py:282
  136.7 11.7 %collective-permute-start.11 = (bf16[96,2048]{1,0:T(8,128)(2,1)S(1)}, bf16[96,2048]{1,0:T(8,128)(2,1)S(1)}, u32[]{:S(2)}, u32[]{:S(2)}) collective-permute-start(bf16[96,2048]{1,0:T(8,128)(2,1)S(1)} %get-tuple-element.30), channel_id=1, source_target_pairs={{0,2},{1,3},{2,0},{3,1},{4,6},{5,7},{6,4},{7,5},{8,10},{9,11},{10,... | collective-permute-start | bytes 1179656 | tf_op jit(solution)/shard_map/ppermute | solution.py:282
  139.2 16.7 %collective-permute-start.9 = (bf16[96,2048]{1,0:T(8,128)(2,1)S(1)}, bf16[96,2048]{1,0:T(8,128)(2,1)S(1)}, u32[]{:S(2)}, u32[]{:S(2)}) collective-permute-start(bf16[96,2048]{1,0:T(8,128)(2,1)S(1)} %get-tuple-element.29), channel_id=1, source_target_pairs={{0,3},{1,0},{2,1},{3,2},{4,7},{5,4},{6,5},{7,6},{8,11},{9,8},{10,9... | collective-permute-start | bytes 1179656 | tf_op jit(solution)/shard_map/ppermute | solution.py:282
Sparse Core Ops, SparseCore 0:
  10.1 108.2 all-gather.1

commit v5 on v4

--- a/solution.py
+++ b/solution.py
@@ -226,14 +226,14 @@
 HB = pl.BlockSpec(memory_space=pltpu.HBM)
 
 
-def call(kernel, in_specs, outs, scratch=(), out_specs=None):
+def call(kernel, in_specs, outs, scratch=(), out_specs=None, room=40):
     return pl.pallas_call(
         kernel,
         in_specs=in_specs,
         out_specs=out_specs or jax.tree.map(lambda _: VM, outs),
         out_shape=outs,
         scratch_shapes=scratch,
-        compiler_params=pltpu.CompilerParams(vmem_limit_bytes=40 * 2**20),
+        compiler_params=pltpu.CompilerParams(vmem_limit_bytes=room * 2**20),
     )
 
 
@@ -245,28 +245,45 @@
     return lax.all_to_all(x, axis, 0, 0, tiled=True)
 
 
-def mixer_kernel(first, second, weights, out_a, out_b, held, act, hidden, sems):
-    n, width = first.shape
-    units = hidden.shape[1]
+def weight_parts(width, units):
     step = width // STAGES
     spans = [pl.ds(k * step, step) for k in range(STAGES)]
-    parts = [(span, pl.ds(at, size)) for at, size in ((0, 2 * units), (2 * units, units)) for span in spans]
-    copies = [pltpu.make_async_copy(weights.at[p], held.at[p], sems.at[k]) for k, p in enumerate(parts)]
-    for copy in copies:
-        copy.start()
+    return spans, [(span, pl.ds(at, size)) for at, size in ((0, 2 * units), (2 * units, units)) for span in spans]
+
+
+def mixed_into(pieces, held, outs, act, hidden, ready):
+    n = pieces[0].shape[0]
+    units = hidden.shape[1]
+    spans, _ = weight_parts(held.shape[0], units)
     for k, span in enumerate(spans):
-        x = jnp.concatenate([first[:, span], second[:, span]], 0)
-        copies[k].wait()
+        x = jnp.concatenate([p[:, span] for p in pieces], 0)
+        ready(k)
         part = nn(x, held[span, : 2 * units])
         act[...] = part if k == 0 else act[...] + part
     gate = act[:, :units]
     hidden[...] = (gate * jax.nn.sigmoid(gate) * act[:, units:]).astype(bf16)
     h = hidden[...]
     for k, span in enumerate(spans):
-        copies[STAGES + k].wait()
+        ready(STAGES + k)
         part = nt(h, held[span, 2 * units :]).astype(bf16)
-        out_a[:, span] = part[:n]
-        out_b[:, span] = part[n:]
+        for j, out in enumerate(outs):
+            out[:, span] = part[j * n : (j + 1) * n]
+
+
+def first_mixer(piece, weights, out, held, act, hidden, sems):
+    _, parts = weight_parts(held.shape[0], hidden.shape[1])
+    copies = [pltpu.make_async_copy(weights.at[p], held.at[p], sems.at[k]) for k, p in enumerate(parts)]
+    for copy in copies:
+        copy.start()
+    mixed_into([piece], held, [out], act, hidden, lambda k: copies[k].wait())
+
+
+def near_mixer(first, second, held, out_a, out_b, act, hidden):
+    mixed_into([first, second], held, [out_a, out_b], act, hidden, lambda k: None)
+
+
+def own_mixer(piece, held, out, act, hidden):
+    mixed_into([piece], held, [out], act, hidden, lambda k: None)
 
 
 def after(x, token):
@@ -275,6 +292,10 @@
 
 def in_hbm(x):
     return pltpu.with_memory_space_constraint(x, pltpu.HBM)
+
+
+def in_vmem(x):
+    return pltpu.with_memory_space_constraint(x, pltpu.VMEM)
 
 
 def shifted(x, by):
@@ -301,7 +322,8 @@
     hidden_units = mlp_gate.shape[1]
     shards = lax.all_gather(jnp.concatenate([mlp_gate, mlp_up, mlp_down.T], 1), SP, axis=0, tiled=True)
 
-    rates = log_decay
+    rates = in_hbm(log_decay)
+    query_narrow, query_wide, key_narrow, key_wide = map(in_hbm, (query_narrow, query_wide, key_narrow, key_wide))
     cosine, sine = angle_tables(length, lax.axis_index(SP) * length)
     v0, v1 = values[:, 0], values[:, 1]
     g0, g1 = out_gate[:, 0], out_gate[:, 1]
@@ -344,26 +366,25 @@
         [SM, VM, VM, VM] + [HB] * 7,
         (own, own),
         (pltpu.VMEM((8, 256, width), bf16), pltpu.SemaphoreType.DMA((8,))),
-    )(place, y, stream, norm_gain[None], in_hbm(out_weight), *pieces)
-
-    def mixed(first, second):
-        n, _ = first.shape
-        return call(
-            mixer_kernel,
-            [VM, VM, HB],
-            (own, own),
-            (
-                pltpu.VMEM(shards.shape, bf16),
-                pltpu.VMEM((2 * n, 2 * hidden_units), f32),
-                pltpu.VMEM((2 * n, hidden_units), bf16),
-                pltpu.SemaphoreType.DMA((2 * STAGES,)),
-            ),
-        )(first, second, in_hbm(shards))
-
-    to_third, to_first = mixed(shifted(normed, 1), shifted(normed, 3))
-    arrivals = [shifted(to_third, 3), shifted(to_first, 1)]
-    total, to_second = mixed(after(normed, to_first), shifted(normed, 2))
-    arrivals.append(shifted(to_second, 2))
+    )(place, y, in_hbm(stream), in_hbm(norm_gain[None]), in_hbm(out_weight), *pieces)
+
+    def room(pieces):
+        m = pieces * own.shape[0]
+        return (pltpu.VMEM((m, 2 * hidden_units), f32), pltpu.VMEM((m, hidden_units), bf16))
+
+    around = [None] + [shifted(normed, s) for s in (1, 2, 3)]
+    to_second, held = call(
+        first_mixer,
+        [VM, HB],
+        (own, pltpu.VMEM(shards.shape, bf16)),
+        room(1) + (pltpu.SemaphoreType.DMA((2 * STAGES,)),),
+        room=12,
+    )(around[2], in_hbm(shards))
+    arrivals = [shifted(to_second, 2)]
+    to_third, to_first = call(near_mixer, [VM] * 3, (own, own), room(2), room=12)(around[1], around[3], in_vmem(held))
+    arrivals.append(shifted(to_third, 3))
+    arrivals.append(shifted(to_first, 1))
+    total = call(own_mixer, [VM] * 2, own, room(1), room=12)(after(normed, to_first), in_vmem(held))
     total = total.astype(f32)
     for arrival in arrivals:
         total = total + arrival.astype(f32)

time: 164 us -> 155 us (0.945)
  waiting for transfers between devices: 59 us -> 50.2 us
    ppermute x9, waiting for transfers between devices: 24.8 us -> 16.1 us  [shifted(): return lax.ppermute(x, 'tp', [(k, (k + by) % n) for k in range(n)])]
    pallas_call x2 -> x3, Pallas kernels: 17 us -> 15.8 us  [the longest x1 7.45 us: body(): call(first_mixer, [VM, HB], (own, pltpu.VMEM(shards.shape, bf16)), room(1...]
  transfers between devices with their start and end apart: 15 -> 15, of which waited for: 6 -> 6; matrix products, arithmetic and copies ran while one was open for 4% -> 5% of each run, Pallas kernels for 19% -> 20%
where the time goes in v5:
time: 155 us; the launch traced here: 154 us
  waiting for transfers between devices  50.2 us (32%)
  Pallas kernels  31.4 us (20%)
  blocking collectives  27.7 us (18%)
  starting transfers between devices  21.9 us (14%)
  between operations  13.5 us (9%)
  local copies, waits for them, and re-layouts  6.14 us (4%)
  other arithmetic  3.69 us (2%)
    all_to_all x1, blocking collectives, exchanged(): return lax.all_to_all(x, axis, 0, 0, tiled=True)  27.7 us
    all_gather x1, waiting for transfers between devices, body(): lax.all_gather(jnp.concatenate([mlp_gate, mlp_up, mlp_down.T], 1), SP, ax...  18.7 us
    ppermute x9, waiting for transfers between devices, shifted(): return lax.ppermute(x, 'tp', [(k, (k + by) % n) for k in range(n)])  16.1 us
    all_to_all x2, waiting for transfers between devices, exchanged(): return lax.all_to_all(x, axis, 0, 0, tiled=True)  15.4 us
    ppermute x9, starting transfers between devices, shifted(): return lax.ppermute(x, 'tp', [(k, (k + by) % n) for k in range(n)])  11.9 us
    all_to_all x2, starting transfers between devices, exchanged(): return lax.all_to_all(x, axis, 0, 0, tiled=True)  8.88 us
    pallas_call x1, Pallas kernels, body(): call(first_mixer, [VM, HB], (own, pltpu.VMEM(shards.shape, bf16)), room(1...  7.45 us
    pallas_call x1, Pallas kernels, body(): call(near_mixer, [VM] * 3, (own, own), room(2), room=12)  4.66 us
  transfers between devices with their start and end apart: 15, of which 6 were waited for; matrix products, arithmetic and copies ran while one was open for 5% of the time, Pallas kernels for 20%

profile of v5, /device:TPU:1, one launch (start us, length us, event | category | flops | bytes accessed | tf_op | source)
XLA Modules:
  0.0 154.5 jit_solution(5908904959687000824)
XLA Ops:
  6.5 1.7 %pad_maximum_fusion = bf16[32,4224]{1,0:T(8,128)(2,1)} fusion(bf16[32,1408]{1,0:T(8,128)(2,1)} %bitcast.15, bf16[32,1408]{1,0:T(8,128)(2,1)} %param.23, bf16[32,1408]{1,0:T(8,128)(2,1)} %param.22), kind=kLoop, calls=%fused_computation.4 | loop fusion | flops 811008 | bytes 540672 | tf_op jit(solution)/shard_map/concatenate | solution.py:323
  8.4 0.8 multiply_sine_fusion
  9.1 1.9 %fusion.1 = (bf16[384,1,256]{2,1,0:T(2,128)(2,1)S(1)}, bf16[384,1,256]{2,1,0:T(2,128)(2,1)S(1)}) fusion(bf16[384,2,256]{2,1,0:T(2,128)(2,1)} %param.18), kind=kLoop, calls=%fused_computation.15 | loop fusion | bytes 786432 | tf_op jit(solution)/shard_map/slice | solution.py:328
  11.1 2.2 %shard_map.128 = bf16[64,2,8,128]{3,2,1,0:T(8,128)(2,1)S(1)} custom-call(f32[2,2,2]{2,1,0:T(2,128)} %ld.7, bf16[384,128]{1,0:T(8,128)(2,1)} %kn.3, bf16[384,256]{1,0:T(8,128)(2,1)} %kw.3, bf16[384,256]{1,0:T(8,128)(2,1)S(1)} %get-tuple-element.38.v0, bf16[384,256]{1,0:T(8,128)(2,1)S(1)} %get-tuple-element.37.v1, f32[384,128]{1,0:T(8,128)S(1)} %get-tuple-element.36.cosine, ...), custom_call_target="tpu_custom_call" | custom-call | tf_op jit(solution)/shard_map/pallas_call | solution.py:331
  13.3 2.3 %dynamic-slice_bitcast_fusion = bf16[256,2048]{1,0:T(8,128)(2,1)} fusion(bf16[2,256,2048]{2,1,0:T(8,128)(2,1)} %own.1, s32[]{:T(128)S(6)} %select_n.4), kind=kLoop, calls=%fused_computation | loop fusion | bytes 2097156 | tf_op jit(solution)/shard_map/jit(dynamic_index_in_dim)/squeeze | solution.py:335
  15.6 3.6 %collective-permute-start.4 = (bf16[256,2048]{1,0:T(8,128)(2,1)}, bf16[256,2048]{1,0:T(8,128)(2,1)S(1)}, u32[]{:S(2)}, u32[]{:S(2)}) collective-permute-start(bf16[256,2048]{1,0:T(8,128)(2,1)} %dynamic-slice_bitcast_fusion), channel_id=1, source_target_pairs={{0,3},{1,0},{2,1},{3,2},{4,7},{5,4},{6,5},{7,6},{8,11},{9,8},{10,9... | collective-permute-start | bytes 3145736 | tf_op jit(solution)/shard_map/ppermute | solution.py:303
  19.2 0.3 collective-permute-start.2
  19.5 0.7 collective-permute-start
  20.2 27.7 %all_to_all.15.x = bf16[64,2,8,128]{3,2,1,0:T(8,128)(2,1)S(1)} all-to-all(bf16[64,2,8,128]{3,2,1,0:T(8,128)(2,1)S(1)} %shard_map.128), channel_id=1, replica_groups=mesh['sp_0'=8,'sp_1'=4,'sp_2'=2,'tp'=4] {'sp_0','sp_1','sp_2'}, dimensions={0} | all-to-all | bytes 524288 | tf_op jit(solution)/shard_map/all_to_all | solution.py:245
  47.9 1.5 shard_map.129
  49.4 5.4 %all-to-all-start.1 = ((bf16[64,2,8,128]{3,2,1,0:T(8,128)(2,1)}), bf16[64,2,8,128]{3,2,1,0:T(8,128)(2,1)S(1)}, u32[]{:S(2)}, u32[]{:S(2)}) async-start(bf16[64,2,8,128]{3,2,1,0:T(8,128)(2,1)} %shard_map.129), calls=%async_computation.1 | async-start | bytes 524288 | tf_op jit(solution)/shard_map/all_to_all | solution.py:245
  54.8 3.6 %shard_map.127 = (bf16[384,384]{1,0:T(8,128)(2,1)}, f32[384,512]{1,0:T(8,128)}) custom-call(f32[2,2,2]{2,1,0:T(2,128)} %ld.7, bf16[384,128]{1,0:T(8,128)(2,1)} %qn.1, bf16[384,256]{1,0:T(8,128)(2,1)} %qw.1, bf16[384,128]{1,0:T(8,128)(2,1)} %kn.3, bf16[384,256]{1,0:T(8,128)(2,1)} %kw.3, bf16[384,256]{1,0:T(8,128)(2,1)S(1)} %get-tuple-element.38.v0, ...), custom_call_target="tpu_custom_call" | custom-call | tf_op jit(solution)/shard_map/pallas_call | solution.py:340
  58.4 1.8 %fusion = (bf16[384,1,256]{2,1,0:T(2,128)(2,1)S(1)}, bf16[384,1,256]{2,1,0:T(2,128)(2,1)S(1)}) fusion(bf16[384,2,256]{2,1,0:T(2,128)(2,1)} %param.19), kind=kLoop, calls=%fused_computation.14 | loop fusion | bytes 786432 | tf_op jit(solution)/shard_map/slice | solution.py:329
  60.3 7.6 %all-to-all-done.1.enter_in = bf16[64,2,8,128]{3,2,1,0:T(8,128)(2,1)S(1)} async-done(((bf16[64,2,8,128]{3,2,1,0:T(8,128)(2,1)}), bf16[64,2,8,128]{3,2,1,0:T(8,128)(2,1)S(1)}, u32[]{:S(2)}, u32[]{:S(2)}) %all-to-all-start.1) | async-done | bytes 262176 | tf_op jit(solution)/shard_map/all_to_all | solution.py:245
  67.9 3.7 %shard_map.130 = bf16[384,512]{1,0:T(8,128)(2,1)} custom-call(f32[2,2,2]{2,1,0:T(2,128)} %ld.7, bf16[384,384]{1,0:T(8,128)(2,1)} %get-tuple-element.18.turned_in, f32[384,512]{1,0:T(8,128)} %get-tuple-element.19.inside_in, bf16[64,2,8,128]{3,2,1,0:T(8,128)(2,1)S(1)} %all-to-all-done.1.enter_in, bf16[384,256]{1,0:T(8,128)(2,1)S(1)} %get-tuple-element.40.g0, ...), custom_call_target="tpu_custom_call" | custom-call | tf_op jit(solution)/shard_map/pallas_call | solution.py:350
  71.6 0.6 collective-permute-start.5
  72.3 0.4 collective-permute-start.1
  72.7 3.5 %all-to-all-start.2 = ((bf16[4,96,512]{2,1,0:T(8,128)(2,1)}), bf16[4,96,512]{2,1,0:T(8,128)(2,1)S(1)}, u32[]{:S(2)}, u32[]{:S(2)}) async-start(bf16[4,96,512]{2,1,0:T(8,128)(2,1)} %bitcast.6), calls=%async_computation.2 | async-start | bytes 786432 | tf_op jit(solution)/shard_map/all_to_all | solution.py:245
  76.2 7.8 %all-to-all-done.2.y = bf16[4,96,512]{2,1,0:T(8,128)(2,1)S(1)} async-done(((bf16[4,96,512]{2,1,0:T(8,128)(2,1)}), bf16[4,96,512]{2,1,0:T(8,128)(2,1)S(1)}, u32[]{:S(2)}, u32[]{:S(2)}) %all-to-all-start.2) | async-done | bytes 393248 | tf_op jit(solution)/shard_map/all_to_all | solution.py:245
  84.0 4.6 %shard_map.131 = (bf16[96,2048]{1,0:T(8,128)(2,1)S(1)}, bf16[96,2048]{1,0:T(8,128)(2,1)S(1)}) custom-call(s32[2]{0:T(128)S(1)} %pad_add_fusion.place, bf16[4,96,512]{2,1,0:T(8,128)(2,1)S(1)} %all-to-all-done.2.y, bf16[96,2048]{1,0:T(8,128)(2,1)} %stream.1, f32[1,2048]{1,0:T(1,128)} %bitcast.16, bf16[2,256,2048]{2,1,0:T(8,128)(2,1)} %own.1, ...), custom_call_target="tpu_custom_call" | custom-call | tf_op jit(solution)/shard_map/pallas_call | solution.py:364
  88.7 0.9 collective-permute-start.8
  89.5 2.1 %collective-permute-start.7 = (bf16[96,2048]{1,0:T(8,128)(2,1)S(1)}, bf16[96,2048]{1,0:T(8,128)(2,1)S(1)}, u32[]{:S(2)}, u32[]{:S(2)}) collective-permute-start(bf16[96,2048]{1,0:T(8,128)(2,1)S(1)} %get-tuple-element.28.piece), channel_id=1, source_target_pairs={{0,3},{1,0},{2,1},{3,2},{4,7},{5,4},{6,5},{7,6},{8,11},{9,8},{10,9... | collective-permute-start | bytes 1179656 | tf_op jit(solution)/shard_map/ppermute | solution.py:303
  91.6 8.2 %collective-permute-done.8.piece = bf16[96,2048]{1,0:T(8,128)(2,1)S(1)} collective-permute-done((bf16[96,2048]{1,0:T(8,128)(2,1)S(1)}, bf16[96,2048]{1,0:T(8,128)(2,1)S(1)}, u32[]{:S(2)}, u32[]{:S(2)}) %collective-permute-start.8) | collective-permute-done | bytes 393248 | tf_op jit(solution)/shard_map/ppermute | solution.py:303
  99.9 18.7 %all-gather.2.cloned.1.call-done.weights = bf16[2048,4224]{1,0:T(8,128)(2,1)} async-done(((bf16[32,4224]{1,0:T(8,128)(2,1)}), bf16[2048,4224]{1,0:T(8,128)(2,1)}) %all-gather.2.cloned.1.call-update) | async-done | bytes 17301520 | tf_op jit(solution)/shard_map/all_gather | solution.py:323
  118.5 7.5 %shard_map.132 = (bf16[96,2048]{1,0:T(8,128)(2,1)S(1)}, bf16[2048,4224]{1,0:T(8,128)(2,1)S(1)}) custom-call(bf16[96,2048]{1,0:T(8,128)(2,1)S(1)} %collective-permute-done.8.piece, bf16[2048,4224]{1,0:T(8,128)(2,1)} %all-gather.2.cloned.1.call-done.weights), custom_call_target="tpu_custom_call" | custom-call | tf_op jit(solution)/shard_map/pallas_call | solution.py:376
  126.0 2.8 %collective-permute-start.9 = (bf16[96,2048]{1,0:T(8,128)(2,1)S(1)}, bf16[96,2048]{1,0:T(8,128)(2,1)S(1)}, u32[]{:S(2)}, u32[]{:S(2)}) collective-permute-start(bf16[96,2048]{1,0:T(8,128)(2,1)S(1)} %get-tuple-element.29), channel_id=1, source_target_pairs={{0,2},{1,3},{2,0},{3,1},{4,6},{5,7},{6,4},{7,5},{8,10},{9,11},{10,... | collective-permute-start | bytes 1179656 | tf_op jit(solution)/shard_map/ppermute | solution.py:303
  128.8 4.7 %shard_map.133 = (bf16[96,2048]{1,0:T(8,128)(2,1)S(1)}, bf16[96,2048]{1,0:T(8,128)(2,1)S(1)}) custom-call(bf16[96,2048]{1,0:T(8,128)(2,1)S(1)} %collective-permute-done.6.first, bf16[96,2048]{1,0:T(8,128)(2,1)S(1)} %collective-permute-done.7.second, bf16[2048,4224]{1,0:T(8,128)(2,1)S(1)} %get-tuple-element.26.held), custom_call_target="tpu_custom_call" | custom-call | tf_op jit(solution)/shard_map/pallas_call | solution.py:384
  133.5 0.9 collective-permute-start.10
  134.4 0.6 collective-permute-start.11
  135.0 3.7 %shard_map.134 = bf16[96,2048]{1,0:T(8,128)(2,1)S(1)} custom-call(bf16[96,2048]{1,0:T(8,128)(2,1)S(1)} %get-tuple-element.28.piece, bf16[2048,4224]{1,0:T(8,128)(2,1)S(1)} %get-tuple-element.26.held), custom_call_target="tpu_custom_call" | custom-call | tf_op jit(solution)/shard_map/pallas_call | solution.py:387
  138.7 7.8 %collective-permute-done.10 = bf16[96,2048]{1,0:T(8,128)(2,1)S(1)} collective-permute-done((bf16[96,2048]{1,0:T(8,128)(2,1)S(1)}, bf16[96,2048]{1,0:T(8,128)(2,1)S(1)}, u32[]{:S(2)}, u32[]{:S(2)}) %collective-permute-start.10) | collective-permute-done | bytes 393248 | tf_op jit(solution)/shard_map/ppermute | solution.py:303
  146.6 1.1 add_convert_fusion
  (21 shorter events, 0.5 us)
Async XLA Ops:
  6.5 112.0 %all-gather.2.cloned.1.call-start = ((), (), s32[]{:S(2)}) async-start(), calls=%async_computation.3 | async-start | bytes 17571840 | tf_op jit(solution)/shard_map/all_gather | solution.py:323
  15.6 56.0 %collective-permute-start.4 = (bf16[256,2048]{1,0:T(8,128)(2,1)}, bf16[256,2048]{1,0:T(8,128)(2,1)S(1)}, u32[]{:S(2)}, u32[]{:S(2)}) collective-permute-start(bf16[256,2048]{1,0:T(8,128)(2,1)} %dynamic-slice_bitcast_fusion), channel_id=1, source_target_pairs={{0,3},{1,0},{2,1},{3,2},{4,7},{5,4},{6,5},{7,6},{8,11},{9,8},{10,9... | collective-permute-start | bytes 3145736 | tf_op jit(solution)/shard_map/ppermute | solution.py:303
  19.2 53.0 %collective-permute-start.2 = (bf16[256,2048]{1,0:T(8,128)(2,1)}, bf16[256,2048]{1,0:T(8,128)(2,1)S(1)}, u32[]{:S(2)}, u32[]{:S(2)}) collective-permute-start(bf16[256,2048]{1,0:T(8,128)(2,1)} %dynamic-slice_bitcast_fusion), channel_id=1, source_target_pairs={{0,2},{1,3},{2,0},{3,1},{4,6},{5,7},{6,4},{7,5},{8,10},{9,11},{10,... | collective-permute-start | bytes 3145736 | tf_op jit(solution)/shard_map/ppermute | solution.py:303
  19.5 52.8 %collective-permute-start = (bf16[256,2048]{1,0:T(8,128)(2,1)}, bf16[256,2048]{1,0:T(8,128)(2,1)}, u32[]{:S(2)}, u32[]{:S(2)}) collective-permute-start(bf16[256,2048]{1,0:T(8,128)(2,1)} %dynamic-slice_bitcast_fusion), channel_id=1, source_target_pairs={{0,1},{1,2},{2,3},{3,0},{4,5},{5,6},{6,7},{7,4},{8,9},{9,10},{10,1... | collective-permute-start | bytes 3145736 | tf_op jit(solution)/shard_map/ppermute | solution.py:303
  49.4 18.5 %all-to-all-start.1 = ((bf16[64,2,8,128]{3,2,1,0:T(8,128)(2,1)}), bf16[64,2,8,128]{3,2,1,0:T(8,128)(2,1)S(1)}, u32[]{:S(2)}, u32[]{:S(2)}) async-start(bf16[64,2,8,128]{3,2,1,0:T(8,128)(2,1)} %shard_map.129), calls=%async_computation.1 | async-start | bytes 524288 | tf_op jit(solution)/shard_map/all_to_all | solution.py:245
  71.6 12.4 %collective-permute-start.5 = (bf16[256,2048]{1,0:T(8,128)(2,1)S(1)}, bf16[256,2048]{1,0:T(8,128)(2,1)}, u32[]{:S(2)}, u32[]{:S(2)}) collective-permute-start(bf16[256,2048]{1,0:T(8,128)(2,1)S(1)} %collective-permute-done.4.refs_4_), channel_id=1, source_target_pairs={{0,4},{4,0},{1,5},{5,1},{2,6},{6,2},{3,7},{7,3},{8,12},{12,8},{9,1... | collective-permute-start | bytes 3145736 | tf_op jit(solution)/shard_map/ppermute | solution.py:358
  72.2 11.9 %collective-permute-start.3 = (bf16[256,2048]{1,0:T(8,128)(2,1)S(1)}, bf16[256,2048]{1,0:T(8,128)(2,1)}, u32[]{:S(2)}, u32[]{:S(2)}) collective-permute-start(bf16[256,2048]{1,0:T(8,128)(2,1)S(1)} %collective-permute-done.2.refs_2_), channel_id=1, source_target_pairs={{0,4},{4,0},{1,5},{5,1},{2,6},{6,2},{3,7},{7,3},{8,12},{12,8},{9,1... | collective-permute-start | bytes 3145736 | tf_op jit(solution)/shard_map/ppermute | solution.py:358
  72.3 11.7 %collective-permute-start.1 = (bf16[256,2048]{1,0:T(8,128)(2,1)}, bf16[256,2048]{1,0:T(8,128)(2,1)}, u32[]{:S(2)}, u32[]{:S(2)}) collective-permute-start(bf16[256,2048]{1,0:T(8,128)(2,1)} %collective-permute-done.refs_0_), channel_id=1, source_target_pairs={{0,4},{4,0},{1,5},{5,1},{2,6},{6,2},{3,7},{7,3},{8,12},{12,8},{9,1... | collective-permute-start | bytes 3145736 | tf_op jit(solution)/shard_map/ppermute | solution.py:358
  72.7 11.3 %all-to-all-start.2 = ((bf16[4,96,512]{2,1,0:T(8,128)(2,1)}), bf16[4,96,512]{2,1,0:T(8,128)(2,1)S(1)}, u32[]{:S(2)}, u32[]{:S(2)}) async-start(bf16[4,96,512]{2,1,0:T(8,128)(2,1)} %bitcast.6), calls=%async_computation.2 | async-start | bytes 786432 | tf_op jit(solution)/shard_map/all_to_all | solution.py:245
  88.7 11.2 %collective-permute-start.8 = (bf16[96,2048]{1,0:T(8,128)(2,1)S(1)}, bf16[96,2048]{1,0:T(8,128)(2,1)S(1)}, u32[]{:S(2)}, u32[]{:S(2)}) collective-permute-start(bf16[96,2048]{1,0:T(8,128)(2,1)S(1)} %get-tuple-element.28.piece), channel_id=1, source_target_pairs={{0,2},{1,3},{2,0},{3,1},{4,6},{5,7},{6,4},{7,5},{8,10},{9,11},{10,... | collective-permute-start | bytes 1179656 | tf_op jit(solution)/shard_map/ppermute | solution.py:303
  89.5 39.3 %collective-permute-start.7 = (bf16[96,2048]{1,0:T(8,128)(2,1)S(1)}, bf16[96,2048]{1,0:T(8,128)(2,1)S(1)}, u32[]{:S(2)}, u32[]{:S(2)}) collective-permute-start(bf16[96,2048]{1,0:T(8,128)(2,1)S(1)} %get-tuple-element.28.piece), channel_id=1, source_target_pairs={{0,3},{1,0},{2,1},{3,2},{4,7},{5,4},{6,5},{7,6},{8,11},{9,8},{10,9... | collective-permute-start | bytes 1179656 | tf_op jit(solution)/shard_map/ppermute | solution.py:303
  91.6 37.2 %collective-permute-start.6 = (bf16[96,2048]{1,0:T(8,128)(2,1)S(1)}, bf16[96,2048]{1,0:T(8,128)(2,1)S(1)}, u32[]{:S(2)}, u32[]{:S(2)}) collective-permute-start(bf16[96,2048]{1,0:T(8,128)(2,1)S(1)} %get-tuple-element.28.piece), channel_id=1, source_target_pairs={{0,1},{1,2},{2,3},{3,0},{4,5},{5,6},{6,7},{7,4},{8,9},{9,10},{10,1... | collective-permute-start | bytes 1179656 | tf_op jit(solution)/shard_map/ppermute | solution.py:303
  126.0 12.7 %collective-permute-start.9 = (bf16[96,2048]{1,0:T(8,128)(2,1)S(1)}, bf16[96,2048]{1,0:T(8,128)(2,1)S(1)}, u32[]{:S(2)}, u32[]{:S(2)}) collective-permute-start(bf16[96,2048]{1,0:T(8,128)(2,1)S(1)} %get-tuple-element.29), channel_id=1, source_target_pairs={{0,2},{1,3},{2,0},{3,1},{4,6},{5,7},{6,4},{7,5},{8,10},{9,11},{10,... | collective-permute-start | bytes 1179656 | tf_op jit(solution)/shard_map/ppermute | solution.py:303
  133.5 13.0 %collective-permute-start.10 = (bf16[96,2048]{1,0:T(8,128)(2,1)S(1)}, bf16[96,2048]{1,0:T(8,128)(2,1)S(1)}, u32[]{:S(2)}, u32[]{:S(2)}) collective-permute-start(bf16[96,2048]{1,0:T(8,128)(2,1)S(1)} %get-tuple-element.30), channel_id=1, source_target_pairs={{0,3},{1,0},{2,1},{3,2},{4,7},{5,4},{6,5},{7,6},{8,11},{9,8},{10,9... | collective-permute-start | bytes 1179656 | tf_op jit(solution)/shard_map/ppermute | solution.py:303
  134.4 12.2 %collective-permute-start.11 = (bf16[96,2048]{1,0:T(8,128)(2,1)S(1)}, bf16[96,2048]{1,0:T(8,128)(2,1)S(1)}, u32[]{:S(2)}, u32[]{:S(2)}) collective-permute-start(bf16[96,2048]{1,0:T(8,128)(2,1)S(1)} %get-tuple-element.27), channel_id=1, source_target_pairs={{0,1},{1,2},{2,3},{3,0},{4,5},{5,6},{6,7},{7,4},{8,9},{9,10},{10,1... | collective-permute-start | bytes 1179656 | tf_op jit(solution)/shard_map/ppermute | solution.py:303
Sparse Core Ops, SparseCore 0:
  10.1 108.4 all-gather.1

commit v6 on v5

--- a/solution.py
+++ b/solution.py
@@ -85,7 +85,7 @@
 KEY_SCALES = (64**-0.5, 128**-0.5)
 
 
-def state_kernel(ld, kn, kw, v0, v1, cosine, sine, out, state):
+def state_kernel(ld, seat, kn, kw, v0, v1, cosine, sine, keep, give, state):
     length = kn.shape[0]
     keys = turned_all(kn, kw, cosine, sine, KEY_SCALES)
     t = rows((length, 128)).astype(f32)
@@ -107,7 +107,8 @@
     for d in range(2):
         for r in (6, 7):
             state[:, d, r, :] = jnp.zeros((64, 128), f32)
-    out[...] = state[...].astype(STATE)
+    keep[...] = state[pl.ds(seat[0] * 32, 32)]
+    give[...] = state[pl.ds((1 - seat[0]) * 32, 32)]
 
 
 def inside_kernel(ld, qn, qw, kn, kw, v0, v1, cosine, sine, turned_out, inside_out, turned, inside, sems):
@@ -134,14 +135,15 @@
     inside_copy.wait()
 
 
-def finish_kernel(ld, turned_in, inside_in, enter_in, g0, g1, out, turned, inside, enter, sems):
+def finish_kernel(ld, seat, turned_in, inside_in, mine, theirs, g0, g1, out, turned, inside, enter, sems):
     copies = [
         pltpu.make_async_copy(turned_in, turned, sems.at[0]),
         pltpu.make_async_copy(inside_in, inside, sems.at[1]),
     ]
     for copy in copies:
         copy.start()
-    enter[...] = enter_in[...].astype(f32)
+    enter[pl.ds(seat[0] * 32, 32)] = mine[...]
+    enter[pl.ds((1 - seat[0]) * 32, 32)] = theirs[...]
     length = turned.shape[0]
     t = rows((length, 128)).astype(f32)
     states = []
@@ -174,18 +176,43 @@
         out[:, h * 128 : (h + 1) * 128] = y.astype(bf16)
 
 
+def decay_tile(ld, d, span):
+    r = rows((8, 128))
+    rate = jnp.full((8, 128), ld[d, 1, 1], f32)
+    rate = jnp.where(r < 4, ld[d, 1, 0], rate)
+    rate = jnp.where(r == 1, ld[d, 0, 1], rate)
+    rate = jnp.where(r == 0, ld[d, 0, 0], rate)
+    return jnp.exp(rate * span)
+
+
+def pair_kernel(ld, seat, keep, got, out):
+    core = seat[0]
+    forward, backward = decay_tile(ld, 0, 384.0), decay_tile(ld, 1, 384.0)
+    low_f = jnp.where(core == 0, keep[:, 0], got[:, 0])
+    high_f = jnp.where(core == 0, got[:, 0], keep[:, 0])
+    low_b = jnp.where(core == 0, keep[:, 1], got[:, 1])
+    high_b = jnp.where(core == 0, got[:, 1], keep[:, 1])
+    out[:, 0] = (low_f * forward[None] + high_f).astype(STATE)
+    out[:, 1] = (high_b * backward[None] + low_b).astype(STATE)
+
+
+def part_kernel(ld, seat, enter, keep, got, mine, theirs):
+    core = seat[0]
+    forward, backward = decay_tile(ld, 0, 384.0), decay_tile(ld, 1, 384.0)
+    before, behind = enter[:, 0].astype(f32), enter[:, 1].astype(f32)
+    low_f = jnp.where(core == 0, keep[:, 0], got[:, 0])
+    high_b = jnp.where(core == 0, got[:, 1], keep[:, 1])
+    second_f = before * forward[None] + low_f
+    first_b = behind * backward[None] + high_b
+    mine[:, 0] = jnp.where(core == 0, before, second_f)
+    mine[:, 1] = jnp.where(core == 0, first_b, behind)
+    theirs[:, 0] = jnp.where(core == 0, second_f, before)
+    theirs[:, 1] = jnp.where(core == 0, behind, first_b)
+
+
 def scan_kernel(ld, x, out):
-    r = rows((8, 128))
-
-    def factor(d):
-        rate = jnp.full((8, 128), ld[d, 1, 1], f32)
-        rate = jnp.where(r < 4, ld[d, 1, 0], rate)
-        rate = jnp.where(r == 1, ld[d, 0, 1], rate)
-        rate = jnp.where(r == 0, ld[d, 0, 0], rate)
-        return jnp.exp(rate * 384.0)
-
     n = x.shape[0]
-    forward, backward = factor(0), factor(1)
+    forward, backward = decay_tile(ld, 0, 768.0), decay_tile(ld, 1, 768.0)
     acc = jnp.zeros((8, 128), f32)
     for k in range(n):
         out[k, 0] = acc.astype(STATE)
@@ -327,11 +354,14 @@
     cosine, sine = angle_tables(length, lax.axis_index(SP) * length)
     v0, v1 = values[:, 0], values[:, 1]
     g0, g1 = out_gate[:, 0], out_gate[:, 1]
-    states = shape(64, 2, 8, 128, dtype=STATE)
-    state = call(state_kernel, [SM] + [VM] * 6, states, (pltpu.VMEM((64, 2, 8, 128), f32),))(
-        rates, key_narrow, key_wide, v0, v1, cosine, sine
-    )
     core = lax.axis_index("sp_2")
+    seat = core[None].astype(jnp.int32)
+    halves, states = shape(32, 2, 8, 128), shape(32, 2, 8, 128, dtype=STATE)
+    keep, give = call(
+        state_kernel, [SM, SM] + [VM] * 6, (halves, halves), (pltpu.VMEM((64, 2, 8, 128), f32),)
+    )(rates, seat, key_narrow, key_wide, v0, v1, cosine, sine)
+    got = lax.ppermute(give, "sp_2", [(0, 1), (1, 0)])
+    state = call(pair_kernel, [SM, SM, VM, VM], states)(rates, seat, keep, got)
     half = lax.dynamic_index_in_dim(after(out_weight, state), core, 0, keepdims=False)
     same = []
     for s in (1, 2, 3):
@@ -344,15 +374,17 @@
         tuple(pltpu.VMEM(*k) for k in kept) + (pltpu.SemaphoreType.DMA((2,)),),
         (HB, HB),
     )(rates, query_narrow, query_wide, key_narrow, key_wide, v0, v1, cosine, sine)
-    arrived = exchanged(state, SP)
+    arrived = exchanged(state, SP[:2])
     enter = call(scan_kernel, [SM, VM], states)(rates, arrived)
-    enter = exchanged(enter, SP)
+    enter = exchanged(enter, SP[:2])
+    mine, theirs = call(part_kernel, [SM, SM, VM, VM, VM], (halves, halves))(rates, seat, enter, keep, got)
+    theirs = lax.ppermute(theirs, "sp_2", [(0, 1), (1, 0)])
     y = call(
         finish_kernel,
-        [SM, HB, HB, VM, VM, VM],
+        [SM, SM, HB, HB, VM, VM, VM, VM],
         shape(length, 512, dtype=bf16),
         (pltpu.VMEM((length, 384), bf16), pltpu.VMEM((length, 512), f32), pltpu.VMEM((64, 2, 8, 128), f32), pltpu.SemaphoreType.DMA((2,))),
-    )(rates, in_hbm(turned), in_hbm(inside), enter, g0, g1)
+    )(rates, seat, in_hbm(turned), in_hbm(inside), mine, theirs, g0, g1)
     other = []
     for s in (1, 2, 3):
         other.append(lax.ppermute(after(same[s - 1], y), "sp_2", [(0, 1), (1, 0)]))

time: 155 us -> 152 us (0.981)
  waiting for transfers between devices: 50.2 us -> 42.3 us
  blocking collectives: 27.7 us -> 34.2 us
    all_to_all x2 -> x1, waiting for transfers between devices: 15.4 us -> 7.81 us  [exchanged(): return lax.all_to_all(x, axis, 0, 0, tiled=True)]
    ppermute x0 -> x2, starting transfers between devices: none -> 6.98 us  [the longest x1 3.7 us: body(): theirs = lax.ppermute(theirs, 'sp_2', [(0, 1), (1, 0)])]
    all_to_all x1 -> x2, blocking collectives: 27.7 us -> 34.2 us  [exchanged(): return lax.all_to_all(x, axis, 0, 0, tiled=True)]
    all_to_all x2 -> x1, starting transfers between devices: 8.88 us -> 3.46 us  [exchanged(): return lax.all_to_all(x, axis, 0, 0, tiled=True)]
    ppermute x9, starting transfers between devices: 11.9 us -> 9.35 us  [shifted(): return lax.ppermute(x, 'tp', [(k, (k + by) % n) for k in range(n)])]
    all_gather x1, waiting for transfers between devices: 18.7 us -> 17 us  [body(): lax.all_gather(jnp.concatenate([mlp_gate, mlp_up, mlp_down.T], 1), SP, ax...]
    pallas_call x2 -> x4, Pallas kernels: 5.85 us -> 7.28 us  [the longest x1 3.56 us: body(): call(finish_kernel, [SM, SM, HB, HB, VM, VM, VM, VM], shape(length, 512,...]
  transfers between devices with their start and end apart: 15 -> 16, of which waited for: 6 -> 5; matrix products, arithmetic and copies ran while one was open for 5% -> 4% of each run, Pallas kernels for 20% -> 21%
where the time goes in v6:
time: 152 us
  waiting for transfers between devices  42.3 us (28%)
  blocking collectives  34.2 us (23%)
  Pallas kernels  32 us (21%)
  starting transfers between devices  20.7 us (14%)
  between operations  13.6 us (9%)
  local copies, waits for them, and re-layouts  5.13 us (3%)
  other arithmetic  3.7 us (2%)
    all_to_all x2, blocking collectives, exchanged(): return lax.all_to_all(x, axis, 0, 0, tiled=True)  34.2 us
    all_gather x1, waiting for transfers between devices, body(): lax.all_gather(jnp.concatenate([mlp_gate, mlp_up, mlp_down.T], 1), SP, ax...  17 us
    ppermute x9, waiting for transfers between devices, shifted(): return lax.ppermute(x, 'tp', [(k, (k + by) % n) for k in range(n)])  16.3 us
    ppermute x9, starting transfers between devices, shifted(): return lax.ppermute(x, 'tp', [(k, (k + by) % n) for k in range(n)])  9.35 us
    all_to_all x1, waiting for transfers between devices, exchanged(): return lax.all_to_all(x, axis, 0, 0, tiled=True)  7.81 us
    pallas_call x1, Pallas kernels, body(): call(first_mixer, [VM, HB], (own, pltpu.VMEM(shards.shape, bf16)), room(1...  7.46 us
    pallas_call x1, Pallas kernels, body(): call(near_mixer, [VM] * 3, (own, own), room(2), room=12)  4.66 us
    pallas_call x1, Pallas kernels, body(): call(proj_kernel, [SM, VM, VM, VM] + [HB] * 7, (own, own), (pltpu.VMEM((8...  4.59 us
  transfers between devices with their start and end apart: 16, of which 5 were waited for; matrix products, arithmetic and copies ran while one was open for 4% of the time, Pallas kernels for 21%

profile of v6, /device:TPU:1, one launch (start us, length us, event | category | flops | bytes accessed | tf_op | source)
XLA Modules:
  0.0 151.6 jit_solution(16348150521944255844)
XLA Ops:
  6.5 1.7 %pad_maximum_fusion = bf16[32,4224]{1,0:T(8,128)(2,1)} fusion(bf16[32,1408]{1,0:T(8,128)(2,1)} %bitcast.15, bf16[32,1408]{1,0:T(8,128)(2,1)} %param.23, bf16[32,1408]{1,0:T(8,128)(2,1)} %param.22), kind=kLoop, calls=%fused_computation.4 | loop fusion | flops 811008 | bytes 540672 | tf_op jit(solution)/shard_map/concatenate | solution.py:350
  8.4 0.8 multiply_sine_fusion
  9.2 1.9 %fusion.1 = (bf16[384,1,256]{2,1,0:T(2,128)(2,1)S(1)}, bf16[384,1,256]{2,1,0:T(2,128)(2,1)S(1)}) fusion(bf16[384,2,256]{2,1,0:T(2,128)(2,1)} %param.18), kind=kLoop, calls=%fused_computation.15 | loop fusion | bytes 786432 | tf_op jit(solution)/shard_map/slice | solution.py:355
  11.1 2.2 %shard_map.128 = (f32[32,2,8,128]{3,2,1,0:T(8,128)S(1)}, f32[32,2,8,128]{3,2,1,0:T(8,128)S(1)}) custom-call(f32[2,2,2]{2,1,0:T(2,128)} %ld.11, s32[1]{0:T(128)} %bitcast.1.seat, bf16[384,128]{1,0:T(8,128)(2,1)} %kn.3, bf16[384,256]{1,0:T(8,128)(2,1)} %kw.3, bf16[384,256]{1,0:T(8,128)(2,1)S(1)} %get-tuple-element.46.v0, ...), custom_call_target="tpu_custom_call" | custom-call | tf_op jit(solution)/shard_map/pallas_call | solution.py:360
  13.3 3.3 %collective-permute-start = (f32[32,2,8,128]{3,2,1,0:T(8,128)S(1)}, f32[32,2,8,128]{3,2,1,0:T(8,128)S(1)}, u32[]{:S(2)}, u32[]{:S(2)}) collective-permute-start(f32[32,2,8,128]{3,2,1,0:T(8,128)S(1)} %get-tuple-element.25), channel_id=1, source_target_pairs={{0,4},{4,0},{1,5},{5,1},{2,6},{6,2},{3,7},{7,3},{8,12},{12,8},{9,1... | collective-permute-start | bytes 786440 | tf_op jit(solution)/shard_map/ppermute | solution.py:363
  16.6 1.2 collective-permute-done.got
  17.7 0.8 shard_map.129
  18.5 1.3 dynamic-slice_bitcast_fusion
  19.8 1.1 collective-permute-start.6
  21.3 0.7 collective-permute-start.2
  22.0 21.0 %all_to_all.15.x = bf16[32,2,8,128]{3,2,1,0:T(8,128)(2,1)S(1)} all-to-all(bf16[32,2,8,128]{3,2,1,0:T(8,128)(2,1)S(1)} %shard_map.129), channel_id=1, replica_groups=mesh['sp_0'=8,'sp_1'=4,'sp_2'=2,'tp'=4] {'sp_0','sp_1'}, dimensions={0} | all-to-all | bytes 262144 | tf_op jit(solution)/shard_map/all_to_all | solution.py:272
  43.0 0.8 shard_map.130
  43.7 13.2 %all_to_all.16.enter = bf16[32,2,8,128]{3,2,1,0:T(8,128)(2,1)S(1)} all-to-all(bf16[32,2,8,128]{3,2,1,0:T(8,128)(2,1)S(1)} %shard_map.130), channel_id=1, replica_groups=mesh['sp_0'=8,'sp_1'=4,'sp_2'=2,'tp'=4] {'sp_0','sp_1'}, dimensions={0} | all-to-all | bytes 262144 | tf_op jit(solution)/shard_map/all_to_all | solution.py:272
  57.0 0.8 shard_map.131
  57.8 3.7 %collective-permute-start.1 = (f32[32,2,8,128]{3,2,1,0:T(8,128)S(1)}, f32[32,2,8,128]{3,2,1,0:T(8,128)S(1)}, u32[]{:S(2)}, u32[]{:S(2)}) collective-permute-start(f32[32,2,8,128]{3,2,1,0:T(8,128)S(1)} %get-tuple-element.27), channel_id=1, source_target_pairs={{0,4},{4,0},{1,5},{5,1},{2,6},{6,2},{3,7},{7,3},{8,12},{12,8},{9,1... | collective-permute-start | bytes 786440 | tf_op jit(solution)/shard_map/ppermute | solution.py:381
  61.5 1.8 %fusion = (bf16[384,1,256]{2,1,0:T(2,128)(2,1)S(1)}, bf16[384,1,256]{2,1,0:T(2,128)(2,1)S(1)}) fusion(bf16[384,2,256]{2,1,0:T(2,128)(2,1)} %param.19), kind=kLoop, calls=%fused_computation.14 | loop fusion | bytes 786432 | tf_op jit(solution)/shard_map/slice | solution.py:356
  63.3 3.6 %shard_map.127 = (bf16[384,384]{1,0:T(8,128)(2,1)}, f32[384,512]{1,0:T(8,128)}) custom-call(f32[2,2,2]{2,1,0:T(2,128)} %ld.11, bf16[384,128]{1,0:T(8,128)(2,1)} %qn.1, bf16[384,256]{1,0:T(8,128)(2,1)} %qw.1, bf16[384,128]{1,0:T(8,128)(2,1)} %kn.3, bf16[384,256]{1,0:T(8,128)(2,1)} %kw.3, bf16[384,256]{1,0:T(8,128)(2,1)S(1)} %get-tuple-element.46.v0, ...), custom_call_target="tpu_custom_call" | custom-call | tf_op jit(solution)/shard_map/pallas_call | solution.py:370
  66.9 3.6 %shard_map.132 = bf16[384,512]{1,0:T(8,128)(2,1)} custom-call(f32[2,2,2]{2,1,0:T(2,128)} %ld.11, s32[1]{0:T(128)} %bitcast.1.seat, bf16[384,384]{1,0:T(8,128)(2,1)} %get-tuple-element.22.turned_in, f32[384,512]{1,0:T(8,128)} %get-tuple-element.23.inside_in, f32[32,2,8,128]{3,2,1,0:T(8,128)S(1)} %get-tuple-element.26.mine, ...), custom_call_target="tpu_custom_call" | custom-call | tf_op jit(solution)/shard_map/pallas_call | solution.py:382
  71.4 3.5 %all-to-all-start.2 = ((bf16[4,96,512]{2,1,0:T(8,128)(2,1)}), bf16[4,96,512]{2,1,0:T(8,128)(2,1)S(1)}, u32[]{:S(2)}, u32[]{:S(2)}) async-start(bf16[4,96,512]{2,1,0:T(8,128)(2,1)} %bitcast.6), calls=%async_computation.2 | async-start | bytes 786432 | tf_op jit(solution)/shard_map/all_to_all | solution.py:272
  74.9 7.8 %all-to-all-done.2.y = bf16[4,96,512]{2,1,0:T(8,128)(2,1)S(1)} async-done(((bf16[4,96,512]{2,1,0:T(8,128)(2,1)}), bf16[4,96,512]{2,1,0:T(8,128)(2,1)S(1)}, u32[]{:S(2)}, u32[]{:S(2)}) %all-to-all-start.2) | async-done | bytes 393248 | tf_op jit(solution)/shard_map/all_to_all | solution.py:272
  82.8 4.6 %shard_map.133 = (bf16[96,2048]{1,0:T(8,128)(2,1)S(1)}, bf16[96,2048]{1,0:T(8,128)(2,1)S(1)}) custom-call(s32[2]{0:T(128)S(1)} %pad_add_fusion.place, bf16[4,96,512]{2,1,0:T(8,128)(2,1)S(1)} %all-to-all-done.2.y, bf16[96,2048]{1,0:T(8,128)(2,1)} %stream.1, f32[1,2048]{1,0:T(1,128)} %bitcast.16, bf16[2,256,2048]{2,1,0:T(8,128)(2,1)} %own.1, ...), custom_call_target="tpu_custom_call" | custom-call | tf_op jit(solution)/shard_map/pallas_call | solution.py:396
  87.9 2.3 %collective-permute-start.9 = (bf16[96,2048]{1,0:T(8,128)(2,1)S(1)}, bf16[96,2048]{1,0:T(8,128)(2,1)S(1)}, u32[]{:S(2)}, u32[]{:S(2)}) collective-permute-start(bf16[96,2048]{1,0:T(8,128)(2,1)S(1)} %get-tuple-element.36.piece), channel_id=1, source_target_pairs={{0,3},{1,0},{2,1},{3,2},{4,7},{5,4},{6,5},{7,6},{8,11},{9,8},{10,9... | collective-permute-start | bytes 1179656 | tf_op jit(solution)/shard_map/ppermute | solution.py:330
  90.2 8.4 %collective-permute-done.10.piece = bf16[96,2048]{1,0:T(8,128)(2,1)S(1)} collective-permute-done((bf16[96,2048]{1,0:T(8,128)(2,1)S(1)}, bf16[96,2048]{1,0:T(8,128)(2,1)S(1)}, u32[]{:S(2)}, u32[]{:S(2)}) %collective-permute-start.10) | collective-permute-done | bytes 393248 | tf_op jit(solution)/shard_map/ppermute | solution.py:330
  98.6 17.0 %all-gather.2.cloned.1.call-done.weights = bf16[2048,4224]{1,0:T(8,128)(2,1)} async-done(((bf16[32,4224]{1,0:T(8,128)(2,1)}), bf16[2048,4224]{1,0:T(8,128)(2,1)}) %all-gather.2.cloned.1.call-update) | async-done | bytes 17301520 | tf_op jit(solution)/shard_map/all_gather | solution.py:350
  115.7 7.5 %shard_map.134 = (bf16[96,2048]{1,0:T(8,128)(2,1)S(1)}, bf16[2048,4224]{1,0:T(8,128)(2,1)S(1)}) custom-call(bf16[96,2048]{1,0:T(8,128)(2,1)S(1)} %collective-permute-done.10.piece, bf16[2048,4224]{1,0:T(8,128)(2,1)} %all-gather.2.cloned.1.call-done.weights), custom_call_target="tpu_custom_call" | custom-call | tf_op jit(solution)/shard_map/pallas_call | solution.py:408
  123.1 2.8 %collective-permute-start.11 = (bf16[96,2048]{1,0:T(8,128)(2,1)S(1)}, bf16[96,2048]{1,0:T(8,128)(2,1)S(1)}, u32[]{:S(2)}, u32[]{:S(2)}) collective-permute-start(bf16[96,2048]{1,0:T(8,128)(2,1)S(1)} %get-tuple-element.37), channel_id=1, source_target_pairs={{0,2},{1,3},{2,0},{3,1},{4,6},{5,7},{6,4},{7,5},{8,10},{9,11},{10,... | collective-permute-start | bytes 1179656 | tf_op jit(solution)/shard_map/ppermute | solution.py:330
  125.9 4.7 %shard_map.135 = (bf16[96,2048]{1,0:T(8,128)(2,1)S(1)}, bf16[96,2048]{1,0:T(8,128)(2,1)S(1)}) custom-call(bf16[96,2048]{1,0:T(8,128)(2,1)S(1)} %collective-permute-done.8.first, bf16[96,2048]{1,0:T(8,128)(2,1)S(1)} %collective-permute-done.9.second, bf16[2048,4224]{1,0:T(8,128)(2,1)S(1)} %get-tuple-element.34.held), custom_call_target="tpu_custom_call" | custom-call | tf_op jit(solution)/shard_map/pallas_call | solution.py:416
  130.6 0.9 collective-permute-start.12
  131.6 0.6 collective-permute-start.13
  132.2 3.7 %shard_map.136 = bf16[96,2048]{1,0:T(8,128)(2,1)S(1)} custom-call(bf16[96,2048]{1,0:T(8,128)(2,1)S(1)} %get-tuple-element.36.piece, bf16[2048,4224]{1,0:T(8,128)(2,1)S(1)} %get-tuple-element.34.held), custom_call_target="tpu_custom_call" | custom-call | tf_op jit(solution)/shard_map/pallas_call | solution.py:419
  135.9 7.8 %collective-permute-done.12 = bf16[96,2048]{1,0:T(8,128)(2,1)S(1)} collective-permute-done((bf16[96,2048]{1,0:T(8,128)(2,1)S(1)}, bf16[96,2048]{1,0:T(8,128)(2,1)S(1)}, u32[]{:S(2)}, u32[]{:S(2)}) %collective-permute-start.12) | collective-permute-done | bytes 393248 | tf_op jit(solution)/shard_map/ppermute | solution.py:330
  143.7 1.1 add_convert_fusion
  (26 shorter events, 2.2 us)
Async XLA Ops:
  6.5 109.1 %all-gather.2.cloned.1.call-start = ((), (), s32[]{:S(2)}) async-start(), calls=%async_computation.3 | async-start | bytes 17571840 | tf_op jit(solution)/shard_map/all_gather | solution.py:350
  13.3 4.4 %collective-permute-start = (f32[32,2,8,128]{3,2,1,0:T(8,128)S(1)}, f32[32,2,8,128]{3,2,1,0:T(8,128)S(1)}, u32[]{:S(2)}, u32[]{:S(2)}) collective-permute-start(f32[32,2,8,128]{3,2,1,0:T(8,128)S(1)} %get-tuple-element.25), channel_id=1, source_target_pairs={{0,4},{4,0},{1,5},{5,1},{2,6},{6,2},{3,7},{7,3},{8,12},{12,8},{9,1... | collective-permute-start | bytes 786440 | tf_op jit(solution)/shard_map/ppermute | solution.py:363
  19.8 50.7 %collective-permute-start.6 = (bf16[256,2048]{1,0:T(8,128)(2,1)S(1)}, bf16[256,2048]{1,0:T(8,128)(2,1)S(1)}, u32[]{:S(2)}, u32[]{:S(2)}) collective-permute-start(bf16[256,2048]{1,0:T(8,128)(2,1)S(1)} %dynamic-slice_bitcast_fusion), channel_id=1, source_target_pairs={{0,3},{1,0},{2,1},{3,2},{4,7},{5,4},{6,5},{7,6},{8,11},{9,8},{10,9... | collective-permute-start | bytes 3145736 | tf_op jit(solution)/shard_map/ppermute | solution.py:330
  21.0 49.7 %collective-permute-start.4 = (bf16[256,2048]{1,0:T(8,128)(2,1)S(1)}, bf16[256,2048]{1,0:T(8,128)(2,1)S(1)}, u32[]{:S(2)}, u32[]{:S(2)}) collective-permute-start(bf16[256,2048]{1,0:T(8,128)(2,1)S(1)} %dynamic-slice_bitcast_fusion), channel_id=1, source_target_pairs={{0,2},{1,3},{2,0},{3,1},{4,6},{5,7},{6,4},{7,5},{8,10},{9,11},{10,... | collective-permute-start | bytes 3145736 | tf_op jit(solution)/shard_map/ppermute | solution.py:330
  21.3 49.8 %collective-permute-start.2 = (bf16[256,2048]{1,0:T(8,128)(2,1)S(1)}, bf16[256,2048]{1,0:T(8,128)(2,1)}, u32[]{:S(2)}, u32[]{:S(2)}) collective-permute-start(bf16[256,2048]{1,0:T(8,128)(2,1)S(1)} %dynamic-slice_bitcast_fusion), channel_id=1, source_target_pairs={{0,1},{1,2},{2,3},{3,0},{4,5},{5,6},{6,7},{7,4},{8,9},{9,10},{10,1... | collective-permute-start | bytes 3145736 | tf_op jit(solution)/shard_map/ppermute | solution.py:330
  57.8 9.2 %collective-permute-start.1 = (f32[32,2,8,128]{3,2,1,0:T(8,128)S(1)}, f32[32,2,8,128]{3,2,1,0:T(8,128)S(1)}, u32[]{:S(2)}, u32[]{:S(2)}) collective-permute-start(f32[32,2,8,128]{3,2,1,0:T(8,128)S(1)} %get-tuple-element.27), channel_id=1, source_target_pairs={{0,4},{4,0},{1,5},{5,1},{2,6},{6,2},{3,7},{7,3},{8,12},{12,8},{9,1... | collective-permute-start | bytes 786440 | tf_op jit(solution)/shard_map/ppermute | solution.py:381
  70.5 12.2 %collective-permute-start.7 = (bf16[256,2048]{1,0:T(8,128)(2,1)S(1)}, bf16[256,2048]{1,0:T(8,128)(2,1)}, u32[]{:S(2)}, u32[]{:S(2)}) collective-permute-start(bf16[256,2048]{1,0:T(8,128)(2,1)S(1)} %collective-permute-done.6.refs_4_), channel_id=1, source_target_pairs={{0,4},{4,0},{1,5},{5,1},{2,6},{6,2},{3,7},{7,3},{8,12},{12,8},{9,1... | collective-permute-start | bytes 3145736 | tf_op jit(solution)/shard_map/ppermute | solution.py:390
  70.6 12.1 %collective-permute-start.5 = (bf16[256,2048]{1,0:T(8,128)(2,1)S(1)}, bf16[256,2048]{1,0:T(8,128)(2,1)}, u32[]{:S(2)}, u32[]{:S(2)}) collective-permute-start(bf16[256,2048]{1,0:T(8,128)(2,1)S(1)} %collective-permute-done.4.refs_2_), channel_id=1, source_target_pairs={{0,4},{4,0},{1,5},{5,1},{2,6},{6,2},{3,7},{7,3},{8,12},{12,8},{9,1... | collective-permute-start | bytes 3145736 | tf_op jit(solution)/shard_map/ppermute | solution.py:390
  71.1 11.6 %collective-permute-start.3 = (bf16[256,2048]{1,0:T(8,128)(2,1)}, bf16[256,2048]{1,0:T(8,128)(2,1)}, u32[]{:S(2)}, u32[]{:S(2)}) collective-permute-start(bf16[256,2048]{1,0:T(8,128)(2,1)} %collective-permute-done.2.refs_0_), channel_id=1, source_target_pairs={{0,4},{4,0},{1,5},{5,1},{2,6},{6,2},{3,7},{7,3},{8,12},{12,8},{9,1... | collective-permute-start | bytes 3145736 | tf_op jit(solution)/shard_map/ppermute | solution.py:390
  71.4 11.4 %all-to-all-start.2 = ((bf16[4,96,512]{2,1,0:T(8,128)(2,1)}), bf16[4,96,512]{2,1,0:T(8,128)(2,1)S(1)}, u32[]{:S(2)}, u32[]{:S(2)}) async-start(bf16[4,96,512]{2,1,0:T(8,128)(2,1)} %bitcast.6), calls=%async_computation.2 | async-start | bytes 786432 | tf_op jit(solution)/shard_map/all_to_all | solution.py:272
  87.4 11.2 %collective-permute-start.10 = (bf16[96,2048]{1,0:T(8,128)(2,1)S(1)}, bf16[96,2048]{1,0:T(8,128)(2,1)S(1)}, u32[]{:S(2)}, u32[]{:S(2)}) collective-permute-start(bf16[96,2048]{1,0:T(8,128)(2,1)S(1)} %get-tuple-element.36.piece), channel_id=1, source_target_pairs={{0,2},{1,3},{2,0},{3,1},{4,6},{5,7},{6,4},{7,5},{8,10},{9,11},{10,... | collective-permute-start | bytes 1179656 | tf_op jit(solution)/shard_map/ppermute | solution.py:330
  87.9 38.0 %collective-permute-start.9 = (bf16[96,2048]{1,0:T(8,128)(2,1)S(1)}, bf16[96,2048]{1,0:T(8,128)(2,1)S(1)}, u32[]{:S(2)}, u32[]{:S(2)}) collective-permute-start(bf16[96,2048]{1,0:T(8,128)(2,1)S(1)} %get-tuple-element.36.piece), channel_id=1, source_target_pairs={{0,3},{1,0},{2,1},{3,2},{4,7},{5,4},{6,5},{7,6},{8,11},{9,8},{10,9... | collective-permute-start | bytes 1179656 | tf_op jit(solution)/shard_map/ppermute | solution.py:330
  90.2 35.7 %collective-permute-start.8 = (bf16[96,2048]{1,0:T(8,128)(2,1)S(1)}, bf16[96,2048]{1,0:T(8,128)(2,1)S(1)}, u32[]{:S(2)}, u32[]{:S(2)}) collective-permute-start(bf16[96,2048]{1,0:T(8,128)(2,1)S(1)} %get-tuple-element.36.piece), channel_id=1, source_target_pairs={{0,1},{1,2},{2,3},{3,0},{4,5},{5,6},{6,7},{7,4},{8,9},{9,10},{10,1... | collective-permute-start | bytes 1179656 | tf_op jit(solution)/shard_map/ppermute | solution.py:330
  123.1 12.7 %collective-permute-start.11 = (bf16[96,2048]{1,0:T(8,128)(2,1)S(1)}, bf16[96,2048]{1,0:T(8,128)(2,1)S(1)}, u32[]{:S(2)}, u32[]{:S(2)}) collective-permute-start(bf16[96,2048]{1,0:T(8,128)(2,1)S(1)} %get-tuple-element.37), channel_id=1, source_target_pairs={{0,2},{1,3},{2,0},{3,1},{4,6},{5,7},{6,4},{7,5},{8,10},{9,11},{10,... | collective-permute-start | bytes 1179656 | tf_op jit(solution)/shard_map/ppermute | solution.py:330
  130.6 13.0 %collective-permute-start.12 = (bf16[96,2048]{1,0:T(8,128)(2,1)S(1)}, bf16[96,2048]{1,0:T(8,128)(2,1)S(1)}, u32[]{:S(2)}, u32[]{:S(2)}) collective-permute-start(bf16[96,2048]{1,0:T(8,128)(2,1)S(1)} %get-tuple-element.38), channel_id=1, source_target_pairs={{0,3},{1,0},{2,1},{3,2},{4,7},{5,4},{6,5},{7,6},{8,11},{9,8},{10,9... | collective-permute-start | bytes 1179656 | tf_op jit(solution)/shard_map/ppermute | solution.py:330
  131.6 12.1 %collective-permute-start.13 = (bf16[96,2048]{1,0:T(8,128)(2,1)S(1)}, bf16[96,2048]{1,0:T(8,128)(2,1)S(1)}, u32[]{:S(2)}, u32[]{:S(2)}) collective-permute-start(bf16[96,2048]{1,0:T(8,128)(2,1)S(1)} %get-tuple-element.35), channel_id=1, source_target_pairs={{0,1},{1,2},{2,3},{3,0},{4,5},{5,6},{6,7},{7,4},{8,9},{9,10},{10,1... | collective-permute-start | bytes 1179656 | tf_op jit(solution)/shard_map/ppermute | solution.py:330
Sparse Core Ops, SparseCore 0:
  10.1 105.5 all-gather.1

commit v7 on v6

--- a/solution.py
+++ b/solution.py
@@ -65,7 +65,6 @@
 
 
 STATE = bf16
-STAGES = 4
 
 
 def turned_all(narrow, wide, cosine, sine, scales):
@@ -272,17 +271,23 @@
     return lax.all_to_all(x, axis, 0, 0, tiled=True)
 
 
-def weight_parts(width, units):
-    step = width // STAGES
-    spans = [pl.ds(k * step, step) for k in range(STAGES)]
-    return spans, [(span, pl.ds(at, size)) for at, size in ((0, 2 * units), (2 * units, units)) for span in spans]
+RISING = (512, 512, 512, 256, 256)
+FALLING = (512, 512, 512, 512)
+
+
+def row_spans(sizes):
+    return [pl.ds(sum(sizes[:k]), size) for k, size in enumerate(sizes)]
+
+
+def weight_parts(units):
+    rising = [(span, pl.ds(0, 2 * units)) for span in row_spans(RISING)]
+    return rising + [(span, pl.ds(2 * units, units)) for span in row_spans(FALLING)]
 
 
 def mixed_into(pieces, held, outs, act, hidden, ready):
     n = pieces[0].shape[0]
     units = hidden.shape[1]
-    spans, _ = weight_parts(held.shape[0], units)
-    for k, span in enumerate(spans):
+    for k, span in enumerate(row_spans(RISING)):
         x = jnp.concatenate([p[:, span] for p in pieces], 0)
         ready(k)
         part = nn(x, held[span, : 2 * units])
@@ -290,15 +295,15 @@
     gate = act[:, :units]
     hidden[...] = (gate * jax.nn.sigmoid(gate) * act[:, units:]).astype(bf16)
     h = hidden[...]
-    for k, span in enumerate(spans):
-        ready(STAGES + k)
+    for k, span in enumerate(row_spans(FALLING)):
+        ready(len(RISING) + k)
         part = nt(h, held[span, 2 * units :]).astype(bf16)
         for j, out in enumerate(outs):
             out[:, span] = part[j * n : (j + 1) * n]
 
 
 def first_mixer(piece, weights, out, held, act, hidden, sems):
-    _, parts = weight_parts(held.shape[0], hidden.shape[1])
+    parts = weight_parts(hidden.shape[1])
     copies = [pltpu.make_async_copy(weights.at[p], held.at[p], sems.at[k]) for k, p in enumerate(parts)]
     for copy in copies:
         copy.start()
@@ -409,7 +414,7 @@
         first_mixer,
         [VM, HB],
         (own, pltpu.VMEM(shards.shape, bf16)),
-        room(1) + (pltpu.SemaphoreType.DMA((2 * STAGES,)),),
+        room(1) + (pltpu.SemaphoreType.DMA((len(RISING) + len(FALLING),)),),
         room=12,
     )(around[2], in_hbm(shards))
     arrivals = [shifted(to_second, 2)]

time: 152 us -> 152 us (level)
  transfers between devices with their start and end apart: 16 -> 16, of which waited for: 5 -> 6; matrix products, arithmetic and copies ran while one was open for 4% -> 4% of each run, Pallas kernels for 21% -> 21%
where the time goes in v7:
time: 152 us; the launch traced here: 151 us
  waiting for transfers between devices  42.3 us (28%)
  blocking collectives  34.2 us (23%)
  Pallas kernels  31.8 us (21%)
  starting transfers between devices  20.7 us (14%)
  between operations  13.6 us (9%)
  local copies, waits for them, and re-layouts  5.13 us (3%)
  other arithmetic  3.7 us (2%)
    all_to_all x2, blocking collectives, exchanged(): return lax.all_to_all(x, axis, 0, 0, tiled=True)  34.2 us
    all_gather x1, waiting for transfers between devices, body(): lax.all_gather(jnp.concatenate([mlp_gate, mlp_up, mlp_down.T], 1), SP, ax...  17 us
    ppermute x9, waiting for transfers between devices, shifted(): return lax.ppermute(x, 'tp', [(k, (k + by) % n) for k in range(n)])  16.2 us
    ppermute x9, starting transfers between devices, shifted(): return lax.ppermute(x, 'tp', [(k, (k + by) % n) for k in range(n)])  9.35 us
    all_to_all x1, waiting for transfers between devices, exchanged(): return lax.all_to_all(x, axis, 0, 0, tiled=True)  7.81 us
    pallas_call x1, Pallas kernels, body(): call(first_mixer, [VM, HB], (own, pltpu.VMEM(shards.shape, bf16)), room(1...  7.18 us
    pallas_call x1, Pallas kernels, body(): call(near_mixer, [VM] * 3, (own, own), room(2), room=12)  4.61 us
    pallas_call x1, Pallas kernels, body(): call(proj_kernel, [SM, VM, VM, VM] + [HB] * 7, (own, own), (pltpu.VMEM((8...  4.59 us
  transfers between devices with their start and end apart: 16, of which 6 were waited for; matrix products, arithmetic and copies ran while one was open for 4% of the time, Pallas kernels for 21%

profile of v7, /device:TPU:1, one launch (start us, length us, event | category | flops | bytes accessed | tf_op | source)
XLA Modules:
  0.0 151.3 jit_solution(396721559575976479)
XLA Ops:
  6.5 1.7 %pad_maximum_fusion = bf16[32,4224]{1,0:T(8,128)(2,1)} fusion(bf16[32,1408]{1,0:T(8,128)(2,1)} %bitcast.15, bf16[32,1408]{1,0:T(8,128)(2,1)} %param.23, bf16[32,1408]{1,0:T(8,128)(2,1)} %param.22), kind=kLoop, calls=%fused_computation.4 | loop fusion | flops 811008 | bytes 540672 | tf_op jit(solution)/shard_map/concatenate | solution.py:355
  8.4 0.8 multiply_sine_fusion
  9.2 1.9 %fusion.1 = (bf16[384,1,256]{2,1,0:T(2,128)(2,1)S(1)}, bf16[384,1,256]{2,1,0:T(2,128)(2,1)S(1)}) fusion(bf16[384,2,256]{2,1,0:T(2,128)(2,1)} %param.18), kind=kLoop, calls=%fused_computation.15 | loop fusion | bytes 786432 | tf_op jit(solution)/shard_map/slice | solution.py:360
  11.1 2.2 %shard_map.128 = (f32[32,2,8,128]{3,2,1,0:T(8,128)S(1)}, f32[32,2,8,128]{3,2,1,0:T(8,128)S(1)}) custom-call(f32[2,2,2]{2,1,0:T(2,128)} %ld.11, s32[1]{0:T(128)} %bitcast.1.seat, bf16[384,128]{1,0:T(8,128)(2,1)} %kn.3, bf16[384,256]{1,0:T(8,128)(2,1)} %kw.3, bf16[384,256]{1,0:T(8,128)(2,1)S(1)} %get-tuple-element.46.v0, ...), custom_call_target="tpu_custom_call" | custom-call | tf_op jit(solution)/shard_map/pallas_call | solution.py:365
  13.3 3.3 %collective-permute-start = (f32[32,2,8,128]{3,2,1,0:T(8,128)S(1)}, f32[32,2,8,128]{3,2,1,0:T(8,128)S(1)}, u32[]{:S(2)}, u32[]{:S(2)}) collective-permute-start(f32[32,2,8,128]{3,2,1,0:T(8,128)S(1)} %get-tuple-element.25), channel_id=1, source_target_pairs={{0,4},{4,0},{1,5},{5,1},{2,6},{6,2},{3,7},{7,3},{8,12},{12,8},{9,1... | collective-permute-start | bytes 786440 | tf_op jit(solution)/shard_map/ppermute | solution.py:368
  16.6 1.2 collective-permute-done.got
  17.7 0.8 shard_map.129
  18.5 1.3 dynamic-slice_bitcast_fusion
  19.8 1.1 collective-permute-start.6
  21.3 0.7 collective-permute-start.2
  22.0 21.0 %all_to_all.15.x = bf16[32,2,8,128]{3,2,1,0:T(8,128)(2,1)S(1)} all-to-all(bf16[32,2,8,128]{3,2,1,0:T(8,128)(2,1)S(1)} %shard_map.129), channel_id=1, replica_groups=mesh['sp_0'=8,'sp_1'=4,'sp_2'=2,'tp'=4] {'sp_0','sp_1'}, dimensions={0} | all-to-all | bytes 262144 | tf_op jit(solution)/shard_map/all_to_all | solution.py:271
  43.0 0.8 shard_map.130
  43.7 13.2 %all_to_all.16.enter = bf16[32,2,8,128]{3,2,1,0:T(8,128)(2,1)S(1)} all-to-all(bf16[32,2,8,128]{3,2,1,0:T(8,128)(2,1)S(1)} %shard_map.130), channel_id=1, replica_groups=mesh['sp_0'=8,'sp_1'=4,'sp_2'=2,'tp'=4] {'sp_0','sp_1'}, dimensions={0} | all-to-all | bytes 262144 | tf_op jit(solution)/shard_map/all_to_all | solution.py:271
  57.0 0.8 shard_map.131
  57.8 3.7 %collective-permute-start.1 = (f32[32,2,8,128]{3,2,1,0:T(8,128)S(1)}, f32[32,2,8,128]{3,2,1,0:T(8,128)S(1)}, u32[]{:S(2)}, u32[]{:S(2)}) collective-permute-start(f32[32,2,8,128]{3,2,1,0:T(8,128)S(1)} %get-tuple-element.27), channel_id=1, source_target_pairs={{0,4},{4,0},{1,5},{5,1},{2,6},{6,2},{3,7},{7,3},{8,12},{12,8},{9,1... | collective-permute-start | bytes 786440 | tf_op jit(solution)/shard_map/ppermute | solution.py:386
  61.5 1.8 %fusion = (bf16[384,1,256]{2,1,0:T(2,128)(2,1)S(1)}, bf16[384,1,256]{2,1,0:T(2,128)(2,1)S(1)}) fusion(bf16[384,2,256]{2,1,0:T(2,128)(2,1)} %param.19), kind=kLoop, calls=%fused_computation.14 | loop fusion | bytes 786432 | tf_op jit(solution)/shard_map/slice | solution.py:361
  63.3 3.6 %shard_map.127 = (bf16[384,384]{1,0:T(8,128)(2,1)}, f32[384,512]{1,0:T(8,128)}) custom-call(f32[2,2,2]{2,1,0:T(2,128)} %ld.11, bf16[384,128]{1,0:T(8,128)(2,1)} %qn.1, bf16[384,256]{1,0:T(8,128)(2,1)} %qw.1, bf16[384,128]{1,0:T(8,128)(2,1)} %kn.3, bf16[384,256]{1,0:T(8,128)(2,1)} %kw.3, bf16[384,256]{1,0:T(8,128)(2,1)S(1)} %get-tuple-element.46.v0, ...), custom_call_target="tpu_custom_call" | custom-call | tf_op jit(solution)/shard_map/pallas_call | solution.py:375
  66.9 3.6 %shard_map.132 = bf16[384,512]{1,0:T(8,128)(2,1)} custom-call(f32[2,2,2]{2,1,0:T(2,128)} %ld.11, s32[1]{0:T(128)} %bitcast.1.seat, bf16[384,384]{1,0:T(8,128)(2,1)} %get-tuple-element.22.turned_in, f32[384,512]{1,0:T(8,128)} %get-tuple-element.23.inside_in, f32[32,2,8,128]{3,2,1,0:T(8,128)S(1)} %get-tuple-element.26.mine, ...), custom_call_target="tpu_custom_call" | custom-call | tf_op jit(solution)/shard_map/pallas_call | solution.py:387
  71.4 3.5 %all-to-all-start.2 = ((bf16[4,96,512]{2,1,0:T(8,128)(2,1)}), bf16[4,96,512]{2,1,0:T(8,128)(2,1)S(1)}, u32[]{:S(2)}, u32[]{:S(2)}) async-start(bf16[4,96,512]{2,1,0:T(8,128)(2,1)} %bitcast.6), calls=%async_computation.2 | async-start | bytes 786432 | tf_op jit(solution)/shard_map/all_to_all | solution.py:271
  74.9 7.8 %all-to-all-done.2.y = bf16[4,96,512]{2,1,0:T(8,128)(2,1)S(1)} async-done(((bf16[4,96,512]{2,1,0:T(8,128)(2,1)}), bf16[4,96,512]{2,1,0:T(8,128)(2,1)S(1)}, u32[]{:S(2)}, u32[]{:S(2)}) %all-to-all-start.2) | async-done | bytes 393248 | tf_op jit(solution)/shard_map/all_to_all | solution.py:271
  82.8 4.6 %shard_map.133 = (bf16[96,2048]{1,0:T(8,128)(2,1)S(1)}, bf16[96,2048]{1,0:T(8,128)(2,1)S(1)}) custom-call(s32[2]{0:T(128)S(1)} %pad_add_fusion.place, bf16[4,96,512]{2,1,0:T(8,128)(2,1)S(1)} %all-to-all-done.2.y, bf16[96,2048]{1,0:T(8,128)(2,1)} %stream.1, f32[1,2048]{1,0:T(1,128)} %bitcast.16, bf16[2,256,2048]{2,1,0:T(8,128)(2,1)} %own.1, ...), custom_call_target="tpu_custom_call" | custom-call | tf_op jit(solution)/shard_map/pallas_call | solution.py:401
  87.9 2.3 %collective-permute-start.9 = (bf16[96,2048]{1,0:T(8,128)(2,1)S(1)}, bf16[96,2048]{1,0:T(8,128)(2,1)S(1)}, u32[]{:S(2)}, u32[]{:S(2)}) collective-permute-start(bf16[96,2048]{1,0:T(8,128)(2,1)S(1)} %get-tuple-element.36.piece), channel_id=1, source_target_pairs={{0,3},{1,0},{2,1},{3,2},{4,7},{5,4},{6,5},{7,6},{8,11},{9,8},{10,9... | collective-permute-start | bytes 1179656 | tf_op jit(solution)/shard_map/ppermute | solution.py:335
  90.2 8.4 %collective-permute-done.10.piece = bf16[96,2048]{1,0:T(8,128)(2,1)S(1)} collective-permute-done((bf16[96,2048]{1,0:T(8,128)(2,1)S(1)}, bf16[96,2048]{1,0:T(8,128)(2,1)S(1)}, u32[]{:S(2)}, u32[]{:S(2)}) %collective-permute-start.10) | collective-permute-done | bytes 393248 | tf_op jit(solution)/shard_map/ppermute | solution.py:335
  98.6 17.0 %all-gather.2.cloned.1.call-done.weights = bf16[2048,4224]{1,0:T(8,128)(2,1)} async-done(((bf16[32,4224]{1,0:T(8,128)(2,1)}), bf16[2048,4224]{1,0:T(8,128)(2,1)}) %all-gather.2.cloned.1.call-update) | async-done | bytes 17301520 | tf_op jit(solution)/shard_map/all_gather | solution.py:355
  115.7 7.2 %shard_map.134 = (bf16[96,2048]{1,0:T(8,128)(2,1)S(1)}, bf16[2048,4224]{1,0:T(8,128)(2,1)S(1)}) custom-call(bf16[96,2048]{1,0:T(8,128)(2,1)S(1)} %collective-permute-done.10.piece, bf16[2048,4224]{1,0:T(8,128)(2,1)} %all-gather.2.cloned.1.call-done.weights), custom_call_target="tpu_custom_call" | custom-call | tf_op jit(solution)/shard_map/pallas_call | solution.py:413
  122.8 2.8 %collective-permute-start.11 = (bf16[96,2048]{1,0:T(8,128)(2,1)S(1)}, bf16[96,2048]{1,0:T(8,128)(2,1)S(1)}, u32[]{:S(2)}, u32[]{:S(2)}) collective-permute-start(bf16[96,2048]{1,0:T(8,128)(2,1)S(1)} %get-tuple-element.37), channel_id=1, source_target_pairs={{0,2},{1,3},{2,0},{3,1},{4,6},{5,7},{6,4},{7,5},{8,10},{9,11},{10,... | collective-permute-start | bytes 1179656 | tf_op jit(solution)/shard_map/ppermute | solution.py:335
  125.7 4.6 %shard_map.135 = (bf16[96,2048]{1,0:T(8,128)(2,1)S(1)}, bf16[96,2048]{1,0:T(8,128)(2,1)S(1)}) custom-call(bf16[96,2048]{1,0:T(8,128)(2,1)S(1)} %collective-permute-done.8.first, bf16[96,2048]{1,0:T(8,128)(2,1)S(1)} %collective-permute-done.9.second, bf16[2048,4224]{1,0:T(8,128)(2,1)S(1)} %get-tuple-element.34.held), custom_call_target="tpu_custom_call" | custom-call | tf_op jit(solution)/shard_map/pallas_call | solution.py:421
  130.3 0.9 collective-permute-start.12
  131.2 0.6 collective-permute-start.13
  131.8 3.8 %shard_map.136 = bf16[96,2048]{1,0:T(8,128)(2,1)S(1)} custom-call(bf16[96,2048]{1,0:T(8,128)(2,1)S(1)} %get-tuple-element.36.piece, bf16[2048,4224]{1,0:T(8,128)(2,1)S(1)} %get-tuple-element.34.held), custom_call_target="tpu_custom_call" | custom-call | tf_op jit(solution)/shard_map/pallas_call | solution.py:424
  135.6 7.7 %collective-permute-done.12 = bf16[96,2048]{1,0:T(8,128)(2,1)S(1)} collective-permute-done((bf16[96,2048]{1,0:T(8,128)(2,1)S(1)}, bf16[96,2048]{1,0:T(8,128)(2,1)S(1)}, u32[]{:S(2)}, u32[]{:S(2)}) %collective-permute-start.12) | collective-permute-done | bytes 393248 | tf_op jit(solution)/shard_map/ppermute | solution.py:335
  143.4 1.1 add_convert_fusion
  (26 shorter events, 2.2 us)
Async XLA Ops:
  6.5 109.1 %all-gather.2.cloned.1.call-start = ((), (), s32[]{:S(2)}) async-start(), calls=%async_computation.3 | async-start | bytes 17571840 | tf_op jit(solution)/shard_map/all_gather | solution.py:355
  13.3 4.4 %collective-permute-start = (f32[32,2,8,128]{3,2,1,0:T(8,128)S(1)}, f32[32,2,8,128]{3,2,1,0:T(8,128)S(1)}, u32[]{:S(2)}, u32[]{:S(2)}) collective-permute-start(f32[32,2,8,128]{3,2,1,0:T(8,128)S(1)} %get-tuple-element.25), channel_id=1, source_target_pairs={{0,4},{4,0},{1,5},{5,1},{2,6},{6,2},{3,7},{7,3},{8,12},{12,8},{9,1... | collective-permute-start | bytes 786440 | tf_op jit(solution)/shard_map/ppermute | solution.py:368
  19.8 50.7 %collective-permute-start.6 = (bf16[256,2048]{1,0:T(8,128)(2,1)S(1)}, bf16[256,2048]{1,0:T(8,128)(2,1)S(1)}, u32[]{:S(2)}, u32[]{:S(2)}) collective-permute-start(bf16[256,2048]{1,0:T(8,128)(2,1)S(1)} %dynamic-slice_bitcast_fusion), channel_id=1, source_target_pairs={{0,3},{1,0},{2,1},{3,2},{4,7},{5,4},{6,5},{7,6},{8,11},{9,8},{10,9... | collective-permute-start | bytes 3145736 | tf_op jit(solution)/shard_map/ppermute | solution.py:335
  21.0 49.7 %collective-permute-start.4 = (bf16[256,2048]{1,0:T(8,128)(2,1)S(1)}, bf16[256,2048]{1,0:T(8,128)(2,1)S(1)}, u32[]{:S(2)}, u32[]{:S(2)}) collective-permute-start(bf16[256,2048]{1,0:T(8,128)(2,1)S(1)} %dynamic-slice_bitcast_fusion), channel_id=1, source_target_pairs={{0,2},{1,3},{2,0},{3,1},{4,6},{5,7},{6,4},{7,5},{8,10},{9,11},{10,... | collective-permute-start | bytes 3145736 | tf_op jit(solution)/shard_map/ppermute | solution.py:335
  21.3 49.8 %collective-permute-start.2 = (bf16[256,2048]{1,0:T(8,128)(2,1)S(1)}, bf16[256,2048]{1,0:T(8,128)(2,1)}, u32[]{:S(2)}, u32[]{:S(2)}) collective-permute-start(bf16[256,2048]{1,0:T(8,128)(2,1)S(1)} %dynamic-slice_bitcast_fusion), channel_id=1, source_target_pairs={{0,1},{1,2},{2,3},{3,0},{4,5},{5,6},{6,7},{7,4},{8,9},{9,10},{10,1... | collective-permute-start | bytes 3145736 | tf_op jit(solution)/shard_map/ppermute | solution.py:335
  57.8 9.2 %collective-permute-start.1 = (f32[32,2,8,128]{3,2,1,0:T(8,128)S(1)}, f32[32,2,8,128]{3,2,1,0:T(8,128)S(1)}, u32[]{:S(2)}, u32[]{:S(2)}) collective-permute-start(f32[32,2,8,128]{3,2,1,0:T(8,128)S(1)} %get-tuple-element.27), channel_id=1, source_target_pairs={{0,4},{4,0},{1,5},{5,1},{2,6},{6,2},{3,7},{7,3},{8,12},{12,8},{9,1... | collective-permute-start | bytes 786440 | tf_op jit(solution)/shard_map/ppermute | solution.py:386
  70.5 12.2 %collective-permute-start.7 = (bf16[256,2048]{1,0:T(8,128)(2,1)S(1)}, bf16[256,2048]{1,0:T(8,128)(2,1)}, u32[]{:S(2)}, u32[]{:S(2)}) collective-permute-start(bf16[256,2048]{1,0:T(8,128)(2,1)S(1)} %collective-permute-done.6.refs_4_), channel_id=1, source_target_pairs={{0,4},{4,0},{1,5},{5,1},{2,6},{6,2},{3,7},{7,3},{8,12},{12,8},{9,1... | collective-permute-start | bytes 3145736 | tf_op jit(solution)/shard_map/ppermute | solution.py:395
  70.6 12.1 %collective-permute-start.5 = (bf16[256,2048]{1,0:T(8,128)(2,1)S(1)}, bf16[256,2048]{1,0:T(8,128)(2,1)}, u32[]{:S(2)}, u32[]{:S(2)}) collective-permute-start(bf16[256,2048]{1,0:T(8,128)(2,1)S(1)} %collective-permute-done.4.refs_2_), channel_id=1, source_target_pairs={{0,4},{4,0},{1,5},{5,1},{2,6},{6,2},{3,7},{7,3},{8,12},{12,8},{9,1... | collective-permute-start | bytes 3145736 | tf_op jit(solution)/shard_map/ppermute | solution.py:395
  71.1 11.6 %collective-permute-start.3 = (bf16[256,2048]{1,0:T(8,128)(2,1)}, bf16[256,2048]{1,0:T(8,128)(2,1)}, u32[]{:S(2)}, u32[]{:S(2)}) collective-permute-start(bf16[256,2048]{1,0:T(8,128)(2,1)} %collective-permute-done.2.refs_0_), channel_id=1, source_target_pairs={{0,4},{4,0},{1,5},{5,1},{2,6},{6,2},{3,7},{7,3},{8,12},{12,8},{9,1... | collective-permute-start | bytes 3145736 | tf_op jit(solution)/shard_map/ppermute | solution.py:395
  71.4 11.4 %all-to-all-start.2 = ((bf16[4,96,512]{2,1,0:T(8,128)(2,1)}), bf16[4,96,512]{2,1,0:T(8,128)(2,1)S(1)}, u32[]{:S(2)}, u32[]{:S(2)}) async-start(bf16[4,96,512]{2,1,0:T(8,128)(2,1)} %bitcast.6), calls=%async_computation.2 | async-start | bytes 786432 | tf_op jit(solution)/shard_map/all_to_all | solution.py:271
  87.4 11.2 %collective-permute-start.10 = (bf16[96,2048]{1,0:T(8,128)(2,1)S(1)}, bf16[96,2048]{1,0:T(8,128)(2,1)S(1)}, u32[]{:S(2)}, u32[]{:S(2)}) collective-permute-start(bf16[96,2048]{1,0:T(8,128)(2,1)S(1)} %get-tuple-element.36.piece), channel_id=1, source_target_pairs={{0,2},{1,3},{2,0},{3,1},{4,6},{5,7},{6,4},{7,5},{8,10},{9,11},{10,... | collective-permute-start | bytes 1179656 | tf_op jit(solution)/shard_map/ppermute | solution.py:335
  87.9 37.7 %collective-permute-start.9 = (bf16[96,2048]{1,0:T(8,128)(2,1)S(1)}, bf16[96,2048]{1,0:T(8,128)(2,1)S(1)}, u32[]{:S(2)}, u32[]{:S(2)}) collective-permute-start(bf16[96,2048]{1,0:T(8,128)(2,1)S(1)} %get-tuple-element.36.piece), channel_id=1, source_target_pairs={{0,3},{1,0},{2,1},{3,2},{4,7},{5,4},{6,5},{7,6},{8,11},{9,8},{10,9... | collective-permute-start | bytes 1179656 | tf_op jit(solution)/shard_map/ppermute | solution.py:335
  90.2 35.5 %collective-permute-start.8 = (bf16[96,2048]{1,0:T(8,128)(2,1)S(1)}, bf16[96,2048]{1,0:T(8,128)(2,1)S(1)}, u32[]{:S(2)}, u32[]{:S(2)}) collective-permute-start(bf16[96,2048]{1,0:T(8,128)(2,1)S(1)} %get-tuple-element.36.piece), channel_id=1, source_target_pairs={{0,1},{1,2},{2,3},{3,0},{4,5},{5,6},{6,7},{7,4},{8,9},{9,10},{10,1... | collective-permute-start | bytes 1179656 | tf_op jit(solution)/shard_map/ppermute | solution.py:335
  122.8 12.8 %collective-permute-start.11 = (bf16[96,2048]{1,0:T(8,128)(2,1)S(1)}, bf16[96,2048]{1,0:T(8,128)(2,1)S(1)}, u32[]{:S(2)}, u32[]{:S(2)}) collective-permute-start(bf16[96,2048]{1,0:T(8,128)(2,1)S(1)} %get-tuple-element.37), channel_id=1, source_target_pairs={{0,2},{1,3},{2,0},{3,1},{4,6},{5,7},{6,4},{7,5},{8,10},{9,11},{10,... | collective-permute-start | bytes 1179656 | tf_op jit(solution)/shard_map/ppermute | solution.py:335
  130.3 13.1 %collective-permute-start.12 = (bf16[96,2048]{1,0:T(8,128)(2,1)S(1)}, bf16[96,2048]{1,0:T(8,128)(2,1)S(1)}, u32[]{:S(2)}, u32[]{:S(2)}) collective-permute-start(bf16[96,2048]{1,0:T(8,128)(2,1)S(1)} %get-tuple-element.38), channel_id=1, source_target_pairs={{0,3},{1,0},{2,1},{3,2},{4,7},{5,4},{6,5},{7,6},{8,11},{9,8},{10,9... | collective-permute-start | bytes 1179656 | tf_op jit(solution)/shard_map/ppermute | solution.py:335
  131.2 12.2 %collective-permute-start.13 = (bf16[96,2048]{1,0:T(8,128)(2,1)S(1)}, bf16[96,2048]{1,0:T(8,128)(2,1)S(1)}, u32[]{:S(2)}, u32[]{:S(2)}) collective-permute-start(bf16[96,2048]{1,0:T(8,128)(2,1)S(1)} %get-tuple-element.35), channel_id=1, source_target_pairs={{0,1},{1,2},{2,3},{3,0},{4,5},{5,6},{6,7},{7,4},{8,9},{9,10},{10,1... | collective-permute-start | bytes 1179656 | tf_op jit(solution)/shard_map/ppermute | solution.py:335
Sparse Core Ops, SparseCore 0:
  10.1 105.5 all-gather.1
